TPU v7x, 256 devices: a whole 4x4x8 slice. The times are simulated.
256 devices in a mesh: ep: 64 (over z, y, core), tp: 4 (over x).
Axes of the slice: x: 4, y: 4, z: 8, core: 2. Of those that a mesh axis runs over, the one named last changes fastest.
Arguments:
- tokens: bfloat16 [16384, 1024], P('ep'), may hold values from -6 to 6
- cotangent: bfloat16 [16384, 1024], P('ep'), may hold values from -1.5 to 1.5
- routing: int32 [16384, 2], P('ep'), may hold values from 0 to 127, all different within a row; in each aligned block of 256 rows (0 to 255, 256 to 511, ...) at most 12 rows name the same one
- gate_weights: float32 [16384, 2], P('ep'), may hold values from 0.1 to 0.9
- gate_proj: bfloat16 [128, 1024, 512], P('ep', None, 'tp'), may hold values from -0.1875 to 0.1875
- up_proj: bfloat16 [128, 1024, 512], P('ep', None, 'tp'), may hold values from -0.1875 to 0.1875
- down_proj: bfloat16 [128, 512, 1024], P('ep', 'tp'), may hold values from -0.25 to 0.25
Outputs:
- tokens_grad: bfloat16 [16384, 1024], P('ep')
- gates_grad: float32 [16384, 2], P('ep')
- gate_proj_grad: float32 [128, 1024, 512], P('ep', None, 'tp')
- up_proj_grad: float32 [128, 1024, 512], P('ep', None, 'tp')
- down_proj_grad: float32 [128, 512, 1024], P('ep', 'tp')
Inputs may be any that keep to these rules, and one draw needn't show every extreme that they name: `routing`: each row names 2 different experts; every expert is named by some row; within each aligned block of 256 rows (the tokens of one index of ep) no expert is named by more than 12 rows, a bound that some block reaches.
All inputs are finite; a program needn't handle non-finite values.
Results may differ from a plain program's by a relative error of at most 0.0015.
Values may be sent and summed in bfloat16 or wider, within the bound.
No kernel may reach another device: no remote copies, remote signals or barrier semaphores. Data moves between devices by JAX's collectives and lax.ppermute only.
A program may use at most 128 MiB of HBM per device.

v0:
```python
import jax
import jax.numpy as jnp
from jax import lax
from jax.experimental import pallas as pl
from jax.experimental.pallas import tpu as pltpu
from jax.sharding import PartitionSpec as P

F32 = jnp.float32
BF16 = jnp.bfloat16
LANES = 128
VMEM = pltpu.VMEM
SMEM = pltpu.SMEM


def mm(a, b, dims):
    return lax.dot_general(a, b, (dims, ((), ())), preferred_element_type=F32)


def dispatch_kernel(
    experts, local_experts, quarter, member, routing, weights, tokens, cotangent, rows_out, pick
):
    token_count = tokens.shape[0]
    row_count = rows_out.shape[0]
    slots = row_count // 2
    lane = lax.broadcasted_iota(jnp.int32, (token_count, experts), 1)
    chosen = [routing[:, k : k + 1] for k in range(2)]
    onehot = [jnp.where(lane == c, 1.0, 0.0) for c in chosen]
    earlier = lax.broadcasted_iota(jnp.int32, (token_count, token_count), 0)
    later = lax.broadcasted_iota(jnp.int32, (token_count, token_count), 1)
    lower = jnp.where(earlier > later, 1.0, 0.0).astype(BF16)
    before = mm(lower, (onehot[0] + onehot[1]).astype(BF16), ((1,), (0,)))
    row = lax.broadcasted_iota(jnp.int32, (token_count, row_count), 1)
    slot = lax.broadcasted_iota(jnp.int32, (token_count, slots), 1)
    cot = cotangent[...].astype(F32)
    total = None
    token_pick = None
    per_device = local_experts * quarter
    for k in range(2):
        position = jnp.sum(onehot[k] * before, axis=1, keepdims=True).astype(jnp.int32)
        local = position - member[0] * quarter
        present = (local >= 0) & (local < quarter)
        device = chosen[k] // local_experts
        within = (chosen[k] - device * local_experts) * quarter + local
        slot_of = jnp.where(present, device * per_device + within, -1)
        pick[k] = jnp.where(slot == slot_of, 1.0, 0.0).astype(BF16)
        token_row = jnp.where(present, device * (2 * per_device) + within, -1)
        scaled_row = jnp.where(present, device * (2 * per_device) + per_device + within, -1)
        hit = jnp.where(row == token_row, 1.0, 0.0)
        token_pick = hit if token_pick is None else token_pick + hit
        scaled = (weights[:, k : k + 1] * cot).astype(BF16)
        part = mm(jnp.where(row == scaled_row, 1.0, 0.0).astype(BF16), scaled, ((0,), (0,)))
        total = part if total is None else total + part
    total = total + mm(token_pick.astype(BF16), tokens[...], ((0,), (0,)))
    rows_out[...] = total.astype(BF16)


def hidden_terms(rows, scaled, gate, up, down):
    gate_pre = mm(rows, gate, ((1,), (0,))).astype(BF16).astype(F32)
    up_pre = mm(rows, up, ((1,), (0,))).astype(BF16).astype(F32)
    hidden_grad = mm(scaled, down, ((1,), (1,)))
    sigmoid = jax.nn.sigmoid(gate_pre)
    activated = gate_pre * sigmoid
    hidden = activated * up_pre
    gate_grad = (hidden_grad * up_pre * sigmoid * (1.0 + gate_pre * (1.0 - sigmoid))).astype(BF16)
    up_grad = (hidden_grad * activated).astype(BF16)
    return hidden, hidden_grad, gate_grad, up_grad


def input_kernel(rows, scaled, gate, up, down, out):
    width = rows.shape[-1]
    hidden, hidden_grad, gate_grad, up_grad = hidden_terms(
        rows[0, 0], scaled[0, 0], gate[0, 0], up[0, 0], down[0, 0]
    )
    product = jnp.sum(hidden_grad * hidden, axis=1, keepdims=True)
    grad = mm(gate_grad, gate[0, 0], ((1,), (1,))) + mm(up_grad, up[0, 0], ((1,), (1,)))
    tail = jnp.broadcast_to(product, (product.shape[0], LANES))

    @pl.when(pl.program_id(1) == 0)
    def _():
        out[0, :, :width] = grad
        out[0, :, width:] = tail

    @pl.when(pl.program_id(1) != 0)
    def _():
        out[0, :, :width] += grad
        out[0, :, width:] += tail


def weight_kernel(rows, scaled, gate, up, down, gate_out, up_out, down_out):
    own_rows, own_scaled = rows[0, 0, 0], scaled[0, 0, 0]
    hidden, _, gate_grad, up_grad = hidden_terms(own_rows, own_scaled, gate[0], up[0], down[0])
    gate_part = mm(own_rows, gate_grad, ((0,), (0,)))
    up_part = mm(own_rows, up_grad, ((0,), (0,)))
    down_part = mm(hidden.astype(BF16), own_scaled, ((0,), (0,)))

    @pl.when(pl.program_id(1) == 0)
    def _():
        gate_out[0] = gate_part
        up_out[0] = up_part
        down_out[0] = down_part

    @pl.when(pl.program_id(1) != 0)
    def _():
        gate_out[0] += gate_part
        up_out[0] += up_part
        down_out[0] += down_part


def split3(value):
    high = value.astype(BF16)
    rest = value - high.astype(F32)
    middle = rest.astype(BF16)
    low = (rest - middle.astype(F32)).astype(BF16)
    return high, middle, low


def combine_kernel(back, pick, grad_out, product_out):
    width = grad_out.shape[-1]
    both = pick[0] + pick[1]
    dims = ((1,), (0,))
    grad_out[...] = sum(mm(both, part, dims) for part in split3(back[:, :width]))
    tails = split3(back[:, width:])
    first = sum(mm(pick[0], part, dims) for part in tails)
    second = sum(mm(pick[1], part, dims) for part in tails)
    lane = lax.broadcasted_iota(jnp.int32, first.shape, 1)
    product_out[...] = jnp.where(lane == 0, first, second)


def shards(tokens, cotangent, routing, gate_weights, gate_proj, up_proj, down_proj):
    token_count, model_width = tokens.shape
    top_count = routing.shape[1]
    local_experts, _, hidden_width = gate_proj.shape
    groups = lax.axis_size("ep")
    members = lax.axis_size("tp")
    experts = local_experts * groups
    capacity = members * (
        (3 * token_count * top_count + experts * members - 1) // (experts * members)
    )
    quarter = capacity // members
    slots = experts * quarter
    own = groups * quarter
    member = lax.axis_index("tp").astype(jnp.int32).reshape(1)

    gate_all = lax.all_gather(gate_proj, "tp")
    up_all = lax.all_gather(up_proj, "tp")
    down_all = lax.all_gather(down_proj, "tp")

    whole = pl.BlockSpec(memory_space=VMEM)
    send, pick = pl.pallas_call(
        lambda *refs: dispatch_kernel(experts, local_experts, quarter, *refs),
        out_shape=(
            jax.ShapeDtypeStruct((2 * slots, model_width), BF16),
            jax.ShapeDtypeStruct((2, token_count, slots), BF16),
        ),
        in_specs=[pl.BlockSpec(memory_space=SMEM), whole, whole, whole, whole],
        out_specs=(whole, whole),
        name="dispatch",
    )(member, routing, gate_weights, tokens, cotangent)
    send = send.reshape(groups, 2, local_experts, quarter, model_width)
    landed = lax.all_to_all(send, "ep", split_axis=0, concat_axis=0, tiled=True)
    own_rows = landed.transpose(1, 2, 0, 3, 4).reshape(2, local_experts, own, model_width)
    all_rows = lax.all_gather(own_rows, "tp")

    tail_width = model_width + LANES
    grid = (local_experts, members)
    back = pl.pallas_call(
        input_kernel,
        grid=grid,
        out_shape=jax.ShapeDtypeStruct((local_experts, own, tail_width), F32),
        in_specs=[
            pl.BlockSpec((1, 1, own, model_width), lambda e, t: (0, e, 0, 0)),
            pl.BlockSpec((1, 1, own, model_width), lambda e, t: (1, e, 0, 0)),
            pl.BlockSpec((1, 1, model_width, hidden_width), lambda e, t: (t, e, 0, 0)),
            pl.BlockSpec((1, 1, model_width, hidden_width), lambda e, t: (t, e, 0, 0)),
            pl.BlockSpec((1, 1, hidden_width, model_width), lambda e, t: (t, e, 0, 0)),
        ],
        out_specs=pl.BlockSpec((1, own, tail_width), lambda e, t: (e, 0, 0)),
        name="input_grad",
    )(own_rows, own_rows, gate_all, up_all, down_all)
    back = back.reshape(local_experts, groups, quarter, tail_width).transpose(1, 0, 2, 3)
    back = lax.all_to_all(back, "ep", split_axis=0, concat_axis=0, tiled=True)
    token_grad, product = pl.pallas_call(
        combine_kernel,
        out_shape=(
            jax.ShapeDtypeStruct((token_count, model_width), F32),
            jax.ShapeDtypeStruct((token_count, LANES), F32),
        ),
        in_specs=[whole, whole],
        out_specs=(whole, whole),
        name="combine",
    )(back.reshape(slots, tail_width), pick)
    total_grad, total_product = lax.psum((token_grad, product[:, :top_count]), "tp")
    tokens_grad = total_grad.astype(BF16)
    gates_grad = total_product / gate_weights

    gate_grad, up_grad, down_grad = pl.pallas_call(
        weight_kernel,
        grid=grid,
        out_shape=(
            jax.ShapeDtypeStruct((local_experts, model_width, hidden_width), F32),
            jax.ShapeDtypeStruct((local_experts, model_width, hidden_width), F32),
            jax.ShapeDtypeStruct((local_experts, hidden_width, model_width), F32),
        ),
        in_specs=[
            pl.BlockSpec((1, 1, 1, own, model_width), lambda e, t: (t, 0, e, 0, 0)),
            pl.BlockSpec((1, 1, 1, own, model_width), lambda e, t: (t, 1, e, 0, 0)),
            pl.BlockSpec((1, model_width, hidden_width), lambda e, t: (e, 0, 0)),
            pl.BlockSpec((1, model_width, hidden_width), lambda e, t: (e, 0, 0)),
            pl.BlockSpec((1, hidden_width, model_width), lambda e, t: (e, 0, 0)),
        ],
        out_specs=(
            pl.BlockSpec((1, model_width, hidden_width), lambda e, t: (e, 0, 0)),
            pl.BlockSpec((1, model_width, hidden_width), lambda e, t: (e, 0, 0)),
            pl.BlockSpec((1, hidden_width, model_width), lambda e, t: (e, 0, 0)),
        ),
        name="weight_grad",
    )(all_rows, all_rows, gate_proj, up_proj, down_proj)
    return (tokens_grad, gates_grad, gate_grad, up_grad, down_grad)


def solution(mesh):
    in_specs = (
        P("ep", None),
        P("ep", None),
        P("ep", None),
        P("ep", None),
        P("ep", None, "tp"),
        P("ep", None, "tp"),
        P("ep", "tp", None),
    )
    out_specs = (
        P("ep", None),
        P("ep", None),
        P("ep", None, "tp"),
        P("ep", None, "tp"),
        P("ep", "tp", None),
    )
    return jax.shard_map(shards, mesh=mesh, in_specs=in_specs, out_specs=out_specs, check_vma=False)
```

profile of v0, /device:TPU:14, one launch (start us, length us, event | category | flops | bytes accessed | tf_op | source)
XLA Modules:
  0.0 245.3 jit_solution(6639819353612344235)
XLA Ops:
  7.2 0.7 all-gather.10.cloned.1.call-update
  7.9 0.7 all-gather.12.cloned.1.call-update
  8.7 0.7 all-gather.14.cloned.1.call-update
  9.4 0.0 all-gather.8.cloned.1.call-start
  9.4 1.5 copy.30.refs_2_
  10.9 1.5 copy.29.refs_1_
  12.4 4.6 %dispatch.1 = (bf16[768,1024]{1,0:T(8,128)(2,1)}, bf16[2,256,384]{2,1,0:T(8,128)(2,1)}) custom-call(s32[1]{0:T(128)} %bitcast.refs_0_, s32[256,2]{1,0:T(8,128)} %copy.29.refs_1_, f32[256,2]{1,0:T(8,128)} %copy.30.refs_2_, bf16[256,1024]{1,0:T(8,128)(2,1)} %refs_3_.1, bf16[256,1024]{1,0:T(8,128)(2,1)} %refs_4_.1), custom_call_target="tpu_custom_call" | custom-call | tf_op jit(solution)/shard_map/dispatch/pallas_call | solution.py:149
  17.0 4.0 %reshape.26 = bf16[64,2,2,3,1024]{4,3,2,1,0:T(4,128)(2,1)S(1)} reshape(bf16[768,1024]{1,0:T(8,128)(2,1)} %get-tuple-element.12) | data formatting | bytes 3145728 | tf_op jit(solution)/shard_map/reshape | solution.py:159
  21.0 1.4 copy.31
  22.4 52.0 %all_to_all.10 = bf16[64,2,2,3,1024]{4,2,3,1,0:T(2,128)(2,1)S(1)} all-to-all(bf16[64,2,2,3,1024]{4,2,3,1,0:T(2,128)(2,1)S(1)} %copy.31), channel_id=1, replica_groups=mesh['ep'=64,'tp'=4] {'ep'}, dimensions={0} | all-to-all | bytes 3145728 | tf_op jit(solution)/shard_map/all_to_all | solution.py:160
  74.3 1.1 copy.32
  75.4 1.6 copy.39
  77.1 1.6 copy.33.rows.scaled
  78.7 0.4 all-gather.12.cloned.1.call-done
  79.1 35.1 %all-gather.14.cloned.1.call-done = bf16[8,128,1024]{2,1,0:T(8,128)(2,1)} async-done(((bf16[2,128,1024]{2,1,0:T(8,128)(2,1)}), bf16[8,128,1024]{2,1,0:T(8,128)(2,1)}) %all-gather.14.cloned.1.call-update) | async-done | bytes 2097168 | tf_op jit(solution)/shard_map/all_gather | solution.py:146
  114.2 12.4 %input_grad.1 = f32[2,192,1152]{2,1,0:T(8,128)} custom-call(bf16[2,2,192,1024]{3,2,1,0:T(8,128)(2,1)} %copy.33.rows.scaled, bf16[2,2,192,1024]{3,2,1,0:T(8,128)(2,1)} %copy.33.rows.scaled, bf16[4,2,1024,128]{3,2,1,0:T(8,128)(2,1)} %bitcast.15, bf16[4,2,1024,128]{3,2,1,0:T(8,128)(2,1)} %bitcast.16, bf16[4,2,128,1024]{3,2,1,0:T(8,128)(2,1)} %bitcast.17), custom_call_target="tpu_custom_call" | custom-call | tf_op jit(solution)/shard_map/input_grad/pallas_call | solution.py:166
  126.6 2.8 %copy.35 = f32[2,192,1152]{2,0,1:T(2,128)S(1)} copy(f32[2,192,1152]{2,1,0:T(8,128)} %input_grad.1) | data formatting | bytes 3538944 | tf_op jit(solution)/shard_map/input_grad/pallas_call | solution.py:166
  129.4 54.9 %all_to_all.11 = f32[64,2,3,1152]{3,1,2,0:T(2,128)S(1)} all-to-all(f32[64,2,3,1152]{3,1,2,0:T(2,128)S(1)} %bitcast.13), channel_id=1, replica_groups=mesh['ep'=64,'tp'=4] {'ep'}, dimensions={0} | all-to-all | bytes 3538944 | tf_op jit(solution)/shard_map/all_to_all | solution.py:181
  184.3 0.6 copy.36
  184.9 1.8 reshape.29.back
  186.7 3.6 %combine.1 = (f32[256,1024]{1,0:T(8,128)}, f32[256,128]{1,0:T(8,128)}) custom-call(f32[384,1152]{1,0:T(8,128)} %reshape.29.back, bf16[2,256,384]{2,1,0:T(8,128)(2,1)} %get-tuple-element.13.pick), custom_call_target="tpu_custom_call" | custom-call | tf_op jit(solution)/shard_map/combine/pallas_call | solution.py:182
  190.4 34.6 %all-reduce.2 = (bf16[256,1024]{1,0:T(8,128)(2,1)}, f32[256,2]{1,0:T(8,128)S(1)}) all-reduce(f32[256,1024]{1,0:T(8,128)} %get-tuple-element.14, f32[256,2]{1,0:T(8,128)} %bitcast.18), channel_id=1, replica_groups=mesh['ep'=64,'tp'=4] {'tp'}, use_global_device_ids=true, to_apply=%region_0.0 | all-reduce | flops 262656 | bytes 1576960 | tf_op jit(solution)/shard_map/psum | solution.py:192
  225.0 0.7 copy.40
  225.7 13.0 %weight_grad.1 = (f32[2,1024,128]{2,1,0:T(8,128)}, f32[2,1024,128]{2,1,0:T(8,128)}, f32[2,128,1024]{2,1,0:T(8,128)}) custom-call(bf16[4,2,2,192,1024]{4,3,2,1,0:T(8,128)(2,1)} %all-gather.8.cloned.1.call-done.rows.scaled, bf16[4,2,2,192,1024]{4,3,2,1,0:T(8,128)(2,1)} %all-gather.8.cloned.1.call-done.rows.scaled, bf16[2,1024,128]{2,1,0:T(8,128)(2,1)} %gate.1, ...), custom_call_target="tpu_custom_call" | custom-call | tf_op jit(solution)/shard_map/weight_grad/pallas_call | solution.py:196
  (9 shorter events, 0.2 us)
Async XLA Ops:
  7.2 71.5 %all-gather.10.cloned.1.call-start = ((), (), s32[]{:S(2)}) async-start(), calls=%async_computation.3 | async-start | bytes 2621440 | tf_op jit(solution)/shard_map/all_gather | solution.py:144
  7.9 71.2 %all-gather.12.cloned.1.call-start = ((), (), s32[]{:S(2)}) async-start(), calls=%async_computation.4 | async-start | bytes 2621440 | tf_op jit(solution)/shard_map/all_gather | solution.py:145
  8.6 105.5 %all-gather.14.cloned.1.call-start = ((), (), s32[]{:S(2)}) async-start(), calls=%async_computation.5 | async-start | bytes 2621440 | tf_op jit(solution)/shard_map/all_gather | solution.py:146
  9.4 216.3 %all-gather.8.cloned.1.call-start = ((), (), s32[]{:S(2)}) async-start(), calls=%async_computation.2 | async-start | bytes 7864320 | tf_op jit(solution)/shard_map/all_gather | solution.py:162
  186.7 38.3 %copy-start = (f32[256,2]{1,0:T(8,128)S(1)}, f32[256,2]{1,0:T(8,128)}, u32[]{:S(2)}) copy-start(f32[256,2]{1,0:T(8,128)} %copy.30.refs_2_) | copy-start | bytes 6148
Sparse Core Ops, SparseCore 0:
  9.8 34.1 all-gather.9
  45.8 33.2 all-gather.11
  80.9 33.2 all-gather.13
  115.8 68.7 all-gather.7
where the time goes:
time: 246 us; the launch traced here: 245 us
  blocking collectives  141 us (57%)
  waiting for transfers between devices  37.6 us (15%)
  Pallas kernels  33.6 us (14%)
  local copies, waits for them, and re-layouts  18.6 us (8%)
  between operations  13.8 us (6%)
    all_to_all x1, blocking collectives, shards(): back = lax.all_to_all(back, 'ep', split_axis=0, concat_axis=0, tiled=True)  54.9 us
    all_to_all x1, blocking collectives, shards(): landed = lax.all_to_all(send, 'ep', split_axis=0, concat_axis=0, tiled=True)  52 us
    all_gather x1, waiting for transfers between devices, shards(): down_all = lax.all_gather(down_proj, 'tp')  35.1 us
    psum x1, blocking collectives, shards(): lax.psum((token_grad, product[:, :top_count]), 'tp')  34.6 us
    pallas_call x1, Pallas kernels, shards(): pl.pallas_call(weight_kernel, grid=grid, out_shape=(jax.ShapeDtypeStruct(...  13 us
    pallas_call x1, Pallas kernels, shards(): pl.pallas_call(input_kernel, grid=grid, out_shape=jax.ShapeDtypeStruct((l...  12.4 us
    reshape x2, local copies, waits for them, and re-layouts, shards(): send = send.reshape(groups, 2, local_experts, quarter, model_width)  5.36 us
  transfers between devices with their start and end apart: 4, of which 2 were waited for; matrix products, arithmetic and copies ran while one was open for 8% of the time, Pallas kernels for 8%

commit v1 on v0

v1 whole, which is shorter than its diff:
```python
import jax
import jax.numpy as jnp
from jax import lax
from jax.experimental import pallas as pl
from jax.experimental.pallas import tpu as pltpu
from jax.sharding import PartitionSpec as P

F32 = jnp.float32
F16 = jnp.float16
BF16 = jnp.bfloat16
I32 = jnp.int32
LANES = 128
HALVES = 2
SPREAD = 16384.0
VMEM = pltpu.VMEM
SMEM = pltpu.SMEM
NN = ((1,), (0,))
NT = ((1,), (1,))
TN = ((0,), (0,))


def mm(a, b, dims=NN):
    return lax.dot_general(a, b, (dims, ((), ())), preferred_element_type=F32)


def iota(shape, dim):
    return lax.broadcasted_iota(I32, shape, dim)


def split3(value):
    high = value.astype(BF16)
    rest = value - high.astype(F32)
    middle = rest.astype(BF16)
    low = (rest - middle.astype(F32)).astype(BF16)
    return high, middle, low


def exponent(value):
    return jnp.floor(jnp.log(jnp.maximum(value, 1e-30)) * 1.4426950408889634)


def dispatch_kernel(
    experts, local_experts, quarter, member, routing, weights, tokens, cotangent, rows_out, pick
):
    token_count, width = tokens.shape
    half = width // HALVES
    row_count = rows_out.shape[0]
    slots = pick.shape[1]
    group = local_experts * quarter
    chunk = HALVES * 2 * group
    expert = iota((experts, token_count), 0)
    chosen = [routing[k : k + 1, :] for k in range(2)]
    onehot = [jnp.where(expert == c, 1.0, 0.0) for c in chosen]
    earlier = iota((token_count, token_count), 0)
    later = iota((token_count, token_count), 1)
    upper = jnp.where(earlier < later, 1.0, 0.0).astype(BF16)
    before = mm((onehot[0] + onehot[1]).astype(BF16), upper)
    row = iota((row_count, token_count), 0)
    slot = iota((slots, token_count), 0)
    token_rows = []
    for k in range(2):
        position = jnp.sum(onehot[k] * before, axis=0, keepdims=True).astype(I32)
        local = position - member[0] * quarter
        present = (local >= 0) & (local < quarter)
        device = chosen[k] // local_experts
        within = (chosen[k] - device * local_experts) * quarter + local
        pick[k] = jnp.where(slot == jnp.where(present, device * group + within, -1), 1.0, 0.0).astype(BF16)
        token_rows.append(jnp.where(present, device * chunk + within, -chunk))
    total = None
    for h in range(HALVES):
        columns = slice(h * half, (h + 1) * half)
        base = h * 2 * group
        hits = [jnp.where(row == r + base, 1.0, 0.0) for r in token_rows]
        part = mm((hits[0] + hits[1]).astype(BF16), tokens[:, columns])
        hits = [jnp.where(row == r + (base + group), 1.0, 0.0) for r in token_rows]
        slot_weight = jnp.sum(hits[0] * weights[0:1, :] + hits[1] * weights[1:2, :], axis=1, keepdims=True)
        part = part + slot_weight * mm((hits[0] + hits[1]).astype(BF16), cotangent[:, columns])
        total = part if total is None else total + part
    rows_out[...] = total.astype(BF16)


def land(source, expert, local_experts, quarter, rows, scaled, offset):
    half = source.shape[1]
    group = local_experts * quarter
    chunk = HALVES * 2 * group
    devices = 16
    out_rows = devices * quarter
    index = iota((HALVES * 2 * out_rows, devices * chunk), 0)
    column = iota((HALVES * 2 * out_rows, devices * chunk), 1)
    kind = index // out_rows
    rest = index - kind * out_rows
    device = rest // quarter
    wanted = device * chunk + kind * group + expert * quarter + (rest - device * quarter)
    permutation = jnp.where(column == wanted, 1.0, 0.0).astype(BF16)
    for block in range(source.shape[0] // (devices * chunk)):
        moved = mm(permutation, source[block * devices * chunk : (block + 1) * devices * chunk, :])
        moved = moved.astype(BF16)
        at = slice(offset + block * out_rows, offset + (block + 1) * out_rows)
        for h in range(HALVES):
            columns = slice(h * half, (h + 1) * half)
            first = 2 * h * out_rows
            rows[at, columns] = moved[first : first + out_rows]
            scaled[at, columns] = moved[first + out_rows : first + 2 * out_rows]


def hidden_terms(gate_pre, up_pre, hidden_grad):
    gate_pre = gate_pre.astype(BF16).astype(F32)
    up_pre = up_pre.astype(BF16).astype(F32)
    sigmoid = jax.nn.sigmoid(gate_pre)
    activated = gate_pre * sigmoid
    hidden = activated * up_pre
    gate_grad = (hidden_grad * up_pre * sigmoid * (1.0 + gate_pre * (1.0 - sigmoid))).astype(BF16)
    up_grad = (hidden_grad * activated).astype(BF16)
    return hidden, gate_grad, up_grad


def input_kernel(local_experts, quarter, landed, *refs):
    gates, ups, downs = refs[0:4], refs[4:8], refs[8:11]
    down_even, down_odd, out, rows, scaled = refs[11:]
    width = rows.shape[1]
    expert = pl.program_id(0)
    land(landed, expert, local_experts, quarter, rows, scaled, 0)
    gate = jnp.concatenate([g[0] for g in gates], axis=1)
    up = jnp.concatenate([u[0] for u in ups], axis=1)
    last = jnp.where(expert == 0, down_even[0], down_odd[0])
    down = jnp.concatenate([d[0] for d in downs] + [last], axis=0)
    hidden_grad = mm(scaled[...], down, NT)
    hidden, gate_grad, up_grad = hidden_terms(mm(rows[...], gate), mm(rows[...], up), hidden_grad)
    product = jnp.sum(hidden_grad * hidden, axis=1, keepdims=True)
    grad = mm(gate_grad, gate, NT) + mm(up_grad, up, NT)
    power = exponent(jnp.max(jnp.abs(grad), axis=1, keepdims=True))
    out[0, :, :width] = grad * (SPREAD * jnp.exp2(-power))
    product_power = exponent(jnp.abs(product))
    product = product * jnp.exp2(-product_power)
    high = product.astype(BF16).astype(F32)
    low = (product - high) * 256.0
    lane = iota((product.shape[0], LANES), 1)
    out[0, :, width:] = jnp.where(
        lane == 0,
        power,
        jnp.where(lane == 1, product_power, jnp.where(lane == 2, high, low)),
    )


def weight_kernel(local_experts, quarter, *refs):
    sources, (gate, up, down), (gate_out, up_out, down_out) = refs[0:5], refs[5:8], refs[8:11]
    rows, scaled = refs[11:]
    expert = pl.program_id(0)
    offset = 0
    chunk = HALVES * 2 * local_experts * quarter
    for source in sources:
        land(source, expert, local_experts, quarter, rows, scaled, offset)
        offset += source.shape[0] // chunk * quarter
    hidden_width = gate.shape[2]
    both = mm(rows[...], jnp.concatenate([gate[0], up[0]], axis=1))
    hidden_grad = mm(scaled[...], down[0], NT)
    hidden, gate_grad, up_grad = hidden_terms(both[:, :hidden_width], both[:, hidden_width:], hidden_grad)
    grads = mm(rows[...], jnp.concatenate([gate_grad, up_grad], axis=1), TN)
    gate_out[0] = grads[:, :hidden_width]
    up_out[0] = grads[:, hidden_width:]
    down_out[0] = mm(hidden.astype(BF16), scaled[...], TN)


def combine_kernel(back, pick, grad_out, product_out):
    width = grad_out.shape[-1]
    both = pick[0] + pick[1]
    power = back[:, width : width + 1]
    grad = back[:, :width] * (jnp.exp2(power) * (1.0 / SPREAD))
    grad_out[...] = sum(mm(both, part, TN) for part in split3(grad))
    high, low = back[:, width + 2 : width + 3], back[:, width + 3 : width + 4]
    product = (high + low * (1.0 / 256.0)) * jnp.exp2(back[:, width + 1 : width + 2])
    parts = split3(jnp.broadcast_to(product, (product.shape[0], LANES)))
    first = sum(mm(pick[0], part, TN) for part in parts)
    second = sum(mm(pick[1], part, TN) for part in parts)
    lane = iota(first.shape, 1)
    product_out[...] = jnp.where(lane == 0, first, second)


def shards(tokens, cotangent, routing, gate_weights, gate_proj, up_proj, down_proj):
    token_count, model_width = tokens.shape
    top_count = routing.shape[1]
    local_experts, _, hidden_width = gate_proj.shape
    groups = lax.axis_size("ep")
    members = lax.axis_size("tp")
    experts = local_experts * groups
    capacity = members * (
        (3 * token_count * top_count + experts * members - 1) // (experts * members)
    )
    quarter = capacity // members
    slots = experts * quarter
    own = groups * quarter
    chunk = HALVES * 2 * local_experts * quarter
    half = model_width // HALVES
    member = lax.axis_index("tp").astype(I32).reshape(1)
    right = [(i, (i + 1) % members) for i in range(members)]
    left = [(i, (i - 1) % members) for i in range(members)]

    gates, ups, downs = [gate_proj], [up_proj], [down_proj]
    for kept, mine in ((gates, gate_proj), (ups, up_proj), (downs, down_proj)):
        kept.append(lax.ppermute(mine, "tp", right))
        kept.append(lax.ppermute(mine, "tp", left))
    gates.append(lax.ppermute(gates[2], "tp", left))
    ups.append(lax.ppermute(ups[1], "tp", right))
    down_even = lax.ppermute(downs[2][0:1], "tp", left)
    down_odd = lax.ppermute(downs[1][1:2], "tp", right)

    whole = pl.BlockSpec(memory_space=VMEM)
    send, pick = pl.pallas_call(
        lambda *refs: dispatch_kernel(experts, local_experts, quarter, *refs),
        out_shape=(
            jax.ShapeDtypeStruct((groups * chunk, half), BF16),
            jax.ShapeDtypeStruct((2, slots, token_count), BF16),
        ),
        in_specs=[pl.BlockSpec(memory_space=SMEM), whole, whole, whole, whole],
        out_specs=(whole, whole),
        name="dispatch",
    )(member, routing.T, gate_weights.T, tokens, cotangent)
    landed = lax.all_to_all(
        send.reshape(groups, chunk, half), "ep", split_axis=0, concat_axis=0, tiled=True
    ).reshape(groups * chunk, half)

    from_left = lax.ppermute(landed, "tp", right)
    from_right = lax.ppermute(landed, "tp", left)
    middle = groups * chunk // 2
    opposite_low = lax.ppermute(from_right[:middle], "tp", left)
    opposite_high = lax.ppermute(from_left[middle:], "tp", right)

    tail_width = model_width + LANES
    spec_in = pl.BlockSpec((1, model_width, hidden_width), lambda e: (e, 0, 0))
    spec_down = pl.BlockSpec((1, hidden_width, model_width), lambda e: (e, 0, 0))
    spec_one = pl.BlockSpec((1, hidden_width, model_width), lambda e: (0, 0, 0))

    def rows_spec(array):
        return pl.BlockSpec(array.shape, lambda e: (0, 0))

    back = pl.pallas_call(
        lambda *refs: input_kernel(local_experts, quarter, *refs),
        grid=(local_experts,),
        out_shape=jax.ShapeDtypeStruct((local_experts, own, tail_width), F32),
        in_specs=[rows_spec(landed)] + [spec_in] * 8 + [spec_down] * 3 + [spec_one] * 2,
        out_specs=pl.BlockSpec((1, own, tail_width), lambda e: (e, 0, 0)),
        scratch_shapes=[VMEM((own, model_width), BF16)] * 2,
        name="input_grad",
    )(landed, *gates, *ups, *downs, down_even, down_odd)
    back = back.astype(F16).reshape(local_experts, groups, quarter, tail_width).transpose(1, 0, 2, 3)
    back = lax.all_to_all(back, "ep", split_axis=0, concat_axis=0, tiled=True)
    back = back.astype(F32).reshape(slots, tail_width)
    token_grad, product = pl.pallas_call(
        combine_kernel,
        out_shape=(
            jax.ShapeDtypeStruct((token_count, model_width), F32),
            jax.ShapeDtypeStruct((token_count, LANES), F32),
        ),
        in_specs=[whole, whole],
        out_specs=(whole, whole),
        name="combine",
    )(back, pick)
    total_grad, total_product = lax.psum((token_grad, product[:, :top_count]), "tp")
    tokens_grad = total_grad.astype(BF16)
    gates_grad = total_product / gate_weights

    sources = (landed, from_left, from_right, opposite_low, opposite_high)
    all_rows = members * own
    gate_grad, up_grad, down_grad = pl.pallas_call(
        lambda *refs: weight_kernel(local_experts, quarter, *refs),
        grid=(local_experts,),
        out_shape=(
            jax.ShapeDtypeStruct((local_experts, model_width, hidden_width), F32),
            jax.ShapeDtypeStruct((local_experts, model_width, hidden_width), F32),
            jax.ShapeDtypeStruct((local_experts, hidden_width, model_width), F32),
        ),
        in_specs=[rows_spec(s) for s in sources] + [spec_in, spec_in, spec_down],
        out_specs=(spec_in, spec_in, spec_down),
        scratch_shapes=[VMEM((all_rows, model_width), BF16)] * 2,
        name="weight_grad",
    )(*sources, gate_proj, up_proj, down_proj)
    return (tokens_grad, gates_grad, gate_grad, up_grad, down_grad)


def solution(mesh):
    in_specs = (
        P("ep", None),
        P("ep", None),
        P("ep", None),
        P("ep", None),
        P("ep", None, "tp"),
        P("ep", None, "tp"),
        P("ep", "tp", None),
    )
    out_specs = (
        P("ep", None),
        P("ep", None),
        P("ep", None, "tp"),
        P("ep", None, "tp"),
        P("ep", "tp", None),
    )
    return jax.shard_map(shards, mesh=mesh, in_specs=in_specs, out_specs=out_specs, check_vma=False)
```

time: 246 us -> 202 us (0.82)
  blocking collectives: 141 us -> 40.3 us
  starting transfers between devices: 0.15 us -> 41.6 us
  waiting for transfers between devices: 37.6 us -> 76.4 us
  between operations: 13.8 us -> 0.87 us
  local copies, waits for them, and re-layouts: 18.6 us -> 11.3 us
  Pallas kernels: 33.6 us -> 29.5 us
    all_to_all x2 -> x0, blocking collectives: 107 us -> none  [the longest x1 54.9 us: shards(): back = lax.all_to_all(back, 'ep', split_axis=0, concat_axis=0, tiled=True)]
    ppermute x0 -> x14, waiting for transfers between devices: none -> 76.4 us  [the longest x1 34.4 us: shards(): from_right = lax.ppermute(landed, 'tp', left)]
    all_gather x4 -> x0, waiting for transfers between devices: 35.5 us -> none  [the longest x1 35.1 us: shards(): down_all = lax.all_gather(down_proj, 'tp')]
    all_to_all x0 -> x2, starting transfers between devices: none -> 22.6 us  [the longest x1 12.2 us: shards(): lax.all_to_all(send.reshape(groups, chunk, half), 'ep', split_axis=0, con...]
    ppermute x0 -> x14, starting transfers between devices: none -> 19 us  [the longest x3 5.67 us: shards(): kept.append(lax.ppermute(mine, 'tp', right))]
    reshape x4 -> x2, local copies, waits for them, and re-layouts: 8.79 us -> 3.05 us  [shards(): back = back.astype(F32).reshape(slots, tail_width)]
    psum x1, blocking collectives: 34.6 us -> 40.3 us  [shards(): lax.psum((token_grad, product[:, :top_count]), 'tp')]
    pallas_call x2, Pallas kernels: 25.4 us -> 20.1 us  [the longest x1 11.7 us: shards(): pl.pallas_call(lambda *refs: weight_kernel(local_experts, quarter, *refs)...]
  transfers between devices with their start and end apart: 4 -> 16, of which waited for: 2 -> 5; matrix products, arithmetic and copies ran while one was open for 8% -> 4% of each run, Pallas kernels for 8% -> 2%
where the time goes in v1:
time: 202 us
  waiting for transfers between devices  76.4 us (38%)
  starting transfers between devices  41.6 us (21%)
  blocking collectives  40.3 us (20%)
  Pallas kernels  29.5 us (15%)
  local copies, waits for them, and re-layouts  11.3 us (6%)
    psum x1, blocking collectives, shards(): lax.psum((token_grad, product[:, :top_count]), 'tp')  40.3 us
    ppermute x1, waiting for transfers between devices, shards(): from_right = lax.ppermute(landed, 'tp', left)  34.4 us
    ppermute x3, waiting for transfers between devices, shards(): kept.append(lax.ppermute(mine, 'tp', left))  20.6 us
    ppermute x1, waiting for transfers between devices, shards(): down_even = lax.ppermute(downs[2][0:1], 'tp', left)  12.8 us
    all_to_all x1, starting transfers between devices, shards(): lax.all_to_all(send.reshape(groups, chunk, half), 'ep', split_axis=0, con...  12.2 us
    pallas_call x1, Pallas kernels, shards(): pl.pallas_call(lambda *refs: weight_kernel(local_experts, quarter, *refs)...  11.7 us
    all_to_all x1, starting transfers between devices, shards(): back = lax.all_to_all(back, 'ep', split_axis=0, concat_axis=0, tiled=True)  10.3 us
    ppermute x3, waiting for transfers between devices, shards(): kept.append(lax.ppermute(mine, 'tp', right))  8.69 us
  transfers between devices with their start and end apart: 16, of which 5 were waited for; matrix products, arithmetic and copies ran while one was open for 4% of the time, Pallas kernels for 2%

profile of v1, /device:TPU:14, one launch (start us, length us, event | category | flops | bytes accessed | tf_op | source)
XLA Modules:
  0.0 201.6 jit_solution(6998254576505718893)
XLA Ops:
  0.6 5.6 %dispatch.1 = (bf16[1536,512]{1,0:T(8,128)(2,1)}, bf16[2,384,256]{2,1,0:T(8,128)(2,1)}) custom-call(s32[1]{0:T(128)} %bitcast.refs_0_, s32[2,256]{1,0:T(2,128)} %bitcast.16, f32[2,256]{1,0:T(2,128)} %bitcast.15, bf16[256,1024]{1,0:T(8,128)(2,1)} %refs_3_.1, bf16[256,1024]{1,0:T(8,128)(2,1)} %refs_4_.1), custom_call_target="tpu_custom_call" | custom-call | tf_op jit(solution)/shard_map/dispatch/pallas_call | solution.py:208
  6.3 12.2 %all-to-all-start = ((bf16[64,24,512]{2,1,0:T(8,128)(2,1)}), bf16[64,24,512]{2,1,0:T(8,128)(2,1)S(1)}, u32[]{:S(2)}, u32[]{:S(2)}) async-start(bf16[64,24,512]{2,1,0:T(8,128)(2,1)} %bitcast.13), calls=%async_computation | async-start | bytes 3145728 | tf_op jit(solution)/shard_map/all_to_all | solution.py:218
  19.4 2.4 %collective-permute-start.3 = (bf16[2,1024,128]{2,1,0:T(8,128)(2,1)S(1)}, bf16[2,1024,128]{2,1,0:T(8,128)(2,1)S(1)}, u32[]{:S(2)}, u32[]{:S(2)}) collective-permute-start(bf16[2,1024,128]{2,1,0:T(8,128)(2,1)S(1)} %copy-done.3), channel_id=1, source_target_pairs={{0,1},{1,2},{2,3},{3,0},{4,5},{5,6},{6,7},{7,4},{8,9},{9,10},{10,1... | collective-permute-start | bytes 1572872 | tf_op jit(solution)/shard_map/ppermute | solution.py:200
  21.9 3.2 %collective-permute-start.6 = (bf16[2,128,1024]{2,1,0:T(8,128)(2,1)S(1)}, bf16[2,128,1024]{2,1,0:T(8,128)(2,1)S(1)}, u32[]{:S(2)}, u32[]{:S(2)}) collective-permute-start(bf16[2,128,1024]{2,1,0:T(8,128)(2,1)S(1)} %copy-done.4), channel_id=1, source_target_pairs={{0,1},{1,2},{2,3},{3,0},{4,5},{5,6},{6,7},{7,4},{8,9},{9,10},{10,1... | collective-permute-start | bytes 1572872 | tf_op jit(solution)/shard_map/ppermute | solution.py:200
  25.1 9.5 %collective-permute-done.1.refs_3_ = bf16[2,1024,128]{2,1,0:T(8,128)(2,1)S(1)} collective-permute-done((bf16[2,1024,128]{2,1,0:T(8,128)(2,1)S(1)}, bf16[2,1024,128]{2,1,0:T(8,128)(2,1)S(1)}, u32[]{:S(2)}, u32[]{:S(2)}) %collective-permute-start.1) | collective-permute-done | bytes 524320 | tf_op jit(solution)/shard_map/ppermute | solution.py:201
  34.8 11.1 %collective-permute-done.7.refs_11_ = bf16[2,128,1024]{2,1,0:T(8,128)(2,1)S(1)} collective-permute-done((bf16[2,128,1024]{2,1,0:T(8,128)(2,1)S(1)}, bf16[2,128,1024]{2,1,0:T(8,128)(2,1)S(1)}, u32[]{:S(2)}, u32[]{:S(2)}) %collective-permute-start.7) | collective-permute-done | bytes 524320 | tf_op jit(solution)/shard_map/ppermute | solution.py:201
  45.9 2.1 %collective-permute-start.8 = (bf16[1,128,1024]{2,1,0:T(8,128)(2,1)S(1)}, bf16[1,128,1024]{2,1,0:T(8,128)(2,1)S(1)}, u32[]{:S(2)}, u32[]{:S(2)}) collective-permute-start(bf16[1,128,1024]{2,1,0:T(8,128)(2,1)S(1)} %slice.20), channel_id=1, source_target_pairs={{0,3},{1,0},{2,1},{3,2},{4,7},{5,4},{6,5},{7,6},{8,11},{9,8},{10,9... | collective-permute-start | bytes 786440 | tf_op jit(solution)/shard_map/ppermute | solution.py:204
  48.0 8.7 %collective-permute-done.refs_2_ = bf16[2,1024,128]{2,1,0:T(8,128)(2,1)S(1)} collective-permute-done((bf16[2,1024,128]{2,1,0:T(8,128)(2,1)S(1)}, bf16[2,1024,128]{2,1,0:T(8,128)(2,1)S(1)}, u32[]{:S(2)}, u32[]{:S(2)}) %collective-permute-start) | collective-permute-done | bytes 524320 | tf_op jit(solution)/shard_map/ppermute | solution.py:200
  56.7 3.6 %collective-permute-start.9 = (bf16[1,128,1024]{2,1,0:T(8,128)(2,1)S(1)}, bf16[1,128,1024]{2,1,0:T(8,128)(2,1)S(1)}, u32[]{:S(2)}, u32[]{:S(2)}) collective-permute-start(bf16[1,128,1024]{2,1,0:T(8,128)(2,1)S(1)} %slice.21), channel_id=1, source_target_pairs={{0,1},{1,2},{2,3},{3,0},{4,5},{5,6},{6,7},{7,4},{8,9},{9,10},{10,1... | collective-permute-start | bytes 786440 | tf_op jit(solution)/shard_map/ppermute | solution.py:205
  60.3 12.8 %collective-permute-done.8.refs_12_ = bf16[1,128,1024]{2,1,0:T(8,128)(2,1)S(1)} collective-permute-done((bf16[1,128,1024]{2,1,0:T(8,128)(2,1)S(1)}, bf16[1,128,1024]{2,1,0:T(8,128)(2,1)S(1)}, u32[]{:S(2)}, u32[]{:S(2)}) %collective-permute-start.8) | collective-permute-done | bytes 262176 | tf_op jit(solution)/shard_map/ppermute | solution.py:204
  75.2 8.4 %input_grad.1 = f32[2,192,1152]{2,1,0:T(8,128)} custom-call(bf16[1536,512]{1,0:T(8,128)(2,1)} %bitcast.9, bf16[2,1024,128]{2,1,0:T(8,128)(2,1)} %refs_5_.3, bf16[2,1024,128]{2,1,0:T(8,128)(2,1)} %copy-done.9, bf16[2,1024,128]{2,1,0:T(8,128)(2,1)} %copy-done.7, bf16[2,1024,128]{2,1,0:T(8,128)(2,1)} %copy-done.11, bf16[2,1024,128]{2,1,0:T(8,128)(2,1)} %refs_6_.1, ...), custom_call_target="tpu_custom_call" | custom-call | tf_op jit(solution)/shard_map/input_grad/pallas_call | solution.py:236
  83.7 1.6 convert_element_type.7
  85.3 2.1 %copy.30 = f16[2,192,1152]{2,0,1:T(2,128)(2,1)} copy(f16[2,192,1152]{2,1,0:T(8,128)(2,1)S(1)} %convert_element_type.7) | data formatting | bytes 1769472 | tf_op jit(solution)/shard_map/convert_element_type | solution.py:245
  87.3 10.3 %all-to-all-start.1 = ((f16[64,2,3,1152]{3,1,2,0:T(2,128)(2,1)}), f16[64,2,3,1152]{3,1,2,0:T(2,128)(2,1)S(1)}, u32[]{:S(2)}, u32[]{:S(2)}) async-start(f16[64,2,3,1152]{3,1,2,0:T(2,128)(2,1)} %bitcast.6), calls=%async_computation.1 | async-start | bytes 1769472 | tf_op jit(solution)/shard_map/all_to_all | solution.py:246
  97.7 3.2 %collective-permute-start.10 = (bf16[1536,512]{1,0:T(8,128)(2,1)S(1)}, bf16[1536,512]{1,0:T(8,128)(2,1)}, u32[]{:S(2)}, u32[]{:S(2)}) collective-permute-start(bf16[1536,512]{1,0:T(8,128)(2,1)S(1)} %bitcast.12), channel_id=1, source_target_pairs={{0,1},{1,2},{2,3},{3,0},{4,5},{5,6},{6,7},{7,4},{8,9},{9,10},{10,1... | collective-permute-start | bytes 4718600 | tf_op jit(solution)/shard_map/ppermute | solution.py:222
  101.1 34.4 %collective-permute-done.11.refs_2_ = bf16[1536,512]{1,0:T(8,128)(2,1)} collective-permute-done((bf16[1536,512]{1,0:T(8,128)(2,1)S(1)}, bf16[1536,512]{1,0:T(8,128)(2,1)}, u32[]{:S(2)}, u32[]{:S(2)}) %collective-permute-start.11) | collective-permute-done | bytes 1572896 | tf_op jit(solution)/shard_map/ppermute | solution.py:223
  135.4 1.2 slice.22
  136.7 2.1 %slice.23 = bf16[768,512]{1,0:T(8,128)(2,1)} slice(bf16[1536,512]{1,0:T(8,128)(2,1)} %collective-permute-done.10.refs_1_), slice={[768:1536], [0:512]} | slice | bytes 1572864 | tf_op jit(solution)/shard_map/slice | solution.py:226
  138.8 3.2 %collective-permute-start.13 = (bf16[768,512]{1,0:T(8,128)(2,1)}, bf16[768,512]{1,0:T(8,128)(2,1)}, u32[]{:S(2)}, u32[]{:S(2)}) collective-permute-start(bf16[768,512]{1,0:T(8,128)(2,1)} %slice.23), channel_id=1, source_target_pairs={{0,1},{1,2},{2,3},{3,0},{4,5},{5,6},{6,7},{7,4},{8,9},{9,10},{10,1... | collective-permute-start | bytes 2359304 | tf_op jit(solution)/shard_map/ppermute | solution.py:226
  142.2 1.2 copy.32
  143.4 1.8 reshape.34.back
  145.2 3.7 %combine.1 = (f32[256,1024]{1,0:T(8,128)}, f32[256,128]{1,0:T(8,128)}) custom-call(f32[384,1152]{1,0:T(8,128)} %reshape.34.back, bf16[2,384,256]{2,1,0:T(8,128)(2,1)} %get-tuple-element.13.pick), custom_call_target="tpu_custom_call" | custom-call | tf_op jit(solution)/shard_map/combine/pallas_call | solution.py:248
  148.9 40.3 %all-reduce.2 = (bf16[256,1024]{1,0:T(8,128)(2,1)}, f32[256,2]{1,0:T(8,128)S(1)}) all-reduce(f32[256,1024]{1,0:T(8,128)} %get-tuple-element.14, f32[256,2]{1,0:T(8,128)} %bitcast.14), channel_id=1, replica_groups=mesh['ep'=64,'tp'=4] {'tp'}, use_global_device_ids=true, to_apply=%region_0.0 | all-reduce | flops 262656 | bytes 1576960 | tf_op jit(solution)/shard_map/psum | solution.py:258
  189.9 11.7 %weight_grad.1 = (f32[2,1024,128]{2,1,0:T(8,128)}, f32[2,1024,128]{2,1,0:T(8,128)}, f32[2,128,1024]{2,1,0:T(8,128)}) custom-call(bf16[1536,512]{1,0:T(8,128)(2,1)} %bitcast.10, bf16[1536,512]{1,0:T(8,128)(2,1)} %collective-permute-done.10.refs_1_, bf16[1536,512]{1,0:T(8,128)(2,1)} %collective-permute-done.11.refs_2_, ...), custom_call_target="tpu_custom_call" | custom-call | tf_op jit(solution)/shard_map/weight_grad/pallas_call | solution.py:264
  (55 shorter events, 4.4 us)
Async XLA Ops:
  6.3 13.2 %copy-start.3 = (bf16[2,1024,128]{2,1,0:T(8,128)(2,1)S(1)}, bf16[2,1024,128]{2,1,0:T(8,128)(2,1)}, u32[]{:S(2)}) copy-start(bf16[2,1024,128]{2,1,0:T(8,128)(2,1)} %refs_6_.1) | copy-start | bytes 1572868
  6.3 15.6 %copy-start.4 = (bf16[2,128,1024]{2,1,0:T(8,128)(2,1)S(1)}, bf16[2,128,1024]{2,1,0:T(8,128)(2,1)}, u32[]{:S(2)}) copy-start(bf16[2,128,1024]{2,1,0:T(8,128)(2,1)} %refs_7_.1) | copy-start | bytes 1572868
  6.3 67.8 %all-to-all-start = ((bf16[64,24,512]{2,1,0:T(8,128)(2,1)}), bf16[64,24,512]{2,1,0:T(8,128)(2,1)S(1)}, u32[]{:S(2)}, u32[]{:S(2)}) async-start(bf16[64,24,512]{2,1,0:T(8,128)(2,1)} %bitcast.13), calls=%async_computation | async-start | bytes 3145728 | tf_op jit(solution)/shard_map/all_to_all | solution.py:218
  18.5 16.1 %collective-permute-start.1 = (bf16[2,1024,128]{2,1,0:T(8,128)(2,1)S(1)}, bf16[2,1024,128]{2,1,0:T(8,128)(2,1)S(1)}, u32[]{:S(2)}, u32[]{:S(2)}) collective-permute-start(bf16[2,1024,128]{2,1,0:T(8,128)(2,1)S(1)} %copy-done.2), channel_id=1, source_target_pairs={{0,3},{1,0},{2,1},{3,2},{4,7},{5,4},{6,5},{7,6},{8,11},{9,8},{10,9... | collective-permute-start | bytes 1572872 | tf_op jit(solution)/shard_map/ppermute | solution.py:201
  19.4 15.2 %collective-permute-start.3 = (bf16[2,1024,128]{2,1,0:T(8,128)(2,1)S(1)}, bf16[2,1024,128]{2,1,0:T(8,128)(2,1)S(1)}, u32[]{:S(2)}, u32[]{:S(2)}) collective-permute-start(bf16[2,1024,128]{2,1,0:T(8,128)(2,1)S(1)} %copy-done.3), channel_id=1, source_target_pairs={{0,1},{1,2},{2,3},{3,0},{4,5},{5,6},{6,7},{7,4},{8,9},{9,10},{10,1... | collective-permute-start | bytes 1572872 | tf_op jit(solution)/shard_map/ppermute | solution.py:200
  21.9 24.0 %collective-permute-start.7 = (bf16[2,128,1024]{2,1,0:T(8,128)(2,1)S(1)}, bf16[2,128,1024]{2,1,0:T(8,128)(2,1)S(1)}, u32[]{:S(2)}, u32[]{:S(2)}) collective-permute-start(bf16[2,128,1024]{2,1,0:T(8,128)(2,1)S(1)} %copy-done.4), channel_id=1, source_target_pairs={{0,3},{1,0},{2,1},{3,2},{4,7},{5,4},{6,5},{7,6},{8,11},{9,8},{10,9... | collective-permute-start | bytes 1572872 | tf_op jit(solution)/shard_map/ppermute | solution.py:201
  21.9 24.0 %collective-permute-start.6 = (bf16[2,128,1024]{2,1,0:T(8,128)(2,1)S(1)}, bf16[2,128,1024]{2,1,0:T(8,128)(2,1)S(1)}, u32[]{:S(2)}, u32[]{:S(2)}) collective-permute-start(bf16[2,128,1024]{2,1,0:T(8,128)(2,1)S(1)} %copy-done.4), channel_id=1, source_target_pairs={{0,1},{1,2},{2,3},{3,0},{4,5},{5,6},{6,7},{7,4},{8,9},{9,10},{10,1... | collective-permute-start | bytes 1572872 | tf_op jit(solution)/shard_map/ppermute | solution.py:200
  25.1 31.6 %collective-permute-start = (bf16[2,1024,128]{2,1,0:T(8,128)(2,1)S(1)}, bf16[2,1024,128]{2,1,0:T(8,128)(2,1)S(1)}, u32[]{:S(2)}, u32[]{:S(2)}) collective-permute-start(bf16[2,1024,128]{2,1,0:T(8,128)(2,1)S(1)} %copy-done.2), channel_id=1, source_target_pairs={{0,1},{1,2},{2,3},{3,0},{4,5},{5,6},{6,7},{7,4},{8,9},{9,10},{10,1... | collective-permute-start | bytes 1572872 | tf_op jit(solution)/shard_map/ppermute | solution.py:200
  34.6 38.5 %copy-start.7 = (bf16[2,1024,128]{2,1,0:T(8,128)(2,1)}, bf16[2,1024,128]{2,1,0:T(8,128)(2,1)S(1)}, u32[]{:S(2)}) copy-start(bf16[2,1024,128]{2,1,0:T(8,128)(2,1)S(1)} %collective-permute-done.1.refs_3_) | copy-start | bytes 1572868
  34.6 25.7 %collective-permute-start.4 = (bf16[2,1024,128]{2,1,0:T(8,128)(2,1)S(1)}, bf16[2,1024,128]{2,1,0:T(8,128)(2,1)S(1)}, u32[]{:S(2)}, u32[]{:S(2)}) collective-permute-start(bf16[2,1024,128]{2,1,0:T(8,128)(2,1)S(1)} %copy-done.3), channel_id=1, source_target_pairs={{0,3},{1,0},{2,1},{3,2},{4,7},{5,4},{6,5},{7,6},{8,11},{9,8},{10,9... | collective-permute-start | bytes 1572872 | tf_op jit(solution)/shard_map/ppermute | solution.py:201
  34.6 38.5 %copy-start.8 = (bf16[2,1024,128]{2,1,0:T(8,128)(2,1)}, bf16[2,1024,128]{2,1,0:T(8,128)(2,1)S(1)}, u32[]{:S(2)}) copy-start(bf16[2,1024,128]{2,1,0:T(8,128)(2,1)S(1)} %collective-permute-done.3.refs_6_) | copy-start | bytes 1572868
  34.6 38.5 %collective-permute-start.2 = (bf16[2,1024,128]{2,1,0:T(8,128)(2,1)S(1)}, bf16[2,1024,128]{2,1,0:T(8,128)(2,1)S(1)}, u32[]{:S(2)}, u32[]{:S(2)}) collective-permute-start(bf16[2,1024,128]{2,1,0:T(8,128)(2,1)S(1)} %collective-permute-done.1.refs_3_), channel_id=1, source_target_pairs={{0,3},{1,0},{2,1},{3,2},{4,7},{5,4},{6,5},{7,6},{8,11},{9,8},{10,9... | collective-permute-start | bytes 1572872 | tf_op jit(solution)/shard_map/ppermute | solution.py:202
  45.9 27.3 %copy-start.5 = (bf16[2,128,1024]{2,1,0:T(8,128)(2,1)}, bf16[2,128,1024]{2,1,0:T(8,128)(2,1)S(1)}, u32[]{:S(2)}) copy-start(bf16[2,128,1024]{2,1,0:T(8,128)(2,1)S(1)} %collective-permute-done.7.refs_11_) | copy-start | bytes 1572868
  45.9 28.2 %collective-permute-start.5 = (bf16[2,1024,128]{2,1,0:T(8,128)(2,1)S(1)}, bf16[2,1024,128]{2,1,0:T(8,128)(2,1)}, u32[]{:S(2)}, u32[]{:S(2)}) collective-permute-start(bf16[2,1024,128]{2,1,0:T(8,128)(2,1)S(1)} %collective-permute-done.3.refs_6_), channel_id=1, source_target_pairs={{0,1},{1,2},{2,3},{3,0},{4,5},{5,6},{6,7},{7,4},{8,9},{9,10},{10,1... | collective-permute-start | bytes 1572872 | tf_op jit(solution)/shard_map/ppermute | solution.py:203
  45.9 27.2 %copy-start.6 = (bf16[2,128,1024]{2,1,0:T(8,128)(2,1)}, bf16[2,128,1024]{2,1,0:T(8,128)(2,1)S(1)}, u32[]{:S(2)}) copy-start(bf16[2,128,1024]{2,1,0:T(8,128)(2,1)S(1)} %collective-permute-done.6.refs_10_) | copy-start | bytes 1572868
  45.9 27.2 %collective-permute-start.8 = (bf16[1,128,1024]{2,1,0:T(8,128)(2,1)S(1)}, bf16[1,128,1024]{2,1,0:T(8,128)(2,1)S(1)}, u32[]{:S(2)}, u32[]{:S(2)}) collective-permute-start(bf16[1,128,1024]{2,1,0:T(8,128)(2,1)S(1)} %slice.20), channel_id=1, source_target_pairs={{0,3},{1,0},{2,1},{3,2},{4,7},{5,4},{6,5},{7,6},{8,11},{9,8},{10,9... | collective-permute-start | bytes 786440 | tf_op jit(solution)/shard_map/ppermute | solution.py:204
  56.7 16.4 %copy-start.9 = (bf16[2,1024,128]{2,1,0:T(8,128)(2,1)}, bf16[2,1024,128]{2,1,0:T(8,128)(2,1)S(1)}, u32[]{:S(2)}) copy-start(bf16[2,1024,128]{2,1,0:T(8,128)(2,1)S(1)} %collective-permute-done.refs_2_) | copy-start | bytes 1572868
  56.7 16.4 %collective-permute-start.9 = (bf16[1,128,1024]{2,1,0:T(8,128)(2,1)S(1)}, bf16[1,128,1024]{2,1,0:T(8,128)(2,1)S(1)}, u32[]{:S(2)}, u32[]{:S(2)}) collective-permute-start(bf16[1,128,1024]{2,1,0:T(8,128)(2,1)S(1)} %slice.21), channel_id=1, source_target_pairs={{0,1},{1,2},{2,3},{3,0},{4,5},{5,6},{6,7},{7,4},{8,9},{9,10},{10,1... | collective-permute-start | bytes 786440 | tf_op jit(solution)/shard_map/ppermute | solution.py:205
  85.2 15.7 %copy-start.14 = (f32[256,2]{0,1:T(2,128)S(1)}, f32[256,2]{0,1:T(2,128)}, u32[]{:S(2)}) copy-start(f32[256,2]{0,1:T(2,128)} %param.10) | copy-start | bytes 6148
  87.3 54.7 %all-to-all-start.1 = ((f16[64,2,3,1152]{3,1,2,0:T(2,128)(2,1)}), f16[64,2,3,1152]{3,1,2,0:T(2,128)(2,1)S(1)}, u32[]{:S(2)}, u32[]{:S(2)}) async-start(f16[64,2,3,1152]{3,1,2,0:T(2,128)(2,1)} %bitcast.6), calls=%async_computation.1 | async-start | bytes 1769472 | tf_op jit(solution)/shard_map/all_to_all | solution.py:246
  97.6 37.8 %collective-permute-start.11 = (bf16[1536,512]{1,0:T(8,128)(2,1)S(1)}, bf16[1536,512]{1,0:T(8,128)(2,1)}, u32[]{:S(2)}, u32[]{:S(2)}) collective-permute-start(bf16[1536,512]{1,0:T(8,128)(2,1)S(1)} %bitcast.11), channel_id=1, source_target_pairs={{0,3},{1,0},{2,1},{3,2},{4,7},{5,4},{6,5},{7,6},{8,11},{9,8},{10,9... | collective-permute-start | bytes 4718600 | tf_op jit(solution)/shard_map/ppermute | solution.py:223
  97.7 39.0 %collective-permute-start.10 = (bf16[1536,512]{1,0:T(8,128)(2,1)S(1)}, bf16[1536,512]{1,0:T(8,128)(2,1)}, u32[]{:S(2)}, u32[]{:S(2)}) collective-permute-start(bf16[1536,512]{1,0:T(8,128)(2,1)S(1)} %bitcast.12), channel_id=1, source_target_pairs={{0,1},{1,2},{2,3},{3,0},{4,5},{5,6},{6,7},{7,4},{8,9},{9,10},{10,1... | collective-permute-start | bytes 4718600 | tf_op jit(solution)/shard_map/ppermute | solution.py:222
  136.6 53.3 %collective-permute-start.12 = (bf16[768,512]{1,0:T(8,128)(2,1)S(1)}, bf16[768,512]{1,0:T(8,128)(2,1)}, u32[]{:S(2)}, u32[]{:S(2)}) collective-permute-start(bf16[768,512]{1,0:T(8,128)(2,1)S(1)} %slice.22), channel_id=1, source_target_pairs={{0,3},{1,0},{2,1},{3,2},{4,7},{5,4},{6,5},{7,6},{8,11},{9,8},{10,9... | collective-permute-start | bytes 2359304 | tf_op jit(solution)/shard_map/ppermute | solution.py:225
  138.8 51.1 %collective-permute-start.13 = (bf16[768,512]{1,0:T(8,128)(2,1)}, bf16[768,512]{1,0:T(8,128)(2,1)}, u32[]{:S(2)}, u32[]{:S(2)}) collective-permute-start(bf16[768,512]{1,0:T(8,128)(2,1)} %slice.23), channel_id=1, source_target_pairs={{0,1},{1,2},{2,3},{3,0},{4,5},{5,6},{6,7},{7,4},{8,9},{9,10},{10,1... | collective-permute-start | bytes 2359304 | tf_op jit(solution)/shard_map/ppermute | solution.py:226
  (7 other events, 41.6 us)

commit v2 on v1

v2 whole, which is shorter than its diff:
```python
import jax
import jax.numpy as jnp
from jax import lax
from jax.experimental import pallas as pl
from jax.experimental.pallas import tpu as pltpu
from jax.sharding import PartitionSpec as P


F32 = jnp.float32
F16 = jnp.float16
BF16 = jnp.bfloat16
I32 = jnp.int32
LANES = 128
SUBLANES = 8
BLOCK = 16
HALVES = 2
SPREAD = 16384.0
VMEM = pltpu.VMEM
SMEM = pltpu.SMEM
NN = ((1,), (0,))
NT = ((1,), (1,))
TN = ((0,), (0,))


def mm(a, b, dims=NN):
    return lax.dot_general(a, b, (dims, ((), ())), preferred_element_type=F32)


def iota(shape, dim):
    return lax.broadcasted_iota(I32, shape, dim)


def split3(value):
    high = value.astype(BF16)
    rest = value - high.astype(F32)
    middle = rest.astype(BF16)
    low = (rest - middle.astype(F32)).astype(BF16)
    return high, middle, low


def exponent(value):
    return jnp.floor(jnp.log(jnp.maximum(value, 1e-30)) * 1.4426950408889634)


def dispatch_kernel(
    experts, local_experts, quarter, member, routing, weights, tokens, cotangent, rows_out, pick
):
    token_count, width = tokens.shape
    half = width // HALVES
    row_count = rows_out.shape[0]
    slots = pick.shape[1]
    group = local_experts * quarter
    chunk = HALVES * 2 * group
    devices = experts // local_experts
    expert = iota((experts, token_count), 0)
    chosen = [routing[k : k + 1, :] for k in range(2)]
    onehot = [jnp.where(expert == c, 1.0, 0.0) for c in chosen]
    earlier = iota((token_count, token_count), 0)
    later = iota((token_count, token_count), 1)
    upper = jnp.where(earlier < later, 1.0, 0.0).astype(BF16)
    before = mm((onehot[0] + onehot[1]).astype(BF16), upper)
    row = iota((row_count, token_count), 0)
    slot = iota((slots, token_count), 0)
    token_rows = []
    for k in range(2):
        position = jnp.sum(onehot[k] * before, axis=0, keepdims=True).astype(I32)
        local = position - member[0] * quarter
        present = (local >= 0) & (local < quarter)
        device = chosen[k] // local_experts
        within = (chosen[k] - device * local_experts) * quarter + local
        pick[k] = jnp.where(slot == jnp.where(present, within * devices + device, -1), 1.0, 0.0).astype(BF16)
        token_rows.append(jnp.where(present, device * chunk + within, -chunk))
    total = None
    for h in range(HALVES):
        columns = slice(h * half, (h + 1) * half)
        base = h * 2 * group
        hits = [jnp.where(row == r + base, 1.0, 0.0) for r in token_rows]
        part = mm((hits[0] + hits[1]).astype(BF16), tokens[:, columns])
        hits = [jnp.where(row == r + (base + group), 1.0, 0.0) for r in token_rows]
        slot_weight = jnp.sum(hits[0] * weights[0:1, :] + hits[1] * weights[1:2, :], axis=1, keepdims=True)
        part = part + slot_weight * mm((hits[0] + hits[1]).astype(BF16), cotangent[:, columns])
        total = part if total is None else total + part
    rows_out[...] = total.astype(BF16)


def land(source, expert, local_experts, quarter, rows, scaled, offset):
    half = source.shape[1]
    group = local_experts * quarter
    chunk = HALVES * 2 * group
    out_rows = BLOCK * quarter
    index = iota((HALVES * 2 * out_rows, 1), 0)
    kind = index // out_rows
    rest = index - kind * out_rows
    slot = rest // BLOCK
    wanted = (rest - slot * BLOCK) * chunk + kind * group + expert * quarter + slot
    column = iota((HALVES * 2 * out_rows, BLOCK * chunk), 1)
    permutation = jnp.where(column == wanted, 1.0, 0.0).astype(BF16)
    for block in range(source.shape[0] // (BLOCK * chunk)):
        moved = mm(permutation, source[block * BLOCK * chunk : (block + 1) * BLOCK * chunk, :])
        moved = moved.astype(BF16)
        at = slice(offset + block * out_rows, offset + (block + 1) * out_rows)
        for h in range(HALVES):
            columns = slice(h * half, (h + 1) * half)
            first = 2 * h * out_rows
            rows[at, columns] = moved[first : first + out_rows]
            scaled[at, columns] = moved[first + out_rows : first + 2 * out_rows]


def hidden_terms(gate_pre, up_pre, hidden_grad):
    gate_pre = gate_pre.astype(BF16).astype(F32)
    up_pre = up_pre.astype(BF16).astype(F32)
    sigmoid = jax.nn.sigmoid(gate_pre)
    activated = gate_pre * sigmoid
    hidden = activated * up_pre
    gate_grad = (hidden_grad * up_pre * sigmoid * (1.0 + gate_pre * (1.0 - sigmoid))).astype(BF16)
    up_grad = (hidden_grad * activated).astype(BF16)
    return hidden, gate_grad, up_grad


def input_kernel(local_experts, quarter, landed, *refs):
    gates, ups, downs = refs[0:4], refs[4:8], refs[8:11]
    down_even, down_odd, out, rows, scaled = refs[11:]
    own, _ = rows.shape
    slots = local_experts * quarter
    devices = own // quarter
    stride = (slots + 1) * SUBLANES
    for i in range(slots, SUBLANES):
        at = slots * SUBLANES + i
        out[pl.ds(at, devices, stride=stride), :] = jnp.zeros((devices, LANES), F32)
    for expert in range(local_experts):
        land(landed, expert, local_experts, quarter, rows, scaled, 0)
        gate = jnp.concatenate([g[expert] for g in gates], axis=1)
        up = jnp.concatenate([u[expert] for u in ups], axis=1)
        last = (down_even, down_odd)[expert][0]
        down = jnp.concatenate([d[expert] for d in downs] + [last], axis=0)
        hidden_grad = mm(scaled[...], down, NT)
        hidden, gate_grad, up_grad = hidden_terms(mm(rows[...], gate), mm(rows[...], up), hidden_grad)
        product = jnp.sum(hidden_grad * hidden, axis=1, keepdims=True)
        grad = mm(gate_grad, gate, NT) + mm(up_grad, up, NT)
        power = exponent(jnp.max(jnp.abs(grad), axis=1, keepdims=True))
        grad = grad * (SPREAD * jnp.exp2(-power))
        product_power = exponent(jnp.abs(product))
        product = product * jnp.exp2(-product_power)
        high = product.astype(BF16).astype(F32)
        low = (product - high) * 256.0
        lane = iota((own, LANES), 1)
        tail = jnp.where(
            lane == 0,
            power,
            jnp.where(lane == 1, product_power, jnp.where(lane == 2, high, low)),
        )
        for block in range(devices // BLOCK):
            for q in range(quarter):
                at = (block * quarter + q) * BLOCK
                to = block * BLOCK * stride
                slot = expert * quarter + q
                for i in range(SUBLANES):
                    piece = grad[at : at + BLOCK, i * LANES : (i + 1) * LANES]
                    out[pl.ds(to + slot * SUBLANES + i, BLOCK, stride=stride), :] = piece
                to += slots * SUBLANES + slot
                out[pl.ds(to, BLOCK, stride=stride), :] = tail[at : at + BLOCK]


def weight_kernel(local_experts, quarter, *refs):
    sources, (gate, up, down), (gate_out, up_out, down_out) = refs[0:5], refs[5:8], refs[8:11]
    rows, scaled = refs[11:]
    chunk = HALVES * 2 * local_experts * quarter
    hidden_width = gate.shape[2]
    for expert in range(local_experts):
        offset = 0
        for source in sources:
            land(source, expert, local_experts, quarter, rows, scaled, offset)
            offset += source.shape[0] // chunk * quarter
        both = mm(rows[...], jnp.concatenate([gate[expert], up[expert]], axis=1))
        hidden_grad = mm(scaled[...], down[expert], NT)
        hidden, gate_grad, up_grad = hidden_terms(
            both[:, :hidden_width], both[:, hidden_width:], hidden_grad
        )
        grads = mm(rows[...], jnp.concatenate([gate_grad, up_grad], axis=1), TN)
        gate_out[expert] = grads[:, :hidden_width]
        up_out[expert] = grads[:, hidden_width:]
        down_out[expert] = mm(hidden.astype(BF16), scaled[...], TN)


def member_rows(member, distance, members, count):
    return pl.ds(pl.multiple_of(lax.rem(member + distance, members) * count, count), count)


def combine_kernel(members, devices, member, back, pick, *refs):
    outs, total = refs[:-1], refs[-1]
    token_count, width = total.shape
    slots = pick.shape[1] // devices
    stride = (slots + 1) * SUBLANES
    tails = [
        back[pl.ds(slots * SUBLANES + slot, devices, stride=stride), :] for slot in range(slots)
    ]
    tail = jnp.concatenate(tails, axis=0)
    scale = jnp.exp2(tail[:, 0:1]) * (1.0 / SPREAD)
    columns = []
    for i in range(SUBLANES):
        pieces = [
            back[pl.ds(slot * SUBLANES + i, devices, stride=stride), :] for slot in range(slots)
        ]
        columns.append(jnp.concatenate(pieces, axis=0))
    grad = jnp.concatenate(columns, axis=1) * scale
    both = pick[0] + pick[1]
    total[...] = sum(mm(both, part, TN) for part in split3(grad))
    product = (tail[:, 2:3] + tail[:, 3:4] * (1.0 / 256.0)) * jnp.exp2(tail[:, 1:2])
    sums = [jnp.sum(pick[k].astype(F32) * product, axis=0, keepdims=True) for k in range(2)]
    spare = jnp.zeros((1, width - 2 * token_count), F32)
    line = jnp.broadcast_to(jnp.concatenate(sums + [spare], axis=1), (SUBLANES, width))
    count = token_count // members
    for out, distance in zip(outs, (0, 1, 3, 2)):
        out[0:count, :] = total[member_rows(member[0], distance, members, count), :]
        out[count : count + SUBLANES, :] = line


def sum_kernel(own, from_left, from_right, from_opposite, weights, grad_out, gates_out):
    count = grad_out.shape[0]
    token_count = weights.shape[1]
    total = (own[...] + from_opposite[...]) + (from_left[...] + from_right[...])
    grad_out[...] = total[0:count].astype(BF16)
    for k in range(2):
        product = total[count : count + 1, k * token_count : (k + 1) * token_count]
        gates_out[k : k + 1, :] = product / weights[k : k + 1, :]


def place_kernel(members, member, own, from_left, from_right, from_opposite, out):
    count = own.shape[0]
    for piece, distance in ((own, 0), (from_left, 3), (from_right, 1), (from_opposite, 2)):
        out[member_rows(member[0], distance, members, count), :] = piece[...]


def step(tokens, cotangent, routing, gate_weights, gate_proj, up_proj, down_proj):
    token_count, model_width = tokens.shape
    top_count = routing.shape[1]
    local_experts, _, hidden_width = gate_proj.shape
    groups = lax.axis_size("ep")
    members = lax.axis_size("tp")
    experts = local_experts * groups
    capacity = members * (
        (3 * token_count * top_count + experts * members - 1) // (experts * members)
    )
    quarter = capacity // members
    slots = experts * quarter
    own = groups * quarter
    chunk = HALVES * 2 * local_experts * quarter
    half = model_width // HALVES
    member = lax.axis_index("tp").astype(I32).reshape(1)
    right = [(i, (i + 1) % members) for i in range(members)]
    left = [(i, (i - 1) % members) for i in range(members)]
    across = [(i, (i + 2) % members) for i in range(members)]
    whole = pl.BlockSpec(memory_space=VMEM)
    scalar = pl.BlockSpec(memory_space=SMEM)

    def call(kernel, out_shape, args, scalars=0, scratch=()):
        return pl.pallas_call(
            kernel,
            out_shape=out_shape,
            in_specs=[scalar] * scalars + [whole] * (len(args) - scalars),
            out_specs=jax.tree.map(lambda _: whole, out_shape),
            scratch_shapes=list(scratch),
        )(*args)

    def shape(dims, dtype):
        return jax.ShapeDtypeStruct(dims, dtype)

    gates, ups, downs = [gate_proj], [up_proj], [down_proj]
    for kept, mine in ((gates, gate_proj), (ups, up_proj), (downs, down_proj)):
        kept.append(lax.ppermute(mine, "tp", right))
        kept.append(lax.ppermute(mine, "tp", left))
    gates.append(lax.ppermute(gates[2], "tp", left))
    ups.append(lax.ppermute(ups[1], "tp", right))
    down_even = lax.ppermute(downs[2][0:1], "tp", left)
    down_odd = lax.ppermute(downs[1][1:2], "tp", right)

    send, pick = call(
        lambda *refs: dispatch_kernel(experts, local_experts, quarter, *refs),
        (shape((groups * chunk, half), BF16), shape((2, slots, token_count), BF16)),
        (member, routing.T, gate_weights.T, tokens, cotangent),
        scalars=1,
    )
    landed = lax.all_to_all(
        send.reshape(groups, chunk, half), "ep", split_axis=0, concat_axis=0, tiled=True
    ).reshape(groups * chunk, half)

    from_left = lax.ppermute(landed, "tp", right)
    from_right = lax.ppermute(landed, "tp", left)
    middle = groups * chunk // 2
    opposite_low = lax.ppermute(from_right[:middle], "tp", left)
    opposite_high = lax.ppermute(from_left[middle:], "tp", right)

    back_rows = (local_experts * quarter + 1) * SUBLANES
    back = call(
        lambda *refs: input_kernel(local_experts, quarter, *refs),
        shape((groups * back_rows, LANES), F32),
        (landed, *gates, *ups, *downs, down_even, down_odd),
        scratch=[VMEM((own, model_width), BF16)] * 2,
    )
    back = back.astype(F16).reshape(groups, back_rows, LANES)
    back = lax.all_to_all(back, "ep", split_axis=0, concat_axis=0, tiled=True)
    back = back.astype(F32).reshape(groups * back_rows, LANES)
    count = token_count // members
    part = shape((count + SUBLANES, model_width), F32)
    mine, to_right, to_left, to_across = call(
        lambda *refs: combine_kernel(members, groups, *refs),
        (part,) * 4,
        (member, back, pick),
        scalars=1,
        scratch=[VMEM((token_count, model_width), F32)],
    )
    pieces = (
        lax.ppermute(to_right, "tp", right),
        lax.ppermute(to_left, "tp", left),
        lax.ppermute(to_across, "tp", across),
    )
    summed, gates_grad = call(
        sum_kernel,
        (shape((count, model_width), BF16), shape((top_count, token_count), F32)),
        (mine, *pieces, gate_weights.T),
    )
    pieces = (
        lax.ppermute(summed, "tp", right),
        lax.ppermute(summed, "tp", left),
        lax.ppermute(summed, "tp", across),
    )
    tokens_grad = call(
        lambda *refs: place_kernel(members, *refs),
        shape((token_count, model_width), BF16),
        (member, summed, *pieces),
        scalars=1,
    )

    gate_grad, up_grad, down_grad = call(
        lambda *refs: weight_kernel(local_experts, quarter, *refs),
        (
            shape((local_experts, model_width, hidden_width), F32),
            shape((local_experts, model_width, hidden_width), F32),
            shape((local_experts, hidden_width, model_width), F32),
        ),
        (landed, from_left, from_right, opposite_low, opposite_high, gate_proj, up_proj, down_proj),
        scratch=[VMEM((members * own, model_width), BF16)] * 2,
    )
    return (tokens_grad, gates_grad.T, gate_grad, up_grad, down_grad)


def solution(mesh):
    in_specs = (
        P("ep", None),
        P("ep", None),
        P("ep", None),
        P("ep", None),
        P("ep", None, "tp"),
        P("ep", None, "tp"),
        P("ep", "tp", None),
    )
    out_specs = (
        P("ep", None),
        P("ep", None),
        P("ep", None, "tp"),
        P("ep", None, "tp"),
        P("ep", "tp", None),
    )
    return jax.shard_map(step, mesh=mesh, in_specs=in_specs, out_specs=out_specs, check_vma=False)
```

time: 202 us -> 198 us (0.980)
  blocking collectives: 40.3 us -> 0 us
  waiting for transfers between devices: 76.4 us -> 103 us
  starting transfers between devices: 41.6 us -> 47.9 us
  local copies, waits for them, and re-layouts: 11.3 us -> 6.09 us
  Pallas kernels: 29.5 us -> 33.9 us
  other arithmetic: 1.74 us -> 3.99 us
    psum x1 -> x0, blocking collectives: 40.3 us -> none  [shards(): lax.psum((token_grad, product[:, :top_count]), 'tp')]
    ppermute x14 -> x20, waiting for transfers between devices: 76.4 us -> 103 us  [the longest x1 34.4 us: step(): from_right = lax.ppermute(landed, 'tp', left)]
    ppermute x14 -> x20, starting transfers between devices: 19 us -> 25.2 us  [the longest x3 5.67 us: step(): kept.append(lax.ppermute(mine, 'tp', right))]
    pallas_call x4 -> x6, Pallas kernels: 29.5 us -> 33.9 us  [call(): pl.pallas_call(kernel, out_shape=out_shape, in_specs=[scalar] * scalars +...]
    slice x4, local copies, waits for them, and re-layouts: 3.28 us -> 0.14 us  [the longest x1 0.05 us: step(): opposite_high = lax.ppermute(from_left[middle:], 'tp', right)]
    unnamed x32 -> x46, local copies, waits for them, and re-layouts: 2.88 us -> 5.95 us
    reshape x2 -> x0, local copies, waits for them, and re-layouts: 3.05 us -> none  [shards(): back = back.astype(F32).reshape(slots, tail_width)]
    convert_element_type x1 -> x0, local copies, waits for them, and re-layouts: 2.05 us -> none  [shards(): back.astype(F16).reshape(local_experts, groups, quarter, tail_width)]
  transfers between devices with their start and end apart: 16 -> 22, of which waited for: 5 -> 9; matrix products, arithmetic and copies ran while one was open for 4% -> 1% of each run, Pallas kernels for 2% -> 4%
where the time goes in v2:
time: 198 us; the launch traced here: 196 us
  waiting for transfers between devices  103 us (52%)
  starting transfers between devices  47.9 us (24%)
  Pallas kernels  33.9 us (17%)
  local copies, waits for them, and re-layouts  6.09 us (3%)
  other arithmetic  3.99 us (2%)
    ppermute x1, waiting for transfers between devices, step(): from_right = lax.ppermute(landed, 'tp', left)  34.4 us
    pallas_call x6, Pallas kernels, call(): pl.pallas_call(kernel, out_shape=out_shape, in_specs=[scalar] * scalars +...  33.9 us
    ppermute x1, waiting for transfers between devices, step(): lax.ppermute(to_right, 'tp', right)  21.3 us
    ppermute x3, waiting for transfers between devices, step(): kept.append(lax.ppermute(mine, 'tp', left))  20.6 us
    ppermute x1, waiting for transfers between devices, step(): down_even = lax.ppermute(downs[2][0:1], 'tp', left)  12.8 us
    all_to_all x1, starting transfers between devices, step(): lax.all_to_all(send.reshape(groups, chunk, half), 'ep', split_axis=0, con...  12.2 us
    all_to_all x1, starting transfers between devices, step(): back = lax.all_to_all(back, 'ep', split_axis=0, concat_axis=0, tiled=True)  10.4 us
    ppermute x3, waiting for transfers between devices, step(): kept.append(lax.ppermute(mine, 'tp', right))  8.69 us
  transfers between devices with their start and end apart: 22, of which 9 were waited for; matrix products, arithmetic and copies ran while one was open for 1% of the time, Pallas kernels for 4%

profile of v2, /device:TPU:14, one launch (start us, length us, event | category | flops | bytes accessed | tf_op | source)
XLA Modules:
  0.0 195.6 jit_solution(13789559688780243891)
XLA Ops:
  0.6 5.6 %shard_map.110 = (bf16[1536,512]{1,0:T(8,128)(2,1)}, bf16[2,384,256]{2,1,0:T(8,128)(2,1)}) custom-call(s32[1]{0:T(128)} %bitcast.refs_0_, s32[2,256]{1,0:T(2,128)} %bitcast.17, f32[2,256]{1,0:T(2,128)} %bitcast.15, bf16[256,1024]{1,0:T(8,128)(2,1)} %refs_3_.1, bf16[256,1024]{1,0:T(8,128)(2,1)} %refs_4_.1), custom_call_target="tpu_custom_call" | custom-call | tf_op jit(solution)/shard_map/pallas_call | solution.py:257
  6.3 12.2 %all-to-all-start = ((bf16[64,24,512]{2,1,0:T(8,128)(2,1)}), bf16[64,24,512]{2,1,0:T(8,128)(2,1)S(1)}, u32[]{:S(2)}, u32[]{:S(2)}) async-start(bf16[64,24,512]{2,1,0:T(8,128)(2,1)} %bitcast.14), calls=%async_computation | async-start | bytes 3145728 | tf_op jit(solution)/shard_map/all_to_all | solution.py:283
  19.5 2.4 %collective-permute-start.3 = (bf16[2,1024,128]{2,1,0:T(8,128)(2,1)S(1)}, bf16[2,1024,128]{2,1,0:T(8,128)(2,1)S(1)}, u32[]{:S(2)}, u32[]{:S(2)}) collective-permute-start(bf16[2,1024,128]{2,1,0:T(8,128)(2,1)S(1)} %copy-done.5), channel_id=1, source_target_pairs={{0,1},{1,2},{2,3},{3,0},{4,5},{5,6},{6,7},{7,4},{8,9},{9,10},{10,1... | collective-permute-start | bytes 1572872 | tf_op jit(solution)/shard_map/ppermute | solution.py:270
  21.9 3.2 %collective-permute-start.6 = (bf16[2,128,1024]{2,1,0:T(8,128)(2,1)S(1)}, bf16[2,128,1024]{2,1,0:T(8,128)(2,1)S(1)}, u32[]{:S(2)}, u32[]{:S(2)}) collective-permute-start(bf16[2,128,1024]{2,1,0:T(8,128)(2,1)S(1)} %copy-done.6), channel_id=1, source_target_pairs={{0,1},{1,2},{2,3},{3,0},{4,5},{5,6},{6,7},{7,4},{8,9},{9,10},{10,1... | collective-permute-start | bytes 1572872 | tf_op jit(solution)/shard_map/ppermute | solution.py:270
  25.1 9.5 %collective-permute-done.1.refs_3_ = bf16[2,1024,128]{2,1,0:T(8,128)(2,1)S(1)} collective-permute-done((bf16[2,1024,128]{2,1,0:T(8,128)(2,1)S(1)}, bf16[2,1024,128]{2,1,0:T(8,128)(2,1)S(1)}, u32[]{:S(2)}, u32[]{:S(2)}) %collective-permute-start.1) | collective-permute-done | bytes 524320 | tf_op jit(solution)/shard_map/ppermute | solution.py:271
  34.8 11.1 %collective-permute-done.7.refs_11_ = bf16[2,128,1024]{2,1,0:T(8,128)(2,1)S(1)} collective-permute-done((bf16[2,128,1024]{2,1,0:T(8,128)(2,1)S(1)}, bf16[2,128,1024]{2,1,0:T(8,128)(2,1)S(1)}, u32[]{:S(2)}, u32[]{:S(2)}) %collective-permute-start.7) | collective-permute-done | bytes 524320 | tf_op jit(solution)/shard_map/ppermute | solution.py:271
  45.9 2.1 %collective-permute-start.8 = (bf16[1,128,1024]{2,1,0:T(8,128)(2,1)S(1)}, bf16[1,128,1024]{2,1,0:T(8,128)(2,1)S(1)}, u32[]{:S(2)}, u32[]{:S(2)}) collective-permute-start(bf16[1,128,1024]{2,1,0:T(8,128)(2,1)S(1)} %slice.16), channel_id=1, source_target_pairs={{0,3},{1,0},{2,1},{3,2},{4,7},{5,4},{6,5},{7,6},{8,11},{9,8},{10,9... | collective-permute-start | bytes 786440 | tf_op jit(solution)/shard_map/ppermute | solution.py:274
  48.0 8.7 %collective-permute-done.refs_2_ = bf16[2,1024,128]{2,1,0:T(8,128)(2,1)S(1)} collective-permute-done((bf16[2,1024,128]{2,1,0:T(8,128)(2,1)S(1)}, bf16[2,1024,128]{2,1,0:T(8,128)(2,1)S(1)}, u32[]{:S(2)}, u32[]{:S(2)}) %collective-permute-start) | collective-permute-done | bytes 524320 | tf_op jit(solution)/shard_map/ppermute | solution.py:270
  56.7 3.6 %collective-permute-start.9 = (bf16[1,128,1024]{2,1,0:T(8,128)(2,1)S(1)}, bf16[1,128,1024]{2,1,0:T(8,128)(2,1)S(1)}, u32[]{:S(2)}, u32[]{:S(2)}) collective-permute-start(bf16[1,128,1024]{2,1,0:T(8,128)(2,1)S(1)} %slice.17), channel_id=1, source_target_pairs={{0,1},{1,2},{2,3},{3,0},{4,5},{5,6},{6,7},{7,4},{8,9},{9,10},{10,1... | collective-permute-start | bytes 786440 | tf_op jit(solution)/shard_map/ppermute | solution.py:275
  60.3 12.8 %collective-permute-done.8.refs_12_ = bf16[1,128,1024]{2,1,0:T(8,128)(2,1)S(1)} collective-permute-done((bf16[1,128,1024]{2,1,0:T(8,128)(2,1)S(1)}, bf16[1,128,1024]{2,1,0:T(8,128)(2,1)S(1)}, u32[]{:S(2)}, u32[]{:S(2)}) %collective-permute-start.8) | collective-permute-done | bytes 262176 | tf_op jit(solution)/shard_map/ppermute | solution.py:274
  75.2 8.9 %shard_map.111 = f32[3584,128]{1,0:T(8,128)} custom-call(bf16[1536,512]{1,0:T(8,128)(2,1)} %bitcast.10, bf16[2,1024,128]{2,1,0:T(8,128)(2,1)} %refs_5_.3, bf16[2,1024,128]{2,1,0:T(8,128)(2,1)} %copy-done.12, bf16[2,1024,128]{2,1,0:T(8,128)(2,1)} %copy-done.10, bf16[2,1024,128]{2,1,0:T(8,128)(2,1)} %copy-done.14, bf16[2,1024,128]{2,1,0:T(8,128)(2,1)} %refs_6_.1, ...), custom_call_target="tpu_custom_call" | custom-call | tf_op jit(solution)/shard_map/pallas_call | solution.py:257
  84.1 2.5 %convert_element_type.4 = f16[3584,128]{1,0:T(8,128)(2,1)} convert(f32[3584,128]{1,0:T(8,128)} %shard_map.111) | non-fusion elementwise | flops 458752 | bytes 2752512 | tf_op jit(solution)/shard_map/convert_element_type | solution.py:300
  86.6 10.4 %all-to-all-start.1 = ((f16[64,56,128]{2,1,0:T(8,128)(2,1)}), f16[64,56,128]{2,1,0:T(8,128)(2,1)S(1)}, u32[]{:S(2)}, u32[]{:S(2)}) async-start(f16[64,56,128]{2,1,0:T(8,128)(2,1)} %bitcast.5), calls=%async_computation.1 | async-start | bytes 1835008 | tf_op jit(solution)/shard_map/all_to_all | solution.py:301
  97.2 3.2 %collective-permute-start.16 = (bf16[1536,512]{1,0:T(8,128)(2,1)S(1)}, bf16[1536,512]{1,0:T(8,128)(2,1)S(1)}, u32[]{:S(2)}, u32[]{:S(2)}) collective-permute-start(bf16[1536,512]{1,0:T(8,128)(2,1)S(1)} %bitcast.13), channel_id=1, source_target_pairs={{0,1},{1,2},{2,3},{3,0},{4,5},{5,6},{6,7},{7,4},{8,9},{9,10},{10,1... | collective-permute-start | bytes 4718600 | tf_op jit(solution)/shard_map/ppermute | solution.py:287
  100.4 34.4 %collective-permute-done.17.refs_2_ = bf16[1536,512]{1,0:T(8,128)(2,1)S(1)} collective-permute-done((bf16[1536,512]{1,0:T(8,128)(2,1)S(1)}, bf16[1536,512]{1,0:T(8,128)(2,1)S(1)}, u32[]{:S(2)}, u32[]{:S(2)}) %collective-permute-start.17) | collective-permute-done | bytes 1572896 | tf_op jit(solution)/shard_map/ppermute | solution.py:288
  136.5 2.9 %collective-permute-start.19 = (bf16[768,512]{1,0:T(8,128)(2,1)S(1)}, bf16[768,512]{1,0:T(8,128)(2,1)S(1)}, u32[]{:S(2)}, u32[]{:S(2)}) collective-permute-start(bf16[768,512]{1,0:T(8,128)(2,1)S(1)} %slice.19), channel_id=1, source_target_pairs={{0,1},{1,2},{2,3},{3,0},{4,5},{5,6},{6,7},{7,4},{8,9},{9,10},{10,1... | collective-permute-start | bytes 2359304 | tf_op jit(solution)/shard_map/ppermute | solution.py:291
  140.8 3.9 %shard_map.112 = (f32[72,1024]{1,0:T(8,128)}, f32[72,1024]{1,0:T(8,128)}, f32[72,1024]{1,0:T(8,128)}, f32[72,1024]{1,0:T(8,128)}) custom-call(s32[1]{0:T(128)} %bitcast.refs_0_, f32[3584,128]{1,0:T(8,128)} %bitcast_convert_fusion.refs_1_, bf16[2,384,256]{2,1,0:T(8,128)(2,1)} %get-tuple-element.17.refs_2_), custom_call_target="tpu_custom_call" | custom-call | tf_op jit(solution)/shard_map/pallas_call | solution.py:257
  145.2 1.6 collective-permute-start.11
  146.8 21.3 %collective-permute-done.10.from_left = f32[72,1024]{1,0:T(8,128)S(1)} collective-permute-done((f32[72,1024]{1,0:T(8,128)}, f32[72,1024]{1,0:T(8,128)S(1)}, u32[]{:S(2)}, u32[]{:S(2)}) %collective-permute-start.10) | collective-permute-done | bytes 294944 | tf_op jit(solution)/shard_map/ppermute | solution.py:313
  169.0 1.9 shard_map.113
  170.9 4.4 %collective-permute-start.14 = (bf16[64,1024]{1,0:T(8,128)(2,1)}, bf16[64,1024]{1,0:T(8,128)(2,1)S(1)}, u32[]{:S(2)}, u32[]{:S(2)}) collective-permute-start(bf16[64,1024]{1,0:T(8,128)(2,1)} %get-tuple-element.22.refs_1_), channel_id=1, source_target_pairs={{0,3},{1,0},{2,1},{3,2},{4,7},{5,4},{6,5},{7,6},{8,11},{9,8},{10,9... | collective-permute-start | bytes 393224 | tf_op jit(solution)/shard_map/ppermute | solution.py:324
  175.3 2.7 %collective-permute-done.15.refs_4_ = bf16[64,1024]{1,0:T(8,128)(2,1)S(1)} collective-permute-done((bf16[64,1024]{1,0:T(8,128)(2,1)}, bf16[64,1024]{1,0:T(8,128)(2,1)S(1)}, u32[]{:S(2)}, u32[]{:S(2)}) %collective-permute-start.15) | collective-permute-done | bytes 131104 | tf_op jit(solution)/shard_map/ppermute | solution.py:325
  181.2 1.9 shard_map.114
  184.0 11.6 %shard_map.115 = (f32[2,1024,128]{2,1,0:T(8,128)}, f32[2,1024,128]{2,1,0:T(8,128)}, f32[2,128,1024]{2,1,0:T(8,128)}) custom-call(bf16[1536,512]{1,0:T(8,128)(2,1)} %bitcast.11, bf16[1536,512]{1,0:T(8,128)(2,1)} %copy-done.3, bf16[1536,512]{1,0:T(8,128)(2,1)} %copy-done.2, bf16[768,512]{1,0:T(8,128)(2,1)} %collective-permute-done.18.refs_3_, ...), custom_call_target="tpu_custom_call" | custom-call | tf_op jit(solution)/shard_map/pallas_call | solution.py:257
  (78 shorter events, 11.8 us)
Async XLA Ops:
  6.3 67.8 %all-to-all-start = ((bf16[64,24,512]{2,1,0:T(8,128)(2,1)}), bf16[64,24,512]{2,1,0:T(8,128)(2,1)S(1)}, u32[]{:S(2)}, u32[]{:S(2)}) async-start(bf16[64,24,512]{2,1,0:T(8,128)(2,1)} %bitcast.14), calls=%async_computation | async-start | bytes 3145728 | tf_op jit(solution)/shard_map/all_to_all | solution.py:283
  18.5 16.1 %collective-permute-start.1 = (bf16[2,1024,128]{2,1,0:T(8,128)(2,1)S(1)}, bf16[2,1024,128]{2,1,0:T(8,128)(2,1)S(1)}, u32[]{:S(2)}, u32[]{:S(2)}) collective-permute-start(bf16[2,1024,128]{2,1,0:T(8,128)(2,1)S(1)} %copy-done.4), channel_id=1, source_target_pairs={{0,3},{1,0},{2,1},{3,2},{4,7},{5,4},{6,5},{7,6},{8,11},{9,8},{10,9... | collective-permute-start | bytes 1572872 | tf_op jit(solution)/shard_map/ppermute | solution.py:271
  19.5 15.2 %collective-permute-start.3 = (bf16[2,1024,128]{2,1,0:T(8,128)(2,1)S(1)}, bf16[2,1024,128]{2,1,0:T(8,128)(2,1)S(1)}, u32[]{:S(2)}, u32[]{:S(2)}) collective-permute-start(bf16[2,1024,128]{2,1,0:T(8,128)(2,1)S(1)} %copy-done.5), channel_id=1, source_target_pairs={{0,1},{1,2},{2,3},{3,0},{4,5},{5,6},{6,7},{7,4},{8,9},{9,10},{10,1... | collective-permute-start | bytes 1572872 | tf_op jit(solution)/shard_map/ppermute | solution.py:270
  21.9 24.0 %collective-permute-start.7 = (bf16[2,128,1024]{2,1,0:T(8,128)(2,1)S(1)}, bf16[2,128,1024]{2,1,0:T(8,128)(2,1)S(1)}, u32[]{:S(2)}, u32[]{:S(2)}) collective-permute-start(bf16[2,128,1024]{2,1,0:T(8,128)(2,1)S(1)} %copy-done.6), channel_id=1, source_target_pairs={{0,3},{1,0},{2,1},{3,2},{4,7},{5,4},{6,5},{7,6},{8,11},{9,8},{10,9... | collective-permute-start | bytes 1572872 | tf_op jit(solution)/shard_map/ppermute | solution.py:271
  21.9 24.0 %collective-permute-start.6 = (bf16[2,128,1024]{2,1,0:T(8,128)(2,1)S(1)}, bf16[2,128,1024]{2,1,0:T(8,128)(2,1)S(1)}, u32[]{:S(2)}, u32[]{:S(2)}) collective-permute-start(bf16[2,128,1024]{2,1,0:T(8,128)(2,1)S(1)} %copy-done.6), channel_id=1, source_target_pairs={{0,1},{1,2},{2,3},{3,0},{4,5},{5,6},{6,7},{7,4},{8,9},{9,10},{10,1... | collective-permute-start | bytes 1572872 | tf_op jit(solution)/shard_map/ppermute | solution.py:270
  25.1 31.6 %collective-permute-start = (bf16[2,1024,128]{2,1,0:T(8,128)(2,1)S(1)}, bf16[2,1024,128]{2,1,0:T(8,128)(2,1)S(1)}, u32[]{:S(2)}, u32[]{:S(2)}) collective-permute-start(bf16[2,1024,128]{2,1,0:T(8,128)(2,1)S(1)} %copy-done.4), channel_id=1, source_target_pairs={{0,1},{1,2},{2,3},{3,0},{4,5},{5,6},{6,7},{7,4},{8,9},{9,10},{10,1... | collective-permute-start | bytes 1572872 | tf_op jit(solution)/shard_map/ppermute | solution.py:270
  34.6 38.5 %copy-start.10 = (bf16[2,1024,128]{2,1,0:T(8,128)(2,1)}, bf16[2,1024,128]{2,1,0:T(8,128)(2,1)S(1)}, u32[]{:S(2)}) copy-start(bf16[2,1024,128]{2,1,0:T(8,128)(2,1)S(1)} %collective-permute-done.1.refs_3_) | copy-start | bytes 1572868
  34.6 25.7 %collective-permute-start.4 = (bf16[2,1024,128]{2,1,0:T(8,128)(2,1)S(1)}, bf16[2,1024,128]{2,1,0:T(8,128)(2,1)S(1)}, u32[]{:S(2)}, u32[]{:S(2)}) collective-permute-start(bf16[2,1024,128]{2,1,0:T(8,128)(2,1)S(1)} %copy-done.5), channel_id=1, source_target_pairs={{0,3},{1,0},{2,1},{3,2},{4,7},{5,4},{6,5},{7,6},{8,11},{9,8},{10,9... | collective-permute-start | bytes 1572872 | tf_op jit(solution)/shard_map/ppermute | solution.py:271
  34.6 38.5 %copy-start.11 = (bf16[2,1024,128]{2,1,0:T(8,128)(2,1)}, bf16[2,1024,128]{2,1,0:T(8,128)(2,1)S(1)}, u32[]{:S(2)}) copy-start(bf16[2,1024,128]{2,1,0:T(8,128)(2,1)S(1)} %collective-permute-done.3.refs_6_) | copy-start | bytes 1572868
  34.7 38.5 %collective-permute-start.2 = (bf16[2,1024,128]{2,1,0:T(8,128)(2,1)S(1)}, bf16[2,1024,128]{2,1,0:T(8,128)(2,1)S(1)}, u32[]{:S(2)}, u32[]{:S(2)}) collective-permute-start(bf16[2,1024,128]{2,1,0:T(8,128)(2,1)S(1)} %collective-permute-done.1.refs_3_), channel_id=1, source_target_pairs={{0,3},{1,0},{2,1},{3,2},{4,7},{5,4},{6,5},{7,6},{8,11},{9,8},{10,9... | collective-permute-start | bytes 1572872 | tf_op jit(solution)/shard_map/ppermute | solution.py:272
  45.9 28.2 %collective-permute-start.5 = (bf16[2,1024,128]{2,1,0:T(8,128)(2,1)S(1)}, bf16[2,1024,128]{2,1,0:T(8,128)(2,1)}, u32[]{:S(2)}, u32[]{:S(2)}) collective-permute-start(bf16[2,1024,128]{2,1,0:T(8,128)(2,1)S(1)} %collective-permute-done.3.refs_6_), channel_id=1, source_target_pairs={{0,1},{1,2},{2,3},{3,0},{4,5},{5,6},{6,7},{7,4},{8,9},{9,10},{10,1... | collective-permute-start | bytes 1572872 | tf_op jit(solution)/shard_map/ppermute | solution.py:273
  45.9 27.2 %collective-permute-start.8 = (bf16[1,128,1024]{2,1,0:T(8,128)(2,1)S(1)}, bf16[1,128,1024]{2,1,0:T(8,128)(2,1)S(1)}, u32[]{:S(2)}, u32[]{:S(2)}) collective-permute-start(bf16[1,128,1024]{2,1,0:T(8,128)(2,1)S(1)} %slice.16), channel_id=1, source_target_pairs={{0,3},{1,0},{2,1},{3,2},{4,7},{5,4},{6,5},{7,6},{8,11},{9,8},{10,9... | collective-permute-start | bytes 786440 | tf_op jit(solution)/shard_map/ppermute | solution.py:274
  56.7 16.4 %collective-permute-start.9 = (bf16[1,128,1024]{2,1,0:T(8,128)(2,1)S(1)}, bf16[1,128,1024]{2,1,0:T(8,128)(2,1)S(1)}, u32[]{:S(2)}, u32[]{:S(2)}) collective-permute-start(bf16[1,128,1024]{2,1,0:T(8,128)(2,1)S(1)} %slice.17), channel_id=1, source_target_pairs={{0,1},{1,2},{2,3},{3,0},{4,5},{5,6},{6,7},{7,4},{8,9},{9,10},{10,1... | collective-permute-start | bytes 786440 | tf_op jit(solution)/shard_map/ppermute | solution.py:275
  86.6 52.7 %all-to-all-start.1 = ((f16[64,56,128]{2,1,0:T(8,128)(2,1)}), f16[64,56,128]{2,1,0:T(8,128)(2,1)S(1)}, u32[]{:S(2)}, u32[]{:S(2)}) async-start(f16[64,56,128]{2,1,0:T(8,128)(2,1)} %bitcast.5), calls=%async_computation.1 | async-start | bytes 1835008 | tf_op jit(solution)/shard_map/all_to_all | solution.py:301
  97.1 37.7 %collective-permute-start.17 = (bf16[1536,512]{1,0:T(8,128)(2,1)S(1)}, bf16[1536,512]{1,0:T(8,128)(2,1)S(1)}, u32[]{:S(2)}, u32[]{:S(2)}) collective-permute-start(bf16[1536,512]{1,0:T(8,128)(2,1)S(1)} %bitcast.12), channel_id=1, source_target_pairs={{0,3},{1,0},{2,1},{3,2},{4,7},{5,4},{6,5},{7,6},{8,11},{9,8},{10,9... | collective-permute-start | bytes 4718600 | tf_op jit(solution)/shard_map/ppermute | solution.py:288
  97.2 37.8 %collective-permute-start.16 = (bf16[1536,512]{1,0:T(8,128)(2,1)S(1)}, bf16[1536,512]{1,0:T(8,128)(2,1)S(1)}, u32[]{:S(2)}, u32[]{:S(2)}) collective-permute-start(bf16[1536,512]{1,0:T(8,128)(2,1)S(1)} %bitcast.13), channel_id=1, source_target_pairs={{0,1},{1,2},{2,3},{3,0},{4,5},{5,6},{6,7},{7,4},{8,9},{9,10},{10,1... | collective-permute-start | bytes 4718600 | tf_op jit(solution)/shard_map/ppermute | solution.py:287
  134.9 48.3 %collective-permute-start.18 = (bf16[768,512]{1,0:T(8,128)(2,1)S(1)}, bf16[768,512]{1,0:T(8,128)(2,1)}, u32[]{:S(2)}, u32[]{:S(2)}) collective-permute-start(bf16[768,512]{1,0:T(8,128)(2,1)S(1)} %slice.18), channel_id=1, source_target_pairs={{0,3},{1,0},{2,1},{3,2},{4,7},{5,4},{6,5},{7,6},{8,11},{9,8},{10,9... | collective-permute-start | bytes 2359304 | tf_op jit(solution)/shard_map/ppermute | solution.py:290
  136.5 46.6 %collective-permute-start.19 = (bf16[768,512]{1,0:T(8,128)(2,1)S(1)}, bf16[768,512]{1,0:T(8,128)(2,1)S(1)}, u32[]{:S(2)}, u32[]{:S(2)}) collective-permute-start(bf16[768,512]{1,0:T(8,128)(2,1)S(1)} %slice.19), channel_id=1, source_target_pairs={{0,1},{1,2},{2,3},{3,0},{4,5},{5,6},{6,7},{7,4},{8,9},{9,10},{10,1... | collective-permute-start | bytes 2359304 | tf_op jit(solution)/shard_map/ppermute | solution.py:291
  144.8 23.3 %collective-permute-start.10 = (f32[72,1024]{1,0:T(8,128)}, f32[72,1024]{1,0:T(8,128)S(1)}, u32[]{:S(2)}, u32[]{:S(2)}) collective-permute-start(f32[72,1024]{1,0:T(8,128)} %get-tuple-element.19), channel_id=1, source_target_pairs={{0,1},{1,2},{2,3},{3,0},{4,5},{5,6},{6,7},{7,4},{8,9},{9,10},{10,1... | collective-permute-start | bytes 884744 | tf_op jit(solution)/shard_map/ppermute | solution.py:313
  145.2 22.9 %collective-permute-start.11 = (f32[72,1024]{1,0:T(8,128)}, f32[72,1024]{1,0:T(8,128)S(1)}, u32[]{:S(2)}, u32[]{:S(2)}) collective-permute-start(f32[72,1024]{1,0:T(8,128)} %get-tuple-element.20), channel_id=1, source_target_pairs={{0,3},{1,0},{2,1},{3,2},{4,7},{5,4},{6,5},{7,6},{8,11},{9,8},{10,9... | collective-permute-start | bytes 884744 | tf_op jit(solution)/shard_map/ppermute | solution.py:314
  146.8 21.3 %collective-permute-start.12 = (f32[72,1024]{1,0:T(8,128)}, f32[72,1024]{1,0:T(8,128)S(1)}, u32[]{:S(2)}, u32[]{:S(2)}) collective-permute-start(f32[72,1024]{1,0:T(8,128)} %get-tuple-element.21), channel_id=1, source_target_pairs={{0,2},{1,3},{2,0},{3,1},{4,6},{5,7},{6,4},{7,5},{8,10},{9,11},{10,... | collective-permute-start | bytes 884744 | tf_op jit(solution)/shard_map/ppermute | solution.py:315
  170.9 7.1 %collective-permute-start.15 = (bf16[64,1024]{1,0:T(8,128)(2,1)}, bf16[64,1024]{1,0:T(8,128)(2,1)S(1)}, u32[]{:S(2)}, u32[]{:S(2)}) collective-permute-start(bf16[64,1024]{1,0:T(8,128)(2,1)} %get-tuple-element.22.refs_1_), channel_id=1, source_target_pairs={{0,2},{1,3},{2,0},{3,1},{4,6},{5,7},{6,4},{7,5},{8,10},{9,11},{10,... | collective-permute-start | bytes 393224 | tf_op jit(solution)/shard_map/ppermute | solution.py:325
  170.9 8.4 %collective-permute-start.14 = (bf16[64,1024]{1,0:T(8,128)(2,1)}, bf16[64,1024]{1,0:T(8,128)(2,1)S(1)}, u32[]{:S(2)}, u32[]{:S(2)}) collective-permute-start(bf16[64,1024]{1,0:T(8,128)(2,1)} %get-tuple-element.22.refs_1_), channel_id=1, source_target_pairs={{0,3},{1,0},{2,1},{3,2},{4,7},{5,4},{6,5},{7,6},{8,11},{9,8},{10,9... | collective-permute-start | bytes 393224 | tf_op jit(solution)/shard_map/ppermute | solution.py:324
  175.3 5.2 %collective-permute-start.13 = (bf16[64,1024]{1,0:T(8,128)(2,1)}, bf16[64,1024]{1,0:T(8,128)(2,1)S(1)}, u32[]{:S(2)}, u32[]{:S(2)}) collective-permute-start(bf16[64,1024]{1,0:T(8,128)(2,1)} %get-tuple-element.22.refs_1_), channel_id=1, source_target_pairs={{0,1},{1,2},{2,3},{3,0},{4,5},{5,6},{6,7},{7,4},{8,9},{9,10},{10,1... | collective-permute-start | bytes 393224 | tf_op jit(solution)/shard_map/ppermute | solution.py:323
  (21 other events, 149.7 us)

commit v3 on v2

v3 whole, which is shorter than its diff:
```python
import jax
import jax.numpy as jnp
from jax import lax
from jax.experimental import pallas as pl
from jax.experimental.pallas import tpu as pltpu
from jax.sharding import PartitionSpec as P


F32 = jnp.float32
I16 = jnp.int16
BF16 = jnp.bfloat16
I32 = jnp.int32
LANES = 128
SUBLANES = 8
BLOCK = 16
PARTS = 4
TOP_CODE = 32766.0
STEPS = 8192.0
FINE = 32768.0
VMEM = pltpu.VMEM
SMEM = pltpu.SMEM
NN = ((1,), (0,))
NT = ((1,), (1,))
TN = ((0,), (0,))


def mm(a, b, dims=NN):
    return lax.dot_general(a, b, (dims, ((), ())), preferred_element_type=F32)


def iota(shape, dim):
    return lax.broadcasted_iota(I32, shape, dim)


def split3(value):
    high = value.astype(BF16)
    rest = value - high.astype(F32)
    middle = rest.astype(BF16)
    low = (rest - middle.astype(F32)).astype(BF16)
    return high, middle, low


def exponent(value):
    return jnp.floor(jnp.log(jnp.maximum(value, 1e-30)) * 1.4426950408889634)


def row_scale(power, steps):
    return steps * jnp.exp2(power) * (1.0 / (STEPS * TOP_CODE))


def code_rows(value):
    largest = jnp.maximum(jnp.max(jnp.abs(value), axis=1, keepdims=True), 1e-30)
    power = exponent(largest)
    steps = jnp.ceil(largest * jnp.exp2(-power) * STEPS)
    return jnp.round(value * (1.0 / row_scale(power, steps))), power, steps


def code_values(value):
    power = exponent(jnp.abs(value))
    value = value * jnp.exp2(-power) * STEPS
    coarse = jnp.round(value)
    return power, coarse, jnp.round((value - coarse) * FINE)


def decode_values(power, coarse, fine):
    return (coarse + fine * (1.0 / FINE)) * (jnp.exp2(power) * (1.0 / STEPS))


def to_code(value):
    return value.astype(I32).astype(I16)


def from_code(value):
    return value.astype(I32).astype(F32)


def slot_rows(experts, local_experts, quarter, member, routing):
    token_count = routing.shape[1]
    expert = iota((experts, token_count), 0)
    chosen = [routing[k : k + 1, :] for k in range(2)]
    onehot = [jnp.where(expert == c, 1.0, 0.0) for c in chosen]
    earlier = iota((token_count, token_count), 0)
    later = iota((token_count, token_count), 1)
    upper = jnp.where(earlier < later, 1.0, 0.0).astype(BF16)
    before = mm((onehot[0] + onehot[1]).astype(BF16), upper)
    places = []
    for k in range(2):
        position = jnp.sum(onehot[k] * before, axis=0, keepdims=True).astype(I32)
        local = position - member[0] * quarter
        present = (local >= 0) & (local < quarter)
        device = chosen[k] // local_experts
        places.append((present, device, (chosen[k] - device * local_experts) * quarter + local))
    return places


def picked(rows_out, source, places, group, weights=None):
    token_count = source.shape[0]
    row_count, part_width = rows_out.shape
    chunk = PARTS * group
    row = iota((row_count, token_count), 0)
    at = [jnp.where(present, device * chunk + within, -chunk) for present, device, within in places]
    total = None
    for part in range(PARTS):
        hits = [jnp.where(row == r + part * group, 1.0, 0.0) for r in at]
        values = source[:, part * part_width : (part + 1) * part_width]
        value = mm((hits[0] + hits[1]).astype(BF16), values)
        if weights is not None:
            weighted = hits[0] * weights[0:1, :] + hits[1] * weights[1:2, :]
            value = jnp.sum(weighted, axis=1, keepdims=True) * value
        total = value if total is None else total + value
    rows_out[...] = total.astype(BF16)


def token_kernel(experts, local_experts, quarter, member, routing, tokens, rows_out):
    places = slot_rows(experts, local_experts, quarter, member, routing)
    picked(rows_out, tokens, places, local_experts * quarter)


def scaled_kernel(
    experts, local_experts, quarter, member, routing, weights, cotangent, rows_out, pick
):
    places = slot_rows(experts, local_experts, quarter, member, routing)
    picked(rows_out, cotangent, places, local_experts * quarter, weights)
    slot = iota(pick.shape[1:], 0)
    devices = experts // local_experts
    for k, (present, device, within) in enumerate(places):
        wanted = jnp.where(present, within * devices + device, -1)
        pick[k] = jnp.where(slot == wanted, 1.0, 0.0).astype(BF16)


def land(source, expert, local_experts, quarter, rows, offset):
    part_width = source.shape[1]
    group = local_experts * quarter
    chunk = PARTS * group
    out_rows = BLOCK * quarter
    index = iota((PARTS * out_rows, 1), 0)
    part = index // out_rows
    rest = index - part * out_rows
    slot = rest // BLOCK
    wanted = (rest - slot * BLOCK) * chunk + part * group + expert * quarter + slot
    column = iota((PARTS * out_rows, BLOCK * chunk), 1)
    permutation = jnp.where(column == wanted, 1.0, 0.0).astype(BF16)
    for block in range(source.shape[0] // (BLOCK * chunk)):
        moved = mm(permutation, source[block * BLOCK * chunk : (block + 1) * BLOCK * chunk, :])
        moved = moved.astype(BF16)
        at = offset + block * out_rows
        for p in range(PARTS):
            columns = slice(p * part_width, (p + 1) * part_width)
            rows[at : at + out_rows, columns] = moved[p * out_rows : (p + 1) * out_rows]


def hidden_terms(gate_pre, up_pre, hidden_grad):
    gate_pre = gate_pre.astype(BF16).astype(F32)
    up_pre = up_pre.astype(BF16).astype(F32)
    sigmoid = jax.nn.sigmoid(gate_pre)
    activated = gate_pre * sigmoid
    hidden = activated * up_pre
    gate_grad = (hidden_grad * up_pre * sigmoid * (1.0 + gate_pre * (1.0 - sigmoid))).astype(BF16)
    up_grad = (hidden_grad * activated).astype(BF16)
    return hidden, gate_grad, up_grad


def input_kernel(local_experts, quarter, landed_rows, landed_scaled, *refs):
    gates, ups, downs = refs[0:4], refs[4:8], refs[8:11]
    down_even, down_odd, out, rows, scaled, coded = refs[11:]
    own, _ = rows.shape
    slots = local_experts * quarter
    devices = own // quarter
    stride = (slots + 1) * SUBLANES
    for i in range(slots, SUBLANES):
        at = slots * SUBLANES + i
        coded[pl.ds(at, devices, stride=stride), :] = jnp.zeros((devices, LANES), F32)
    for expert in range(local_experts):
        land(landed_rows, expert, local_experts, quarter, rows, 0)
        land(landed_scaled, expert, local_experts, quarter, scaled, 0)
        gate = jnp.concatenate([g[expert] for g in gates], axis=1)
        up = jnp.concatenate([u[expert] for u in ups], axis=1)
        last = (down_even, down_odd)[expert][0]
        down = jnp.concatenate([d[expert] for d in downs] + [last], axis=0)
        hidden_grad = mm(scaled[...], down, NT)
        hidden, gate_grad, up_grad = hidden_terms(mm(rows[...], gate), mm(rows[...], up), hidden_grad)
        product = jnp.sum(hidden_grad * hidden, axis=1, keepdims=True)
        grad = mm(gate_grad, gate, NT) + mm(up_grad, up, NT)
        grad, power, steps = code_rows(grad)
        lane = iota((own, LANES), 1)
        tail = jnp.zeros((own, LANES), F32)
        for at, column in enumerate((power, steps) + code_values(product)):
            tail = jnp.where(lane == at, column, tail)
        for block in range(devices // BLOCK):
            for q in range(quarter):
                at = (block * quarter + q) * BLOCK
                to = block * BLOCK * stride
                slot = expert * quarter + q
                for i in range(SUBLANES):
                    piece = grad[at : at + BLOCK, i * LANES : (i + 1) * LANES]
                    coded[pl.ds(to + slot * SUBLANES + i, BLOCK, stride=stride), :] = piece
                to += slots * SUBLANES + slot
                coded[pl.ds(to, BLOCK, stride=stride), :] = tail[at : at + BLOCK]
    out[...] = to_code(coded[...])


def weight_kernel(local_experts, quarter, *refs):
    (gate, up, down), (gate_out, up_out, down_out), (rows, scaled) = refs[8:11], refs[11:14], refs[14:]
    own = rows.shape[0] // 4
    hidden_width = gate.shape[2]

    def one(expert, carry):
        for i in range(4):
            land(refs[i], expert, local_experts, quarter, rows, i * own)
            land(refs[4 + i], expert, local_experts, quarter, scaled, i * own)
        both = mm(rows[...], jnp.concatenate([gate[expert], up[expert]], axis=1))
        hidden_grad = mm(scaled[...], down[expert], NT)
        hidden, gate_grad, up_grad = hidden_terms(
            both[:, :hidden_width], both[:, hidden_width:], hidden_grad
        )
        grads = mm(rows[...], jnp.concatenate([gate_grad, up_grad], axis=1), TN)
        gate_out[expert] = grads[:, :hidden_width]
        up_out[expert] = grads[:, hidden_width:]
        down_out[expert] = mm(hidden.astype(BF16), scaled[...], TN)
        return carry

    lax.fori_loop(0, local_experts, one, 0)


def member_rows(member, distance, members, count):
    return pl.ds(pl.multiple_of(lax.rem(member + distance, members) * count, count), count)


def combine_kernel(members, devices, member, coded, pick, *refs):
    outs, total, back = refs[:-2], refs[-2], refs[-1]
    back[...] = from_code(coded[...])
    token_count, tail_width = total.shape
    width = tail_width - LANES
    slots = pick.shape[1] // devices
    stride = (slots + 1) * SUBLANES
    tails = [
        back[pl.ds(slots * SUBLANES + slot, devices, stride=stride), :] for slot in range(slots)
    ]
    tail = jnp.concatenate(tails, axis=0)
    scale = row_scale(tail[:, 0:1], tail[:, 1:2])
    columns = []
    for i in range(SUBLANES):
        pieces = [
            back[pl.ds(slot * SUBLANES + i, devices, stride=stride), :] for slot in range(slots)
        ]
        columns.append(jnp.concatenate(pieces, axis=0))
    grad = jnp.concatenate(columns, axis=1) * scale
    both = pick[0] + pick[1]
    grad, power, steps = code_rows(sum(mm(both, part, TN) for part in split3(grad)))
    total[:, 0:width] = grad
    lane = iota((token_count, LANES), 1)
    total[:, width:] = jnp.where(lane == 0, power, jnp.where(lane == 1, steps, 0.0))
    product = decode_values(tail[:, 2:3], tail[:, 3:4], tail[:, 4:5])
    sums = [jnp.sum(pick[k].astype(F32) * product, axis=0, keepdims=True) for k in range(2)]
    power, coarse, fine = code_values(jnp.concatenate(sums, axis=1))
    spare = jnp.zeros((1, tail_width - 4 * token_count), F32)
    first = jnp.concatenate([power, coarse, spare], axis=1)
    second = jnp.concatenate([fine, jnp.zeros_like(fine), spare], axis=1)
    line = iota((SUBLANES, tail_width), 0)
    lines = to_code(jnp.where(line == 0, first, jnp.where(line == 1, second, 0.0)))
    count = token_count // members
    for out, distance in zip(outs, (0, 1, 3, 2)):
        out[0:count, :] = to_code(total[member_rows(member[0], distance, members, count), :])
        out[count : count + SUBLANES, :] = lines


def sum_kernel(own, from_left, from_right, from_opposite, weights, grad_out, gates_out):
    count, width = grad_out.shape
    token_count = weights.shape[1]
    parts = [from_code(part[...]) for part in (own, from_left, from_right, from_opposite)]
    grads = [
        part[:count, :width] * row_scale(part[:count, width : width + 1], part[:count, width + 1 : width + 2])
        for part in parts
    ]
    grad_out[...] = ((grads[0] + grads[3]) + (grads[1] + grads[2])).astype(BF16)
    values = 2 * token_count
    products = [
        decode_values(
            part[count : count + 1, 0:values],
            part[count : count + 1, values : 2 * values],
            part[count + 1 : count + 2, 0:values],
        )
        for part in parts
    ]
    product = (products[0] + products[3]) + (products[1] + products[2])
    for k in range(2):
        gates_out[k : k + 1, :] = product[:, k * token_count : (k + 1) * token_count] / weights[k : k + 1, :]


def place_kernel(members, member, own, from_left, from_right, from_opposite, out):
    count = own.shape[0]
    for piece, distance in ((own, 0), (from_left, 3), (from_right, 1), (from_opposite, 2)):
        out[member_rows(member[0], distance, members, count), :] = piece[...]


def step(tokens, cotangent, routing, gate_weights, gate_proj, up_proj, down_proj):
    token_count, model_width = tokens.shape
    top_count = routing.shape[1]
    local_experts, _, hidden_width = gate_proj.shape
    groups = lax.axis_size("ep")
    members = lax.axis_size("tp")
    experts = local_experts * groups
    capacity = members * (
        (3 * token_count * top_count + experts * members - 1) // (experts * members)
    )
    quarter = capacity // members
    slots = experts * quarter
    own = groups * quarter
    chunk = PARTS * local_experts * quarter
    part_width = model_width // PARTS
    member = lax.axis_index("tp").astype(I32).reshape(1)
    right = [(i, (i + 1) % members) for i in range(members)]
    left = [(i, (i - 1) % members) for i in range(members)]
    across = [(i, (i + 2) % members) for i in range(members)]
    whole = pl.BlockSpec(memory_space=VMEM)
    scalar = pl.BlockSpec(memory_space=SMEM)

    def call(kernel, out_shape, args, scalars=0, scratch=()):
        return pl.pallas_call(
            kernel,
            out_shape=out_shape,
            in_specs=[scalar] * scalars + [whole] * (len(args) - scalars),
            out_specs=jax.tree.map(lambda _: whole, out_shape),
            scratch_shapes=list(scratch),
        )(*args)

    def shape(dims, dtype):
        return jax.ShapeDtypeStruct(dims, dtype)

    gates, ups, downs = [gate_proj], [up_proj], [down_proj]
    for kept, mine in ((gates, gate_proj), (ups, up_proj), (downs, down_proj)):
        kept.append(lax.ppermute(mine, "tp", right))
        kept.append(lax.ppermute(mine, "tp", left))
    gates.append(lax.ppermute(gates[2], "tp", left))
    ups.append(lax.ppermute(ups[1], "tp", right))
    down_even = lax.ppermute(downs[2][0:1], "tp", left)
    down_odd = lax.ppermute(downs[1][1:2], "tp", right)

    sizes = (experts, local_experts, quarter)
    send_shape = shape((groups * chunk, part_width), BF16)

    def to_experts(send):
        send = send.reshape(groups, chunk, part_width)
        landed = lax.all_to_all(send, "ep", split_axis=0, concat_axis=0, tiled=True)
        return landed.reshape(groups * chunk, part_width)

    def swap(landed):
        return [landed, lax.ppermute(landed, "tp", right), lax.ppermute(landed, "tp", left)]

    send = call(
        lambda *refs: token_kernel(*sizes, *refs),
        send_shape,
        (member, routing.T, tokens),
        scalars=1,
    )
    rows = to_experts(send)
    send, pick = call(
        lambda *refs: scaled_kernel(*sizes, *refs),
        (send_shape, shape((2, slots, token_count), BF16)),
        (member, routing.T, gate_weights.T, cotangent),
        scalars=1,
    )
    scaled = to_experts(send)
    rows = swap(rows)
    scaled = swap(scaled)
    rows.append(lax.ppermute(rows[2], "tp", left))
    scaled.append(lax.ppermute(scaled[1], "tp", right))

    back_rows = (local_experts * quarter + 1) * SUBLANES
    back = call(
        lambda *refs: input_kernel(local_experts, quarter, *refs),
        shape((groups * back_rows, LANES), I16),
        (rows[0], scaled[0], *gates, *ups, *downs, down_even, down_odd),
        scratch=[VMEM((own, model_width), BF16)] * 2 + [VMEM((groups * back_rows, LANES), F32)],
    )
    back = back.reshape(groups, back_rows, LANES)
    back = lax.all_to_all(back, "ep", split_axis=0, concat_axis=0, tiled=True)
    back = back.reshape(groups * back_rows, LANES)
    count = token_count // members
    tail_width = model_width + LANES
    part = shape((count + SUBLANES, tail_width), I16)
    mine, to_right, to_left, to_across = call(
        lambda *refs: combine_kernel(members, groups, *refs),
        (part,) * 4,
        (member, back, pick),
        scalars=1,
        scratch=[VMEM((token_count, tail_width), F32), VMEM((groups * back_rows, LANES), F32)],
    )
    pieces = (
        lax.ppermute(to_right, "tp", right),
        lax.ppermute(to_left, "tp", left),
        lax.ppermute(to_across, "tp", across),
    )
    summed, gates_grad = call(
        sum_kernel,
        (shape((count, model_width), BF16), shape((top_count, token_count), F32)),
        (mine, *pieces, gate_weights.T),
    )
    pieces = (
        lax.ppermute(summed, "tp", right),
        lax.ppermute(summed, "tp", left),
        lax.ppermute(summed, "tp", across),
    )
    tokens_grad = call(
        lambda *refs: place_kernel(members, *refs),
        shape((token_count, model_width), BF16),
        (member, summed, *pieces),
        scalars=1,
    )

    gate_grad, up_grad, down_grad = call(
        lambda *refs: weight_kernel(local_experts, quarter, *refs),
        (
            shape((local_experts, model_width, hidden_width), F32),
            shape((local_experts, model_width, hidden_width), F32),
            shape((local_experts, hidden_width, model_width), F32),
        ),
        (*rows, *scaled, gate_proj, up_proj, down_proj),
        scratch=[VMEM((members * own, model_width), BF16)] * 2,
    )
    return (tokens_grad, gates_grad.T, gate_grad, up_grad, down_grad)


def solution(mesh):
    in_specs = (
        P("ep", None),
        P("ep", None),
        P("ep", None),
        P("ep", None),
        P("ep", None, "tp"),
        P("ep", None, "tp"),
        P("ep", "tp", None),
    )
    out_specs = (
        P("ep", None),
        P("ep", None),
        P("ep", None, "tp"),
        P("ep", None, "tp"),
        P("ep", "tp", None),
    )
    return jax.shard_map(step, mesh=mesh, in_specs=in_specs, out_specs=out_specs, check_vma=False)
```

time: 198 us -> 218 us (1.10)
  starting transfers between devices: 47.9 us -> 60.9 us
  waiting for transfers between devices: 103 us -> 112 us
  Pallas kernels: 33.9 us -> 38 us
  other arithmetic: 3.99 us -> 0 us
    ppermute x4 -> x6, waiting for transfers between devices: 34.4 us -> 16.4 us  [the longest x2 16.4 us: swap(): lax.ppermute(landed, 'tp', left)]
    all_to_all x1 -> x2, waiting for transfers between devices: 0.01 us -> 18 us  [to_experts(): landed = lax.all_to_all(send, 'ep', split_axis=0, concat_axis=0, tiled=True)]
    all_to_all x1 -> x2, starting transfers between devices: 12.2 us -> 17.9 us  [to_experts(): landed = lax.all_to_all(send, 'ep', split_axis=0, concat_axis=0, tiled=True)]
    ppermute x1, waiting for transfers between devices: 0.01 us -> 5.58 us  [step(): lax.ppermute(to_left, 'tp', left)]
    ppermute x1, waiting for transfers between devices: 0.01 us -> 5.3 us  [step(): lax.ppermute(to_across, 'tp', across)]
    pallas_call x6 -> x7, Pallas kernels: 33.9 us -> 38 us  [call(): pl.pallas_call(kernel, out_shape=out_shape, in_specs=[scalar] * scalars +...]
    ppermute x1, starting transfers between devices: 4.41 us -> 0.98 us  [step(): lax.ppermute(summed, 'tp', left)]
    ppermute x1, waiting for transfers between devices: 2.69 us -> 0.01 us  [step(): lax.ppermute(summed, 'tp', across)]
  transfers between devices with their start and end apart: 22 -> 25, of which waited for: 9 -> 10; matrix products, arithmetic and copies ran while one was open for 1% -> 0% of each run, Pallas kernels for 4% -> 11%
where the time goes in v3:
time: 218 us; the launch traced here: 217 us
  waiting for transfers between devices  112 us (51%)
  starting transfers between devices  60.9 us (28%)
  Pallas kernels  38 us (17%)
  local copies, waits for them, and re-layouts  5.6 us (3%)
    pallas_call x7, Pallas kernels, call(): pl.pallas_call(kernel, out_shape=out_shape, in_specs=[scalar] * scalars +...  38 us
    ppermute x1, waiting for transfers between devices, step(): lax.ppermute(to_right, 'tp', right)  23.8 us
    ppermute x3, waiting for transfers between devices, step(): kept.append(lax.ppermute(mine, 'tp', left))  20.4 us
    all_to_all x2, waiting for transfers between devices, to_experts(): landed = lax.all_to_all(send, 'ep', split_axis=0, concat_axis=0, tiled=True)  18 us
    all_to_all x2, starting transfers between devices, to_experts(): landed = lax.all_to_all(send, 'ep', split_axis=0, concat_axis=0, tiled=True)  17.9 us
    ppermute x2, waiting for transfers between devices, swap(): lax.ppermute(landed, 'tp', left)  16.4 us
    ppermute x1, waiting for transfers between devices, step(): down_even = lax.ppermute(downs[2][0:1], 'tp', left)  12.8 us
    all_to_all x1, starting transfers between devices, step(): back = lax.all_to_all(back, 'ep', split_axis=0, concat_axis=0, tiled=True)  10.5 us
  transfers between devices with their start and end apart: 25, of which 10 were waited for; matrix products, arithmetic and copies ran while one was open for 0% of the time, Pallas kernels for 11%

profile of v3, /device:TPU:14, one launch (start us, length us, event | category | flops | bytes accessed | tf_op | source)
XLA Modules:
  0.0 217.2 jit_solution(10552070114965567634)
XLA Ops:
  0.6 3.9 %shard_map.110 = bf16[1536,256]{1,0:T(8,128)(2,1)} custom-call(s32[1]{0:T(128)} %bitcast.refs_0_, s32[2,256]{1,0:T(2,128)} %bitcast.22, bf16[256,1024]{1,0:T(8,128)(2,1)} %refs_2_.2), custom_call_target="tpu_custom_call" | custom-call | tf_op jit(solution)/shard_map/pallas_call | solution.py:319
  4.5 12.1 %all-to-all-start = ((bf16[64,24,256]{2,1,0:T(8,128)(2,1)}), bf16[64,24,256]{2,1,0:T(8,128)(2,1)S(1)}, u32[]{:S(2)}, u32[]{:S(2)}) async-start(bf16[64,24,256]{2,1,0:T(8,128)(2,1)} %bitcast.20), calls=%async_computation | async-start | bytes 1572864 | tf_op jit(solution)/shard_map/all_to_all | solution.py:344
  16.6 5.1 %shard_map.111 = (bf16[1536,256]{1,0:T(8,128)(2,1)}, bf16[2,384,256]{2,1,0:T(8,128)(2,1)}) custom-call(s32[1]{0:T(128)} %bitcast.refs_0_, s32[2,256]{1,0:T(2,128)} %bitcast.23, f32[2,256]{1,0:T(2,128)} %bitcast.24, bf16[256,1024]{1,0:T(8,128)(2,1)} %refs_3_.1), custom_call_target="tpu_custom_call" | custom-call | tf_op jit(solution)/shard_map/pallas_call | solution.py:319
  21.8 18.0 %all-to-all-done = bf16[64,24,256]{2,1,0:T(8,128)(2,1)S(1)} async-done(((bf16[64,24,256]{2,1,0:T(8,128)(2,1)}), bf16[64,24,256]{2,1,0:T(8,128)(2,1)S(1)}, u32[]{:S(2)}, u32[]{:S(2)}) %all-to-all-start) | async-done | bytes 786464 | tf_op jit(solution)/shard_map/all_to_all | solution.py:344
  40.7 5.8 %all-to-all-start.1 = ((bf16[64,24,256]{2,1,0:T(8,128)(2,1)}), bf16[64,24,256]{2,1,0:T(8,128)(2,1)S(1)}, u32[]{:S(2)}, u32[]{:S(2)}) async-start(bf16[64,24,256]{2,1,0:T(8,128)(2,1)} %bitcast.21), calls=%async_computation.1 | async-start | bytes 1572864 | tf_op jit(solution)/shard_map/all_to_all | solution.py:344
  47.3 2.4 %collective-permute-start.3 = (bf16[2,1024,128]{2,1,0:T(8,128)(2,1)S(1)}, bf16[2,1024,128]{2,1,0:T(8,128)(2,1)S(1)}, u32[]{:S(2)}, u32[]{:S(2)}) collective-permute-start(bf16[2,1024,128]{2,1,0:T(8,128)(2,1)S(1)} %copy-done.6), channel_id=1, source_target_pairs={{0,1},{1,2},{2,3},{3,0},{4,5},{5,6},{6,7},{7,4},{8,9},{9,10},{10,1... | collective-permute-start | bytes 1572872 | tf_op jit(solution)/shard_map/ppermute | solution.py:332
  49.8 3.2 %collective-permute-start.6 = (bf16[2,128,1024]{2,1,0:T(8,128)(2,1)S(1)}, bf16[2,128,1024]{2,1,0:T(8,128)(2,1)S(1)}, u32[]{:S(2)}, u32[]{:S(2)}) collective-permute-start(bf16[2,128,1024]{2,1,0:T(8,128)(2,1)S(1)} %copy-done.7), channel_id=1, source_target_pairs={{0,1},{1,2},{2,3},{3,0},{4,5},{5,6},{6,7},{7,4},{8,9},{9,10},{10,1... | collective-permute-start | bytes 1572872 | tf_op jit(solution)/shard_map/ppermute | solution.py:332
  53.0 9.5 %collective-permute-done.1.refs_4_ = bf16[2,1024,128]{2,1,0:T(8,128)(2,1)S(1)} collective-permute-done((bf16[2,1024,128]{2,1,0:T(8,128)(2,1)S(1)}, bf16[2,1024,128]{2,1,0:T(8,128)(2,1)S(1)}, u32[]{:S(2)}, u32[]{:S(2)}) %collective-permute-start.1) | collective-permute-done | bytes 524320 | tf_op jit(solution)/shard_map/ppermute | solution.py:333
  62.8 10.9 %collective-permute-done.7.refs_12_ = bf16[2,128,1024]{2,1,0:T(8,128)(2,1)S(1)} collective-permute-done((bf16[2,128,1024]{2,1,0:T(8,128)(2,1)S(1)}, bf16[2,128,1024]{2,1,0:T(8,128)(2,1)S(1)}, u32[]{:S(2)}, u32[]{:S(2)}) %collective-permute-start.7) | collective-permute-done | bytes 524320 | tf_op jit(solution)/shard_map/ppermute | solution.py:333
  75.9 8.7 %collective-permute-done.refs_3_ = bf16[2,1024,128]{2,1,0:T(8,128)(2,1)S(1)} collective-permute-done((bf16[2,1024,128]{2,1,0:T(8,128)(2,1)S(1)}, bf16[2,1024,128]{2,1,0:T(8,128)(2,1)S(1)}, u32[]{:S(2)}, u32[]{:S(2)}) %collective-permute-start) | collective-permute-done | bytes 524320 | tf_op jit(solution)/shard_map/ppermute | solution.py:332
  84.6 3.6 %collective-permute-start.9 = (bf16[1,128,1024]{2,1,0:T(8,128)(2,1)S(1)}, bf16[1,128,1024]{2,1,0:T(8,128)(2,1)S(1)}, u32[]{:S(2)}, u32[]{:S(2)}) collective-permute-start(bf16[1,128,1024]{2,1,0:T(8,128)(2,1)S(1)} %slice.9), channel_id=1, source_target_pairs={{0,1},{1,2},{2,3},{3,0},{4,5},{5,6},{6,7},{7,4},{8,9},{9,10},{10,1... | collective-permute-start | bytes 786440 | tf_op jit(solution)/shard_map/ppermute | solution.py:337
  88.2 12.8 %collective-permute-done.8.refs_13_ = bf16[1,128,1024]{2,1,0:T(8,128)(2,1)S(1)} collective-permute-done((bf16[1,128,1024]{2,1,0:T(8,128)(2,1)S(1)}, bf16[1,128,1024]{2,1,0:T(8,128)(2,1)S(1)}, u32[]{:S(2)}, u32[]{:S(2)}) %collective-permute-start.8) | collective-permute-done | bytes 262176 | tf_op jit(solution)/shard_map/ppermute | solution.py:336
  102.8 8.8 %shard_map.112 = s16[3584,128]{1,0:T(8,128)(2,1)} custom-call(bf16[1536,256]{1,0:T(8,128)(2,1)} %bitcast.10, bf16[1536,256]{1,0:T(8,128)(2,1)} %bitcast.14, bf16[2,1024,128]{2,1,0:T(8,128)(2,1)} %refs_8_.1, bf16[2,1024,128]{2,1,0:T(8,128)(2,1)} %copy-done.13, bf16[2,1024,128]{2,1,0:T(8,128)(2,1)} %copy-done.11, bf16[2,1024,128]{2,1,0:T(8,128)(2,1)} %copy-done.15, ...), custom_call_target="tpu_custom_call" | custom-call | tf_op jit(solution)/shard_map/pallas_call | solution.py:319
  111.6 10.5 %all-to-all-start.2 = ((s16[64,56,128]{2,1,0:T(8,128)(2,1)}), s16[64,56,128]{2,1,0:T(8,128)(2,1)S(1)}, u32[]{:S(2)}, u32[]{:S(2)}) async-start(s16[64,56,128]{2,1,0:T(8,128)(2,1)} %bitcast.18), calls=%async_computation.2 | async-start | bytes 1835008 | tf_op jit(solution)/shard_map/all_to_all | solution.py:377
  122.2 3.2 %collective-permute-start.19 = (bf16[1536,256]{1,0:T(8,128)(2,1)S(1)}, bf16[1536,256]{1,0:T(8,128)(2,1)}, u32[]{:S(2)}, u32[]{:S(2)}) collective-permute-start(bf16[1536,256]{1,0:T(8,128)(2,1)S(1)} %bitcast.16), channel_id=1, source_target_pairs={{0,1},{1,2},{2,3},{3,0},{4,5},{5,6},{6,7},{7,4},{8,9},{9,10},{10,1... | collective-permute-start | bytes 2359304 | tf_op jit(solution)/shard_map/ppermute | solution.py:348
  127.4 16.4 %collective-permute-done.17.refs_2_ = bf16[1536,256]{1,0:T(8,128)(2,1)S(1)} collective-permute-done((bf16[1536,256]{1,0:T(8,128)(2,1)S(1)}, bf16[1536,256]{1,0:T(8,128)(2,1)S(1)}, u32[]{:S(2)}, u32[]{:S(2)}) %collective-permute-start.17) | collective-permute-done | bytes 786464 | tf_op jit(solution)/shard_map/ppermute | solution.py:348
  143.8 3.3 %collective-permute-start.21 = (bf16[1536,256]{1,0:T(8,128)(2,1)}, bf16[1536,256]{1,0:T(8,128)(2,1)}, u32[]{:S(2)}, u32[]{:S(2)}) collective-permute-start(bf16[1536,256]{1,0:T(8,128)(2,1)} %collective-permute-done.19.refs_5_), channel_id=1, source_target_pairs={{0,1},{1,2},{2,3},{3,0},{4,5},{5,6},{6,7},{7,4},{8,9},{9,10},{10,1... | collective-permute-start | bytes 2359304 | tf_op jit(solution)/shard_map/ppermute | solution.py:367
  148.9 4.0 %shard_map.113 = (s16[72,1152]{1,0:T(8,128)(2,1)}, s16[72,1152]{1,0:T(8,128)(2,1)}, s16[72,1152]{1,0:T(8,128)(2,1)}, s16[72,1152]{1,0:T(8,128)(2,1)}) custom-call(s32[1]{0:T(128)} %bitcast.refs_0_, s16[3584,128]{1,0:T(8,128)(2,1)} %bitcast.19, bf16[2,384,256]{2,1,0:T(8,128)(2,1)} %get-tuple-element.17.refs_2_), custom_call_target="tpu_custom_call" | custom-call | tf_op jit(solution)/shard_map/pallas_call | solution.py:319
  152.9 2.9 %collective-permute-start.10 = (s16[72,1152]{1,0:T(8,128)(2,1)}, s16[72,1152]{1,0:T(8,128)(2,1)S(1)}, u32[]{:S(2)}, u32[]{:S(2)}) collective-permute-start(s16[72,1152]{1,0:T(8,128)(2,1)} %get-tuple-element.19), channel_id=1, source_target_pairs={{0,1},{1,2},{2,3},{3,0},{4,5},{5,6},{6,7},{7,4},{8,9},{9,10},{10,1... | collective-permute-start | bytes 497672 | tf_op jit(solution)/shard_map/ppermute | solution.py:390
  155.8 23.8 %collective-permute-done.10.from_left = s16[72,1152]{1,0:T(8,128)(2,1)S(1)} collective-permute-done((s16[72,1152]{1,0:T(8,128)(2,1)}, s16[72,1152]{1,0:T(8,128)(2,1)S(1)}, u32[]{:S(2)}, u32[]{:S(2)}) %collective-permute-start.10) | collective-permute-done | bytes 165920 | tf_op jit(solution)/shard_map/ppermute | solution.py:390
  181.3 5.6 %collective-permute-done.11.from_right = s16[72,1152]{1,0:T(8,128)(2,1)S(1)} collective-permute-done((s16[72,1152]{1,0:T(8,128)(2,1)}, s16[72,1152]{1,0:T(8,128)(2,1)S(1)}, u32[]{:S(2)}, u32[]{:S(2)}) %collective-permute-start.11) | collective-permute-done | bytes 165920 | tf_op jit(solution)/shard_map/ppermute | solution.py:391
  188.6 5.3 %collective-permute-done.12.from_opposite = s16[72,1152]{1,0:T(8,128)(2,1)S(1)} collective-permute-done((s16[72,1152]{1,0:T(8,128)(2,1)}, s16[72,1152]{1,0:T(8,128)(2,1)S(1)}, u32[]{:S(2)}, u32[]{:S(2)}) %collective-permute-start.12) | collective-permute-done | bytes 165920 | tf_op jit(solution)/shard_map/ppermute | solution.py:392
  199.4 2.3 %collective-permute-start.13 = (bf16[64,1024]{1,0:T(8,128)(2,1)}, bf16[64,1024]{1,0:T(8,128)(2,1)S(1)}, u32[]{:S(2)}, u32[]{:S(2)}) collective-permute-start(bf16[64,1024]{1,0:T(8,128)(2,1)} %get-tuple-element.22.refs_1_), channel_id=1, source_target_pairs={{0,1},{1,2},{2,3},{3,0},{4,5},{5,6},{6,7},{7,4},{8,9},{9,10},{10,1... | collective-permute-start | bytes 393224 | tf_op jit(solution)/shard_map/ppermute | solution.py:400
  201.7 12.2 %shard_map.116 = (f32[2,1024,128]{2,1,0:T(8,128)}, f32[2,1024,128]{2,1,0:T(8,128)}, f32[2,128,1024]{2,1,0:T(8,128)}) custom-call(bf16[1536,256]{1,0:T(8,128)(2,1)} %bitcast.11, bf16[1536,256]{1,0:T(8,128)(2,1)} %collective-permute-done.16.refs_1_, bf16[1536,256]{1,0:T(8,128)(2,1)} %copy-done.10, bf16[1536,256]{1,0:T(8,128)(2,1)} %collective-permute-done.18.refs_3_, ...), custom_call_target="tpu_custom_call" | custom-call | tf_op jit(solution)/shard_map/pallas_call | solution.py:319
  (83 shorter events, 22.1 us)
Async XLA Ops:
  4.5 35.3 %all-to-all-start = ((bf16[64,24,256]{2,1,0:T(8,128)(2,1)}), bf16[64,24,256]{2,1,0:T(8,128)(2,1)S(1)}, u32[]{:S(2)}, u32[]{:S(2)}) async-start(bf16[64,24,256]{2,1,0:T(8,128)(2,1)} %bitcast.20), calls=%async_computation | async-start | bytes 1572864 | tf_op jit(solution)/shard_map/all_to_all | solution.py:344
  40.7 61.2 %all-to-all-start.1 = ((bf16[64,24,256]{2,1,0:T(8,128)(2,1)}), bf16[64,24,256]{2,1,0:T(8,128)(2,1)S(1)}, u32[]{:S(2)}, u32[]{:S(2)}) async-start(bf16[64,24,256]{2,1,0:T(8,128)(2,1)} %bitcast.21), calls=%async_computation.1 | async-start | bytes 1572864 | tf_op jit(solution)/shard_map/all_to_all | solution.py:344
  46.4 16.1 %collective-permute-start.1 = (bf16[2,1024,128]{2,1,0:T(8,128)(2,1)S(1)}, bf16[2,1024,128]{2,1,0:T(8,128)(2,1)S(1)}, u32[]{:S(2)}, u32[]{:S(2)}) collective-permute-start(bf16[2,1024,128]{2,1,0:T(8,128)(2,1)S(1)} %copy-done.5), channel_id=1, source_target_pairs={{0,3},{1,0},{2,1},{3,2},{4,7},{5,4},{6,5},{7,6},{8,11},{9,8},{10,9... | collective-permute-start | bytes 1572872 | tf_op jit(solution)/shard_map/ppermute | solution.py:333
  47.3 15.2 %collective-permute-start.3 = (bf16[2,1024,128]{2,1,0:T(8,128)(2,1)S(1)}, bf16[2,1024,128]{2,1,0:T(8,128)(2,1)S(1)}, u32[]{:S(2)}, u32[]{:S(2)}) collective-permute-start(bf16[2,1024,128]{2,1,0:T(8,128)(2,1)S(1)} %copy-done.6), channel_id=1, source_target_pairs={{0,1},{1,2},{2,3},{3,0},{4,5},{5,6},{6,7},{7,4},{8,9},{9,10},{10,1... | collective-permute-start | bytes 1572872 | tf_op jit(solution)/shard_map/ppermute | solution.py:332
  49.8 24.0 %collective-permute-start.7 = (bf16[2,128,1024]{2,1,0:T(8,128)(2,1)S(1)}, bf16[2,128,1024]{2,1,0:T(8,128)(2,1)S(1)}, u32[]{:S(2)}, u32[]{:S(2)}) collective-permute-start(bf16[2,128,1024]{2,1,0:T(8,128)(2,1)S(1)} %copy-done.7), channel_id=1, source_target_pairs={{0,3},{1,0},{2,1},{3,2},{4,7},{5,4},{6,5},{7,6},{8,11},{9,8},{10,9... | collective-permute-start | bytes 1572872 | tf_op jit(solution)/shard_map/ppermute | solution.py:333
  49.8 24.0 %collective-permute-start.6 = (bf16[2,128,1024]{2,1,0:T(8,128)(2,1)S(1)}, bf16[2,128,1024]{2,1,0:T(8,128)(2,1)S(1)}, u32[]{:S(2)}, u32[]{:S(2)}) collective-permute-start(bf16[2,128,1024]{2,1,0:T(8,128)(2,1)S(1)} %copy-done.7), channel_id=1, source_target_pairs={{0,1},{1,2},{2,3},{3,0},{4,5},{5,6},{6,7},{7,4},{8,9},{9,10},{10,1... | collective-permute-start | bytes 1572872 | tf_op jit(solution)/shard_map/ppermute | solution.py:332
  53.0 31.6 %collective-permute-start = (bf16[2,1024,128]{2,1,0:T(8,128)(2,1)S(1)}, bf16[2,1024,128]{2,1,0:T(8,128)(2,1)S(1)}, u32[]{:S(2)}, u32[]{:S(2)}) collective-permute-start(bf16[2,1024,128]{2,1,0:T(8,128)(2,1)S(1)} %copy-done.5), channel_id=1, source_target_pairs={{0,1},{1,2},{2,3},{3,0},{4,5},{5,6},{6,7},{7,4},{8,9},{9,10},{10,1... | collective-permute-start | bytes 1572872 | tf_op jit(solution)/shard_map/ppermute | solution.py:332
  62.5 25.7 %collective-permute-start.4 = (bf16[2,1024,128]{2,1,0:T(8,128)(2,1)S(1)}, bf16[2,1024,128]{2,1,0:T(8,128)(2,1)S(1)}, u32[]{:S(2)}, u32[]{:S(2)}) collective-permute-start(bf16[2,1024,128]{2,1,0:T(8,128)(2,1)S(1)} %copy-done.6), channel_id=1, source_target_pairs={{0,3},{1,0},{2,1},{3,2},{4,7},{5,4},{6,5},{7,6},{8,11},{9,8},{10,9... | collective-permute-start | bytes 1572872 | tf_op jit(solution)/shard_map/ppermute | solution.py:333
  62.5 38.5 %collective-permute-start.2 = (bf16[2,1024,128]{2,1,0:T(8,128)(2,1)S(1)}, bf16[2,1024,128]{2,1,0:T(8,128)(2,1)S(1)}, u32[]{:S(2)}, u32[]{:S(2)}) collective-permute-start(bf16[2,1024,128]{2,1,0:T(8,128)(2,1)S(1)} %collective-permute-done.1.refs_4_), channel_id=1, source_target_pairs={{0,3},{1,0},{2,1},{3,2},{4,7},{5,4},{6,5},{7,6},{8,11},{9,8},{10,9... | collective-permute-start | bytes 1572872 | tf_op jit(solution)/shard_map/ppermute | solution.py:334
  73.8 28.1 %collective-permute-start.5 = (bf16[2,1024,128]{2,1,0:T(8,128)(2,1)S(1)}, bf16[2,1024,128]{2,1,0:T(8,128)(2,1)}, u32[]{:S(2)}, u32[]{:S(2)}) collective-permute-start(bf16[2,1024,128]{2,1,0:T(8,128)(2,1)S(1)} %collective-permute-done.3.refs_7_), channel_id=1, source_target_pairs={{0,1},{1,2},{2,3},{3,0},{4,5},{5,6},{6,7},{7,4},{8,9},{9,10},{10,1... | collective-permute-start | bytes 1572872 | tf_op jit(solution)/shard_map/ppermute | solution.py:335
  73.8 27.2 %collective-permute-start.8 = (bf16[1,128,1024]{2,1,0:T(8,128)(2,1)S(1)}, bf16[1,128,1024]{2,1,0:T(8,128)(2,1)S(1)}, u32[]{:S(2)}, u32[]{:S(2)}) collective-permute-start(bf16[1,128,1024]{2,1,0:T(8,128)(2,1)S(1)} %slice.8), channel_id=1, source_target_pairs={{0,3},{1,0},{2,1},{3,2},{4,7},{5,4},{6,5},{7,6},{8,11},{9,8},{10,9... | collective-permute-start | bytes 786440 | tf_op jit(solution)/shard_map/ppermute | solution.py:336
  84.6 16.4 %collective-permute-start.9 = (bf16[1,128,1024]{2,1,0:T(8,128)(2,1)S(1)}, bf16[1,128,1024]{2,1,0:T(8,128)(2,1)S(1)}, u32[]{:S(2)}, u32[]{:S(2)}) collective-permute-start(bf16[1,128,1024]{2,1,0:T(8,128)(2,1)S(1)} %slice.9), channel_id=1, source_target_pairs={{0,1},{1,2},{2,3},{3,0},{4,5},{5,6},{6,7},{7,4},{8,9},{9,10},{10,1... | collective-permute-start | bytes 786440 | tf_op jit(solution)/shard_map/ppermute | solution.py:337
  111.6 36.4 %all-to-all-start.2 = ((s16[64,56,128]{2,1,0:T(8,128)(2,1)}), s16[64,56,128]{2,1,0:T(8,128)(2,1)S(1)}, u32[]{:S(2)}, u32[]{:S(2)}) async-start(s16[64,56,128]{2,1,0:T(8,128)(2,1)} %bitcast.18), calls=%async_computation.2 | async-start | bytes 1835008 | tf_op jit(solution)/shard_map/all_to_all | solution.py:377
  122.1 21.7 %collective-permute-start.17 = (bf16[1536,256]{1,0:T(8,128)(2,1)S(1)}, bf16[1536,256]{1,0:T(8,128)(2,1)S(1)}, u32[]{:S(2)}, u32[]{:S(2)}) collective-permute-start(bf16[1536,256]{1,0:T(8,128)(2,1)S(1)} %bitcast.12), channel_id=1, source_target_pairs={{0,3},{1,0},{2,1},{3,2},{4,7},{5,4},{6,5},{7,6},{8,11},{9,8},{10,9... | collective-permute-start | bytes 2359304 | tf_op jit(solution)/shard_map/ppermute | solution.py:348
  122.2 21.6 %collective-permute-start.19 = (bf16[1536,256]{1,0:T(8,128)(2,1)S(1)}, bf16[1536,256]{1,0:T(8,128)(2,1)}, u32[]{:S(2)}, u32[]{:S(2)}) collective-permute-start(bf16[1536,256]{1,0:T(8,128)(2,1)S(1)} %bitcast.16), channel_id=1, source_target_pairs={{0,1},{1,2},{2,3},{3,0},{4,5},{5,6},{6,7},{7,4},{8,9},{9,10},{10,1... | collective-permute-start | bytes 2359304 | tf_op jit(solution)/shard_map/ppermute | solution.py:348
  125.4 73.0 %collective-permute-start.16 = (bf16[1536,256]{1,0:T(8,128)(2,1)S(1)}, bf16[1536,256]{1,0:T(8,128)(2,1)}, u32[]{:S(2)}, u32[]{:S(2)}) collective-permute-start(bf16[1536,256]{1,0:T(8,128)(2,1)S(1)} %bitcast.13), channel_id=1, source_target_pairs={{0,1},{1,2},{2,3},{3,0},{4,5},{5,6},{6,7},{7,4},{8,9},{9,10},{10,1... | collective-permute-start | bytes 2359304 | tf_op jit(solution)/shard_map/ppermute | solution.py:348
  127.1 72.3 %collective-permute-start.20 = (bf16[1536,256]{1,0:T(8,128)(2,1)S(1)}, bf16[1536,256]{1,0:T(8,128)(2,1)}, u32[]{:S(2)}, u32[]{:S(2)}) collective-permute-start(bf16[1536,256]{1,0:T(8,128)(2,1)S(1)} %bitcast.17), channel_id=1, source_target_pairs={{0,3},{1,0},{2,1},{3,2},{4,7},{5,4},{6,5},{7,6},{8,11},{9,8},{10,9... | collective-permute-start | bytes 2359304 | tf_op jit(solution)/shard_map/ppermute | solution.py:348
  143.8 57.9 %collective-permute-start.18 = (bf16[1536,256]{1,0:T(8,128)(2,1)S(1)}, bf16[1536,256]{1,0:T(8,128)(2,1)}, u32[]{:S(2)}, u32[]{:S(2)}) collective-permute-start(bf16[1536,256]{1,0:T(8,128)(2,1)S(1)} %collective-permute-done.17.refs_2_), channel_id=1, source_target_pairs={{0,3},{1,0},{2,1},{3,2},{4,7},{5,4},{6,5},{7,6},{8,11},{9,8},{10,9... | collective-permute-start | bytes 2359304 | tf_op jit(solution)/shard_map/ppermute | solution.py:366
  143.8 57.9 %collective-permute-start.21 = (bf16[1536,256]{1,0:T(8,128)(2,1)}, bf16[1536,256]{1,0:T(8,128)(2,1)}, u32[]{:S(2)}, u32[]{:S(2)}) collective-permute-start(bf16[1536,256]{1,0:T(8,128)(2,1)} %collective-permute-done.19.refs_5_), channel_id=1, source_target_pairs={{0,1},{1,2},{2,3},{3,0},{4,5},{5,6},{6,7},{7,4},{8,9},{9,10},{10,1... | collective-permute-start | bytes 2359304 | tf_op jit(solution)/shard_map/ppermute | solution.py:367
  152.9 26.7 %collective-permute-start.10 = (s16[72,1152]{1,0:T(8,128)(2,1)}, s16[72,1152]{1,0:T(8,128)(2,1)S(1)}, u32[]{:S(2)}, u32[]{:S(2)}) collective-permute-start(s16[72,1152]{1,0:T(8,128)(2,1)} %get-tuple-element.19), channel_id=1, source_target_pairs={{0,1},{1,2},{2,3},{3,0},{4,5},{5,6},{6,7},{7,4},{8,9},{9,10},{10,1... | collective-permute-start | bytes 497672 | tf_op jit(solution)/shard_map/ppermute | solution.py:390
  179.6 7.3 %collective-permute-start.11 = (s16[72,1152]{1,0:T(8,128)(2,1)}, s16[72,1152]{1,0:T(8,128)(2,1)S(1)}, u32[]{:S(2)}, u32[]{:S(2)}) collective-permute-start(s16[72,1152]{1,0:T(8,128)(2,1)} %get-tuple-element.20), channel_id=1, source_target_pairs={{0,3},{1,0},{2,1},{3,2},{4,7},{5,4},{6,5},{7,6},{8,11},{9,8},{10,9... | collective-permute-start | bytes 497672 | tf_op jit(solution)/shard_map/ppermute | solution.py:391
  196.7 17.3 %collective-permute-start.15 = (bf16[64,1024]{1,0:T(8,128)(2,1)}, bf16[64,1024]{1,0:T(8,128)(2,1)S(1)}, u32[]{:S(2)}, u32[]{:S(2)}) collective-permute-start(bf16[64,1024]{1,0:T(8,128)(2,1)} %get-tuple-element.22.refs_1_), channel_id=1, source_target_pairs={{0,2},{1,3},{2,0},{3,1},{4,6},{5,7},{6,4},{7,5},{8,10},{9,11},{10,... | collective-permute-start | bytes 393224 | tf_op jit(solution)/shard_map/ppermute | solution.py:402
  198.4 15.5 %collective-permute-start.14 = (bf16[64,1024]{1,0:T(8,128)(2,1)}, bf16[64,1024]{1,0:T(8,128)(2,1)S(1)}, u32[]{:S(2)}, u32[]{:S(2)}) collective-permute-start(bf16[64,1024]{1,0:T(8,128)(2,1)} %get-tuple-element.22.refs_1_), channel_id=1, source_target_pairs={{0,3},{1,0},{2,1},{3,2},{4,7},{5,4},{6,5},{7,6},{8,11},{9,8},{10,9... | collective-permute-start | bytes 393224 | tf_op jit(solution)/shard_map/ppermute | solution.py:401
  199.4 14.5 %collective-permute-start.13 = (bf16[64,1024]{1,0:T(8,128)(2,1)}, bf16[64,1024]{1,0:T(8,128)(2,1)S(1)}, u32[]{:S(2)}, u32[]{:S(2)}) collective-permute-start(bf16[64,1024]{1,0:T(8,128)(2,1)} %get-tuple-element.22.refs_1_), channel_id=1, source_target_pairs={{0,1},{1,2},{2,3},{3,0},{4,5},{5,6},{6,7},{7,4},{8,9},{9,10},{10,1... | collective-permute-start | bytes 393224 | tf_op jit(solution)/shard_map/ppermute | solution.py:400
  (25 other events, 277.1 us)

commit v4 on v2

--- a/solution.py
+++ b/solution.py
@@ -7,14 +7,16 @@
 
 
 F32 = jnp.float32
-F16 = jnp.float16
+I16 = jnp.int16
 BF16 = jnp.bfloat16
 I32 = jnp.int32
 LANES = 128
 SUBLANES = 8
 BLOCK = 16
 HALVES = 2
-SPREAD = 16384.0
+TOP_CODE = 32766.0
+STEPS = 8192.0
+FINE = 32768.0
 VMEM = pltpu.VMEM
 SMEM = pltpu.SMEM
 NN = ((1,), (0,))
@@ -40,6 +42,36 @@
 
 def exponent(value):
     return jnp.floor(jnp.log(jnp.maximum(value, 1e-30)) * 1.4426950408889634)
+
+
+def row_scale(power, steps):
+    return steps * jnp.exp2(power) * (1.0 / (STEPS * TOP_CODE))
+
+
+def code_rows(value):
+    largest = jnp.maximum(jnp.max(jnp.abs(value), axis=1, keepdims=True), 1e-30)
+    power = exponent(largest)
+    steps = jnp.ceil(largest * jnp.exp2(-power) * STEPS)
+    return jnp.round(value * (1.0 / row_scale(power, steps))), power, steps
+
+
+def code_values(value):
+    power = exponent(jnp.abs(value))
+    value = value * jnp.exp2(-power) * STEPS
+    coarse = jnp.round(value)
+    return power, coarse, jnp.round((value - coarse) * FINE)
+
+
+def decode_values(power, coarse, fine):
+    return (coarse + fine * (1.0 / FINE)) * (jnp.exp2(power) * (1.0 / STEPS))
+
+
+def to_code(value):
+    return value.astype(I32).astype(I16)
+
+
+def from_code(value):
+    return value.astype(I32).astype(F32)
 
 
 def dispatch_kernel(
@@ -74,11 +106,13 @@
     for h in range(HALVES):
         columns = slice(h * half, (h + 1) * half)
         base = h * 2 * group
-        hits = [jnp.where(row == r + base, 1.0, 0.0) for r in token_rows]
-        part = mm((hits[0] + hits[1]).astype(BF16), tokens[:, columns])
-        hits = [jnp.where(row == r + (base + group), 1.0, 0.0) for r in token_rows]
-        slot_weight = jnp.sum(hits[0] * weights[0:1, :] + hits[1] * weights[1:2, :], axis=1, keepdims=True)
-        part = part + slot_weight * mm((hits[0] + hits[1]).astype(BF16), cotangent[:, columns])
+        hits = [row == r + base for r in token_rows]
+        part = mm(jnp.where(hits[0] | hits[1], 1.0, 0.0).astype(BF16), tokens[:, columns])
+        hits = [row == r + (base + group) for r in token_rows]
+        weighted = jnp.where(hits[0], weights[0:1, :], jnp.where(hits[1], weights[1:2, :], 0.0))
+        slot_weight = jnp.sum(weighted, axis=1, keepdims=True)
+        chosen_rows = jnp.where(hits[0] | hits[1], 1.0, 0.0).astype(BF16)
+        part = part + slot_weight * mm(chosen_rows, cotangent[:, columns])
         total = part if total is None else total + part
     rows_out[...] = total.astype(BF16)
 
@@ -119,14 +153,14 @@
 
 def input_kernel(local_experts, quarter, landed, *refs):
     gates, ups, downs = refs[0:4], refs[4:8], refs[8:11]
-    down_even, down_odd, out, rows, scaled = refs[11:]
+    down_even, down_odd, out, rows, scaled, coded = refs[11:]
     own, _ = rows.shape
     slots = local_experts * quarter
     devices = own // quarter
     stride = (slots + 1) * SUBLANES
     for i in range(slots, SUBLANES):
         at = slots * SUBLANES + i
-        out[pl.ds(at, devices, stride=stride), :] = jnp.zeros((devices, LANES), F32)
+        coded[pl.ds(at, devices, stride=stride), :] = jnp.zeros((devices, LANES), F32)
     for expert in range(local_experts):
         land(landed, expert, local_experts, quarter, rows, scaled, 0)
         gate = jnp.concatenate([g[expert] for g in gates], axis=1)
@@ -137,18 +171,11 @@
         hidden, gate_grad, up_grad = hidden_terms(mm(rows[...], gate), mm(rows[...], up), hidden_grad)
         product = jnp.sum(hidden_grad * hidden, axis=1, keepdims=True)
         grad = mm(gate_grad, gate, NT) + mm(up_grad, up, NT)
-        power = exponent(jnp.max(jnp.abs(grad), axis=1, keepdims=True))
-        grad = grad * (SPREAD * jnp.exp2(-power))
-        product_power = exponent(jnp.abs(product))
-        product = product * jnp.exp2(-product_power)
-        high = product.astype(BF16).astype(F32)
-        low = (product - high) * 256.0
+        grad, power, steps = code_rows(grad)
         lane = iota((own, LANES), 1)
-        tail = jnp.where(
-            lane == 0,
-            power,
-            jnp.where(lane == 1, product_power, jnp.where(lane == 2, high, low)),
-        )
+        tail = jnp.zeros((own, LANES), F32)
+        for at, column in enumerate((power, steps) + code_values(product)):
+            tail = jnp.where(lane == at, column, tail)
         for block in range(devices // BLOCK):
             for q in range(quarter):
                 at = (block * quarter + q) * BLOCK
@@ -156,9 +183,10 @@
                 slot = expert * quarter + q
                 for i in range(SUBLANES):
                     piece = grad[at : at + BLOCK, i * LANES : (i + 1) * LANES]
-                    out[pl.ds(to + slot * SUBLANES + i, BLOCK, stride=stride), :] = piece
+                    coded[pl.ds(to + slot * SUBLANES + i, BLOCK, stride=stride), :] = piece
                 to += slots * SUBLANES + slot
-                out[pl.ds(to, BLOCK, stride=stride), :] = tail[at : at + BLOCK]
+                coded[pl.ds(to, BLOCK, stride=stride), :] = tail[at : at + BLOCK]
+    out[...] = to_code(coded[...])
 
 
 def weight_kernel(local_experts, quarter, *refs):
@@ -166,7 +194,8 @@
     rows, scaled = refs[11:]
     chunk = HALVES * 2 * local_experts * quarter
     hidden_width = gate.shape[2]
-    for expert in range(local_experts):
+
+    def one(expert, carry):
         offset = 0
         for source in sources:
             land(source, expert, local_experts, quarter, rows, scaled, offset)
@@ -180,22 +209,27 @@
         gate_out[expert] = grads[:, :hidden_width]
         up_out[expert] = grads[:, hidden_width:]
         down_out[expert] = mm(hidden.astype(BF16), scaled[...], TN)
+        return carry
+
+    lax.fori_loop(0, local_experts, one, 0)
 
 
 def member_rows(member, distance, members, count):
     return pl.ds(pl.multiple_of(lax.rem(member + distance, members) * count, count), count)
 
 
-def combine_kernel(members, devices, member, back, pick, *refs):
-    outs, total = refs[:-1], refs[-1]
-    token_count, width = total.shape
+def combine_kernel(members, devices, member, coded, pick, *refs):
+    outs, total, back = refs[:-2], refs[-2], refs[-1]
+    back[...] = from_code(coded[...])
+    token_count, tail_width = total.shape
+    width = tail_width - LANES
     slots = pick.shape[1] // devices
     stride = (slots + 1) * SUBLANES
     tails = [
         back[pl.ds(slots * SUBLANES + slot, devices, stride=stride), :] for slot in range(slots)
     ]
     tail = jnp.concatenate(tails, axis=0)
-    scale = jnp.exp2(tail[:, 0:1]) * (1.0 / SPREAD)
+    scale = row_scale(tail[:, 0:1], tail[:, 1:2])
     columns = []
     for i in range(SUBLANES):
         pieces = [
@@ -204,31 +238,56 @@
         columns.append(jnp.concatenate(pieces, axis=0))
     grad = jnp.concatenate(columns, axis=1) * scale
     both = pick[0] + pick[1]
-    total[...] = sum(mm(both, part, TN) for part in split3(grad))
-    product = (tail[:, 2:3] + tail[:, 3:4] * (1.0 / 256.0)) * jnp.exp2(tail[:, 1:2])
+    grad, power, steps = code_rows(sum(mm(both, part, TN) for part in split3(grad)))
+    total[:, 0:width] = grad
+    lane = iota((token_count, LANES), 1)
+    total[:, width:] = jnp.where(lane == 0, power, jnp.where(lane == 1, steps, 0.0))
+    product = decode_values(tail[:, 2:3], tail[:, 3:4], tail[:, 4:5])
     sums = [jnp.sum(pick[k].astype(F32) * product, axis=0, keepdims=True) for k in range(2)]
-    spare = jnp.zeros((1, width - 2 * token_count), F32)
-    line = jnp.broadcast_to(jnp.concatenate(sums + [spare], axis=1), (SUBLANES, width))
+    power, coarse, fine = code_values(jnp.concatenate(sums, axis=1))
+    spare = jnp.zeros((1, tail_width - 4 * token_count), F32)
+    first = jnp.concatenate([power, coarse, spare], axis=1)
+    second = jnp.concatenate([fine, jnp.zeros_like(fine), spare], axis=1)
+    line = iota((SUBLANES, tail_width), 0)
+    lines = to_code(jnp.where(line == 0, first, jnp.where(line == 1, second, 0.0)))
     count = token_count // members
     for out, distance in zip(outs, (0, 1, 3, 2)):
-        out[0:count, :] = total[member_rows(member[0], distance, members, count), :]
-        out[count : count + SUBLANES, :] = line
+        out[0:count, :] = to_code(total[member_rows(member[0], distance, members, count), :])
+        out[count : count + SUBLANES, :] = lines
 
 
 def sum_kernel(own, from_left, from_right, from_opposite, weights, grad_out, gates_out):
-    count = grad_out.shape[0]
+    count, width = grad_out.shape
     token_count = weights.shape[1]
-    total = (own[...] + from_opposite[...]) + (from_left[...] + from_right[...])
-    grad_out[...] = total[0:count].astype(BF16)
+    parts = [from_code(part[...]) for part in (own, from_left, from_right, from_opposite)]
+    grads = [
+        part[:count, :width] * row_scale(part[:count, width : width + 1], part[:count, width + 1 : width + 2])
+        for part in parts
+    ]
+    grad_out[...] = ((grads[0] + grads[3]) + (grads[1] + grads[2])).astype(BF16)
+    values = 2 * token_count
+    products = [
+        decode_values(
+            part[count : count + 1, 0:values],
+            part[count : count + 1, values : 2 * values],
+            part[count + 1 : count + 2, 0:values],
+        )
+        for part in parts
+    ]
+    product = (products[0] + products[3]) + (products[1] + products[2])
     for k in range(2):
-        product = total[count : count + 1, k * token_count : (k + 1) * token_count]
-        gates_out[k : k + 1, :] = product / weights[k : k + 1, :]
-
-
-def place_kernel(members, member, own, from_left, from_right, from_opposite, out):
+        gates_out[k : k + 1, :] = product[:, k * token_count : (k + 1) * token_count] / weights[k : k + 1, :]
+
+
+def place_kernel(members, member, own, from_left, from_right, from_opposite, out, sems):
     count = own.shape[0]
+    copies = []
     for piece, distance in ((own, 0), (from_left, 3), (from_right, 1), (from_opposite, 2)):
-        out[member_rows(member[0], distance, members, count), :] = piece[...]
+        to = out.at[member_rows(member[0], distance, members, count), :]
+        copies.append(pltpu.make_async_copy(piece, to, sems.at[distance]))
+        copies[-1].start()
+    for copy in copies:
+        copy.wait()
 
 
 def step(tokens, cotangent, routing, gate_weights, gate_proj, up_proj, down_proj):
@@ -293,21 +352,22 @@
     back_rows = (local_experts * quarter + 1) * SUBLANES
     back = call(
         lambda *refs: input_kernel(local_experts, quarter, *refs),
-        shape((groups * back_rows, LANES), F32),
+        shape((groups * back_rows, LANES), I16),
         (landed, *gates, *ups, *downs, down_even, down_odd),
-        scratch=[VMEM((own, model_width), BF16)] * 2,
-    )
-    back = back.astype(F16).reshape(groups, back_rows, LANES)
+        scratch=[VMEM((own, model_width), BF16)] * 2 + [VMEM((groups * back_rows, LANES), F32)],
+    )
+    back = back.reshape(groups, back_rows, LANES)
     back = lax.all_to_all(back, "ep", split_axis=0, concat_axis=0, tiled=True)
-    back = back.astype(F32).reshape(groups * back_rows, LANES)
+    back = back.reshape(groups * back_rows, LANES)
     count = token_count // members
-    part = shape((count + SUBLANES, model_width), F32)
+    tail_width = model_width + LANES
+    part = shape((count + SUBLANES, tail_width), I16)
     mine, to_right, to_left, to_across = call(
         lambda *refs: combine_kernel(members, groups, *refs),
         (part,) * 4,
         (member, back, pick),
         scalars=1,
-        scratch=[VMEM((token_count, model_width), F32)],
+        scratch=[VMEM((token_count, tail_width), F32), VMEM((groups * back_rows, LANES), F32)],
     )
     pieces = (
         lax.ppermute(to_right, "tp", right),
@@ -324,12 +384,15 @@
         lax.ppermute(summed, "tp", left),
         lax.ppermute(summed, "tp", across),
     )
-    tokens_grad = call(
+    anywhere = pl.BlockSpec(memory_space=pl.ANY)
+    tokens_grad = pl.pallas_call(
         lambda *refs: place_kernel(members, *refs),
-        shape((token_count, model_width), BF16),
-        (member, summed, *pieces),
-        scalars=1,
-    )
+        out_shape=shape((token_count, model_width), BF16),
+        in_specs=[scalar] + [anywhere] * 4,
+        out_specs=anywhere,
+        scratch_shapes=[pltpu.SemaphoreType.DMA((4,))],
+        name="place",
+    )(member, summed, *pieces)
 
     gate_grad, up_grad, down_grad = call(
         lambda *refs: weight_kernel(local_experts, quarter, *refs),

time: 198 us -> 181 us (0.914)
  waiting for transfers between devices: 103 us -> 76.1 us
  Pallas kernels: 33.9 us -> 49.6 us
  other arithmetic: 3.99 us -> 0 us
    ppermute x1, waiting for transfers between devices: 34.4 us -> 13 us  [step(): from_right = lax.ppermute(landed, 'tp', left)]
    pallas_call x0 -> x1, Pallas kernels: none -> 17 us  [step(): pl.pallas_call(lambda *refs: place_kernel(members, *refs), out_shape=shap...]
    ppermute x1, waiting for transfers between devices: 21.3 us -> 7.12 us  [step(): lax.ppermute(to_right, 'tp', right)]
    all_to_all x1, waiting for transfers between devices: 0.01 us -> 7.17 us  [step(): back = lax.all_to_all(back, 'ep', split_axis=0, concat_axis=0, tiled=True)]
    ppermute x1, starting transfers between devices: 3.22 us -> 0.01 us  [step(): from_left = lax.ppermute(landed, 'tp', right)]
    convert_element_type x1 -> x0, other arithmetic: 2.54 us -> none  [step(): back = back.astype(F16).reshape(groups, back_rows, LANES)]
    unnamed x46 -> x34, local copies, waits for them, and re-layouts: 5.95 us -> 4.01 us
    pallas_call x6 -> x5, Pallas kernels: 33.9 us -> 32.5 us  [call(): pl.pallas_call(kernel, out_shape=out_shape, in_specs=[scalar] * scalars +...]
  transfers between devices with their start and end apart: 22 -> 22, of which waited for: 9 -> 12; matrix products, arithmetic and copies ran while one was open for 1% -> 1% of each run, Pallas kernels for 4% -> 18%
where the time goes in v4:
time: 181 us; the launch traced here: 179 us
  waiting for transfers between devices  76.1 us (42%)
  Pallas kernels  49.6 us (27%)
  starting transfers between devices  46.1 us (25%)
  local copies, waits for them, and re-layouts  6.41 us (4%)
    pallas_call x5, Pallas kernels, call(): pl.pallas_call(kernel, out_shape=out_shape, in_specs=[scalar] * scalars +...  32.5 us
    ppermute x3, waiting for transfers between devices, step(): kept.append(lax.ppermute(mine, 'tp', left))  20.6 us
    pallas_call x1, Pallas kernels, step(): pl.pallas_call(lambda *refs: place_kernel(members, *refs), out_shape=shap...  17 us
    ppermute x1, waiting for transfers between devices, step(): down_even = lax.ppermute(downs[2][0:1], 'tp', left)  13.3 us
    ppermute x1, waiting for transfers between devices, step(): from_right = lax.ppermute(landed, 'tp', left)  13 us
    all_to_all x1, starting transfers between devices, step(): lax.all_to_all(send.reshape(groups, chunk, half), 'ep', split_axis=0, con...  12.2 us
    all_to_all x1, starting transfers between devices, step(): back = lax.all_to_all(back, 'ep', split_axis=0, concat_axis=0, tiled=True)  10.3 us
    ppermute x3, waiting for transfers between devices, step(): kept.append(lax.ppermute(mine, 'tp', right))  8.69 us
  transfers between devices with their start and end apart: 22, of which 12 were waited for; matrix products, arithmetic and copies ran while one was open for 1% of the time, Pallas kernels for 18%

profile of v4, /device:TPU:14, one launch (start us, length us, event | category | flops | bytes accessed | tf_op | source)
XLA Modules:
  0.0 179.0 jit_solution(12624588821621247261)
XLA Ops:
  0.6 5.5 %shard_map.110 = (bf16[1536,512]{1,0:T(8,128)(2,1)}, bf16[2,384,256]{2,1,0:T(8,128)(2,1)}) custom-call(s32[1]{0:T(128)} %bitcast.refs_0_, s32[2,256]{1,0:T(2,128)} %bitcast.17, f32[2,256]{1,0:T(2,128)} %bitcast.15, bf16[256,1024]{1,0:T(8,128)(2,1)} %refs_3_.1, bf16[256,1024]{1,0:T(8,128)(2,1)} %refs_4_.1), custom_call_target="tpu_custom_call" | custom-call | tf_op jit(solution)/shard_map/pallas_call | solution.py:316
  6.1 12.2 %all-to-all-start = ((bf16[64,24,512]{2,1,0:T(8,128)(2,1)}), bf16[64,24,512]{2,1,0:T(8,128)(2,1)S(1)}, u32[]{:S(2)}, u32[]{:S(2)}) async-start(bf16[64,24,512]{2,1,0:T(8,128)(2,1)} %bitcast.14), calls=%async_computation | async-start | bytes 3145728 | tf_op jit(solution)/shard_map/all_to_all | solution.py:342
  19.3 2.4 %collective-permute-start.3 = (bf16[2,1024,128]{2,1,0:T(8,128)(2,1)S(1)}, bf16[2,1024,128]{2,1,0:T(8,128)(2,1)}, u32[]{:S(2)}, u32[]{:S(2)}) collective-permute-start(bf16[2,1024,128]{2,1,0:T(8,128)(2,1)S(1)} %copy-done.3), channel_id=1, source_target_pairs={{0,1},{1,2},{2,3},{3,0},{4,5},{5,6},{6,7},{7,4},{8,9},{9,10},{10,1... | collective-permute-start | bytes 1572872 | tf_op jit(solution)/shard_map/ppermute | solution.py:329
  21.7 3.2 %collective-permute-start.6 = (bf16[2,128,1024]{2,1,0:T(8,128)(2,1)S(1)}, bf16[2,128,1024]{2,1,0:T(8,128)(2,1)S(1)}, u32[]{:S(2)}, u32[]{:S(2)}) collective-permute-start(bf16[2,128,1024]{2,1,0:T(8,128)(2,1)S(1)} %copy-done.4), channel_id=1, source_target_pairs={{0,1},{1,2},{2,3},{3,0},{4,5},{5,6},{6,7},{7,4},{8,9},{9,10},{10,1... | collective-permute-start | bytes 1572872 | tf_op jit(solution)/shard_map/ppermute | solution.py:329
  25.0 9.6 %collective-permute-done.1.refs_3_ = bf16[2,1024,128]{2,1,0:T(8,128)(2,1)} collective-permute-done((bf16[2,1024,128]{2,1,0:T(8,128)(2,1)S(1)}, bf16[2,1024,128]{2,1,0:T(8,128)(2,1)}, u32[]{:S(2)}, u32[]{:S(2)}) %collective-permute-start.1) | collective-permute-done | bytes 524320 | tf_op jit(solution)/shard_map/ppermute | solution.py:330
  34.8 11.0 %collective-permute-done.7.refs_11_ = bf16[2,128,1024]{2,1,0:T(8,128)(2,1)S(1)} collective-permute-done((bf16[2,128,1024]{2,1,0:T(8,128)(2,1)S(1)}, bf16[2,128,1024]{2,1,0:T(8,128)(2,1)S(1)}, u32[]{:S(2)}, u32[]{:S(2)}) %collective-permute-start.7) | collective-permute-done | bytes 524320 | tf_op jit(solution)/shard_map/ppermute | solution.py:330
  45.8 2.1 %collective-permute-start.8 = (bf16[1,128,1024]{2,1,0:T(8,128)(2,1)S(1)}, bf16[1,128,1024]{2,1,0:T(8,128)(2,1)S(1)}, u32[]{:S(2)}, u32[]{:S(2)}) collective-permute-start(bf16[1,128,1024]{2,1,0:T(8,128)(2,1)S(1)} %slice.16), channel_id=1, source_target_pairs={{0,3},{1,0},{2,1},{3,2},{4,7},{5,4},{6,5},{7,6},{8,11},{9,8},{10,9... | collective-permute-start | bytes 786440 | tf_op jit(solution)/shard_map/ppermute | solution.py:333
  47.9 8.7 %collective-permute-done.refs_2_ = bf16[2,1024,128]{2,1,0:T(8,128)(2,1)S(1)} collective-permute-done((bf16[2,1024,128]{2,1,0:T(8,128)(2,1)S(1)}, bf16[2,1024,128]{2,1,0:T(8,128)(2,1)S(1)}, u32[]{:S(2)}, u32[]{:S(2)}) %collective-permute-start) | collective-permute-done | bytes 524320 | tf_op jit(solution)/shard_map/ppermute | solution.py:329
  56.6 3.6 %collective-permute-start.9 = (bf16[1,128,1024]{2,1,0:T(8,128)(2,1)S(1)}, bf16[1,128,1024]{2,1,0:T(8,128)(2,1)S(1)}, u32[]{:S(2)}, u32[]{:S(2)}) collective-permute-start(bf16[1,128,1024]{2,1,0:T(8,128)(2,1)S(1)} %slice.17), channel_id=1, source_target_pairs={{0,1},{1,2},{2,3},{3,0},{4,5},{5,6},{6,7},{7,4},{8,9},{9,10},{10,1... | collective-permute-start | bytes 786440 | tf_op jit(solution)/shard_map/ppermute | solution.py:334
  60.5 13.3 %collective-permute-done.8.refs_12_ = bf16[1,128,1024]{2,1,0:T(8,128)(2,1)S(1)} collective-permute-done((bf16[1,128,1024]{2,1,0:T(8,128)(2,1)S(1)}, bf16[1,128,1024]{2,1,0:T(8,128)(2,1)S(1)}, u32[]{:S(2)}, u32[]{:S(2)}) %collective-permute-start.8) | collective-permute-done | bytes 262176 | tf_op jit(solution)/shard_map/ppermute | solution.py:333
  74.7 8.8 %shard_map.111 = s16[3584,128]{1,0:T(8,128)(2,1)} custom-call(bf16[1536,512]{1,0:T(8,128)(2,1)} %bitcast.10, bf16[2,1024,128]{2,1,0:T(8,128)(2,1)} %refs_5_.3, bf16[2,1024,128]{2,1,0:T(8,128)(2,1)} %copy-done.8, bf16[2,1024,128]{2,1,0:T(8,128)(2,1)} %collective-permute-done.1.refs_3_, bf16[2,1024,128]{2,1,0:T(8,128)(2,1)} %collective-permute-done.2.refs_4_, ...), custom_call_target="tpu_custom_call" | custom-call | tf_op jit(solution)/shard_map/pallas_call | solution.py:316
  83.5 10.3 %all-to-all-start.1 = ((s16[64,56,128]{2,1,0:T(8,128)(2,1)}), s16[64,56,128]{2,1,0:T(8,128)(2,1)S(1)}, u32[]{:S(2)}, u32[]{:S(2)}) async-start(s16[64,56,128]{2,1,0:T(8,128)(2,1)} %bitcast.12), calls=%async_computation.1 | async-start | bytes 1835008 | tf_op jit(solution)/shard_map/all_to_all | solution.py:360
  93.8 13.0 %collective-permute-done.17.refs_2_ = bf16[1536,512]{1,0:T(8,128)(2,1)} collective-permute-done((bf16[1536,512]{1,0:T(8,128)(2,1)S(1)}, bf16[1536,512]{1,0:T(8,128)(2,1)}, u32[]{:S(2)}, u32[]{:S(2)}) %collective-permute-start.17) | collective-permute-done | bytes 1572896 | tf_op jit(solution)/shard_map/ppermute | solution.py:347
  109.8 2.7 %collective-permute-start.19 = (bf16[768,512]{1,0:T(8,128)(2,1)S(1)}, bf16[768,512]{1,0:T(8,128)(2,1)S(1)}, u32[]{:S(2)}, u32[]{:S(2)}) collective-permute-start(bf16[768,512]{1,0:T(8,128)(2,1)S(1)} %slice.19), channel_id=1, source_target_pairs={{0,1},{1,2},{2,3},{3,0},{4,5},{5,6},{6,7},{7,4},{8,9},{9,10},{10,1... | collective-permute-start | bytes 2359304 | tf_op jit(solution)/shard_map/ppermute | solution.py:350
  112.6 7.2 %all-to-all-done.1 = s16[64,56,128]{2,1,0:T(8,128)(2,1)S(1)} async-done(((s16[64,56,128]{2,1,0:T(8,128)(2,1)}), s16[64,56,128]{2,1,0:T(8,128)(2,1)S(1)}, u32[]{:S(2)}, u32[]{:S(2)}) %all-to-all-start.1) | async-done | bytes 917536 | tf_op jit(solution)/shard_map/all_to_all | solution.py:360
  120.6 4.0 %shard_map.112 = (s16[72,1152]{1,0:T(8,128)(2,1)}, s16[72,1152]{1,0:T(8,128)(2,1)}, s16[72,1152]{1,0:T(8,128)(2,1)}, s16[72,1152]{1,0:T(8,128)(2,1)}) custom-call(s32[1]{0:T(128)} %bitcast.refs_0_, s16[3584,128]{1,0:T(8,128)(2,1)} %bitcast.13, bf16[2,384,256]{2,1,0:T(8,128)(2,1)} %get-tuple-element.17.refs_2_), custom_call_target="tpu_custom_call" | custom-call | tf_op jit(solution)/shard_map/pallas_call | solution.py:316
  124.6 2.0 %collective-permute-start.10 = (s16[72,1152]{1,0:T(8,128)(2,1)}, s16[72,1152]{1,0:T(8,128)(2,1)S(1)}, u32[]{:S(2)}, u32[]{:S(2)}) collective-permute-start(s16[72,1152]{1,0:T(8,128)(2,1)} %get-tuple-element.19), channel_id=1, source_target_pairs={{0,1},{1,2},{2,3},{3,0},{4,5},{5,6},{6,7},{7,4},{8,9},{9,10},{10,1... | collective-permute-start | bytes 497672 | tf_op jit(solution)/shard_map/ppermute | solution.py:373
  126.6 2.0 %collective-permute-start.12 = (s16[72,1152]{1,0:T(8,128)(2,1)}, s16[72,1152]{1,0:T(8,128)(2,1)S(1)}, u32[]{:S(2)}, u32[]{:S(2)}) collective-permute-start(s16[72,1152]{1,0:T(8,128)(2,1)} %get-tuple-element.21), channel_id=1, source_target_pairs={{0,2},{1,3},{2,0},{3,1},{4,6},{5,7},{6,4},{7,5},{8,10},{9,11},{10,... | collective-permute-start | bytes 497672 | tf_op jit(solution)/shard_map/ppermute | solution.py:375
  128.6 7.1 %collective-permute-done.10.from_left = s16[72,1152]{1,0:T(8,128)(2,1)S(1)} collective-permute-done((s16[72,1152]{1,0:T(8,128)(2,1)}, s16[72,1152]{1,0:T(8,128)(2,1)S(1)}, u32[]{:S(2)}, u32[]{:S(2)}) %collective-permute-start.10) | collective-permute-done | bytes 165920 | tf_op jit(solution)/shard_map/ppermute | solution.py:373
  137.3 2.0 %shard_map.113 = (bf16[64,1024]{1,0:T(8,128)(2,1)}, f32[2,256]{1,0:T(2,128)}) custom-call(s16[72,1152]{1,0:T(8,128)(2,1)} %get-tuple-element.18.own, s16[72,1152]{1,0:T(8,128)(2,1)} %copy-done.11, s16[72,1152]{1,0:T(8,128)(2,1)} %copy-done.12, s16[72,1152]{1,0:T(8,128)(2,1)} %copy-done.13, f32[2,256]{1,0:T(2,128)} %bitcast.16), custom_call_target="tpu_custom_call" | custom-call | tf_op jit(solution)/shard_map/pallas_call | solution.py:316
  140.2 2.8 %collective-permute-start.14 = (bf16[64,1024]{1,0:T(8,128)(2,1)}, bf16[64,1024]{1,0:T(8,128)(2,1)S(1)}, u32[]{:S(2)}, u32[]{:S(2)}) collective-permute-start(bf16[64,1024]{1,0:T(8,128)(2,1)} %get-tuple-element.22.refs_1_), channel_id=1, source_target_pairs={{0,3},{1,0},{2,1},{3,2},{4,7},{5,4},{6,5},{7,6},{8,11},{9,8},{10,9... | collective-permute-start | bytes 393224 | tf_op jit(solution)/shard_map/ppermute | solution.py:384
  143.4 2.7 %collective-permute-done.15.refs_4_ = bf16[64,1024]{1,0:T(8,128)(2,1)S(1)} collective-permute-done((bf16[64,1024]{1,0:T(8,128)(2,1)}, bf16[64,1024]{1,0:T(8,128)(2,1)S(1)}, u32[]{:S(2)}, u32[]{:S(2)}) %collective-permute-start.15) | collective-permute-done | bytes 131104 | tf_op jit(solution)/shard_map/ppermute | solution.py:385
  148.8 17.0 %place.1 = bf16[256,1024]{1,0:T(8,128)(2,1)} custom-call(s32[1]{0:T(128)} %bitcast.refs_0_, bf16[64,1024]{1,0:T(8,128)(2,1)} %get-tuple-element.22.refs_1_, bf16[64,1024]{1,0:T(8,128)(2,1)} %copy-done.16, bf16[64,1024]{1,0:T(8,128)(2,1)} %copy-done.15, bf16[64,1024]{1,0:T(8,128)(2,1)} %copy-done.14), custom_call_target="tpu_custom_call" | custom-call | tf_op jit(solution)/shard_map/place/pallas_call | solution.py:388
  166.8 12.2 %shard_map.114 = (f32[2,1024,128]{2,1,0:T(8,128)}, f32[2,1024,128]{2,1,0:T(8,128)}, f32[2,128,1024]{2,1,0:T(8,128)}) custom-call(bf16[1536,512]{1,0:T(8,128)(2,1)} %bitcast.11, bf16[1536,512]{1,0:T(8,128)(2,1)} %collective-permute-done.16.refs_1_, bf16[1536,512]{1,0:T(8,128)(2,1)} %collective-permute-done.17.refs_2_, ...), custom_call_target="tpu_custom_call" | custom-call | tf_op jit(solution)/shard_map/pallas_call | solution.py:316
  (64 shorter events, 12.6 us)
Async XLA Ops:
  6.1 15.6 %copy-start.4 = (bf16[2,128,1024]{2,1,0:T(8,128)(2,1)S(1)}, bf16[2,128,1024]{2,1,0:T(8,128)(2,1)}, u32[]{:S(2)}) copy-start(bf16[2,128,1024]{2,1,0:T(8,128)(2,1)} %refs_7_.1) | copy-start | bytes 1572868
  6.1 54.1 %all-to-all-start = ((bf16[64,24,512]{2,1,0:T(8,128)(2,1)}), bf16[64,24,512]{2,1,0:T(8,128)(2,1)S(1)}, u32[]{:S(2)}, u32[]{:S(2)}) async-start(bf16[64,24,512]{2,1,0:T(8,128)(2,1)} %bitcast.14), calls=%async_computation | async-start | bytes 3145728 | tf_op jit(solution)/shard_map/all_to_all | solution.py:342
  18.4 16.2 %collective-permute-start.1 = (bf16[2,1024,128]{2,1,0:T(8,128)(2,1)S(1)}, bf16[2,1024,128]{2,1,0:T(8,128)(2,1)}, u32[]{:S(2)}, u32[]{:S(2)}) collective-permute-start(bf16[2,1024,128]{2,1,0:T(8,128)(2,1)S(1)} %copy-done.2), channel_id=1, source_target_pairs={{0,3},{1,0},{2,1},{3,2},{4,7},{5,4},{6,5},{7,6},{8,11},{9,8},{10,9... | collective-permute-start | bytes 1572872 | tf_op jit(solution)/shard_map/ppermute | solution.py:330
  19.3 15.3 %collective-permute-start.3 = (bf16[2,1024,128]{2,1,0:T(8,128)(2,1)S(1)}, bf16[2,1024,128]{2,1,0:T(8,128)(2,1)}, u32[]{:S(2)}, u32[]{:S(2)}) collective-permute-start(bf16[2,1024,128]{2,1,0:T(8,128)(2,1)S(1)} %copy-done.3), channel_id=1, source_target_pairs={{0,1},{1,2},{2,3},{3,0},{4,5},{5,6},{6,7},{7,4},{8,9},{9,10},{10,1... | collective-permute-start | bytes 1572872 | tf_op jit(solution)/shard_map/ppermute | solution.py:329
  21.7 24.0 %collective-permute-start.7 = (bf16[2,128,1024]{2,1,0:T(8,128)(2,1)S(1)}, bf16[2,128,1024]{2,1,0:T(8,128)(2,1)S(1)}, u32[]{:S(2)}, u32[]{:S(2)}) collective-permute-start(bf16[2,128,1024]{2,1,0:T(8,128)(2,1)S(1)} %copy-done.4), channel_id=1, source_target_pairs={{0,3},{1,0},{2,1},{3,2},{4,7},{5,4},{6,5},{7,6},{8,11},{9,8},{10,9... | collective-permute-start | bytes 1572872 | tf_op jit(solution)/shard_map/ppermute | solution.py:330
  21.7 24.0 %collective-permute-start.6 = (bf16[2,128,1024]{2,1,0:T(8,128)(2,1)S(1)}, bf16[2,128,1024]{2,1,0:T(8,128)(2,1)S(1)}, u32[]{:S(2)}, u32[]{:S(2)}) collective-permute-start(bf16[2,128,1024]{2,1,0:T(8,128)(2,1)S(1)} %copy-done.4), channel_id=1, source_target_pairs={{0,1},{1,2},{2,3},{3,0},{4,5},{5,6},{6,7},{7,4},{8,9},{9,10},{10,1... | collective-permute-start | bytes 1572872 | tf_op jit(solution)/shard_map/ppermute | solution.py:329
  25.0 31.6 %collective-permute-start = (bf16[2,1024,128]{2,1,0:T(8,128)(2,1)S(1)}, bf16[2,1024,128]{2,1,0:T(8,128)(2,1)S(1)}, u32[]{:S(2)}, u32[]{:S(2)}) collective-permute-start(bf16[2,1024,128]{2,1,0:T(8,128)(2,1)S(1)} %copy-done.2), channel_id=1, source_target_pairs={{0,1},{1,2},{2,3},{3,0},{4,5},{5,6},{6,7},{7,4},{8,9},{9,10},{10,1... | collective-permute-start | bytes 1572872 | tf_op jit(solution)/shard_map/ppermute | solution.py:329
  34.6 25.6 %collective-permute-start.4 = (bf16[2,1024,128]{2,1,0:T(8,128)(2,1)S(1)}, bf16[2,1024,128]{2,1,0:T(8,128)(2,1)}, u32[]{:S(2)}, u32[]{:S(2)}) collective-permute-start(bf16[2,1024,128]{2,1,0:T(8,128)(2,1)S(1)} %copy-done.3), channel_id=1, source_target_pairs={{0,3},{1,0},{2,1},{3,2},{4,7},{5,4},{6,5},{7,6},{8,11},{9,8},{10,9... | collective-permute-start | bytes 1572872 | tf_op jit(solution)/shard_map/ppermute | solution.py:330
  34.6 39.2 %collective-permute-start.2 = (bf16[2,1024,128]{2,1,0:T(8,128)(2,1)}, bf16[2,1024,128]{2,1,0:T(8,128)(2,1)}, u32[]{:S(2)}, u32[]{:S(2)}) collective-permute-start(bf16[2,1024,128]{2,1,0:T(8,128)(2,1)} %collective-permute-done.1.refs_3_), channel_id=1, source_target_pairs={{0,3},{1,0},{2,1},{3,2},{4,7},{5,4},{6,5},{7,6},{8,11},{9,8},{10,9... | collective-permute-start | bytes 1572872 | tf_op jit(solution)/shard_map/ppermute | solution.py:331
  45.7 14.5 %copy-start.5 = (bf16[2,128,1024]{2,1,0:T(8,128)(2,1)}, bf16[2,128,1024]{2,1,0:T(8,128)(2,1)S(1)}, u32[]{:S(2)}) copy-start(bf16[2,128,1024]{2,1,0:T(8,128)(2,1)S(1)} %collective-permute-done.7.refs_11_) | copy-start | bytes 1572868
  45.7 28.1 %collective-permute-start.5 = (bf16[2,1024,128]{2,1,0:T(8,128)(2,1)}, bf16[2,1024,128]{2,1,0:T(8,128)(2,1)}, u32[]{:S(2)}, u32[]{:S(2)}) collective-permute-start(bf16[2,1024,128]{2,1,0:T(8,128)(2,1)} %collective-permute-done.3.refs_6_), channel_id=1, source_target_pairs={{0,1},{1,2},{2,3},{3,0},{4,5},{5,6},{6,7},{7,4},{8,9},{9,10},{10,1... | collective-permute-start | bytes 1572872 | tf_op jit(solution)/shard_map/ppermute | solution.py:332
  45.8 28.0 %collective-permute-start.8 = (bf16[1,128,1024]{2,1,0:T(8,128)(2,1)S(1)}, bf16[1,128,1024]{2,1,0:T(8,128)(2,1)S(1)}, u32[]{:S(2)}, u32[]{:S(2)}) collective-permute-start(bf16[1,128,1024]{2,1,0:T(8,128)(2,1)S(1)} %slice.16), channel_id=1, source_target_pairs={{0,3},{1,0},{2,1},{3,2},{4,7},{5,4},{6,5},{7,6},{8,11},{9,8},{10,9... | collective-permute-start | bytes 786440 | tf_op jit(solution)/shard_map/ppermute | solution.py:333
  56.6 17.2 %collective-permute-start.9 = (bf16[1,128,1024]{2,1,0:T(8,128)(2,1)S(1)}, bf16[1,128,1024]{2,1,0:T(8,128)(2,1)S(1)}, u32[]{:S(2)}, u32[]{:S(2)}) collective-permute-start(bf16[1,128,1024]{2,1,0:T(8,128)(2,1)S(1)} %slice.17), channel_id=1, source_target_pairs={{0,1},{1,2},{2,3},{3,0},{4,5},{5,6},{6,7},{7,4},{8,9},{9,10},{10,1... | collective-permute-start | bytes 786440 | tf_op jit(solution)/shard_map/ppermute | solution.py:334
  60.2 46.5 %collective-permute-start.17 = (bf16[1536,512]{1,0:T(8,128)(2,1)S(1)}, bf16[1536,512]{1,0:T(8,128)(2,1)}, u32[]{:S(2)}, u32[]{:S(2)}) collective-permute-start(bf16[1536,512]{1,0:T(8,128)(2,1)S(1)} %bitcast.8), channel_id=1, source_target_pairs={{0,3},{1,0},{2,1},{3,2},{4,7},{5,4},{6,5},{7,6},{8,11},{9,8},{10,9... | collective-permute-start | bytes 4718600 | tf_op jit(solution)/shard_map/ppermute | solution.py:347
  73.8 34.8 %collective-permute-start.16 = (bf16[1536,512]{1,0:T(8,128)(2,1)S(1)}, bf16[1536,512]{1,0:T(8,128)(2,1)}, u32[]{:S(2)}, u32[]{:S(2)}) collective-permute-start(bf16[1536,512]{1,0:T(8,128)(2,1)S(1)} %bitcast.9), channel_id=1, source_target_pairs={{0,1},{1,2},{2,3},{3,0},{4,5},{5,6},{6,7},{7,4},{8,9},{9,10},{10,1... | collective-permute-start | bytes 4718600 | tf_op jit(solution)/shard_map/ppermute | solution.py:346
  83.5 36.2 %all-to-all-start.1 = ((s16[64,56,128]{2,1,0:T(8,128)(2,1)}), s16[64,56,128]{2,1,0:T(8,128)(2,1)S(1)}, u32[]{:S(2)}, u32[]{:S(2)}) async-start(s16[64,56,128]{2,1,0:T(8,128)(2,1)} %bitcast.12), calls=%async_computation.1 | async-start | bytes 1835008 | tf_op jit(solution)/shard_map/all_to_all | solution.py:360
  108.0 57.9 %collective-permute-start.18 = (bf16[768,512]{1,0:T(8,128)(2,1)S(1)}, bf16[768,512]{1,0:T(8,128)(2,1)}, u32[]{:S(2)}, u32[]{:S(2)}) collective-permute-start(bf16[768,512]{1,0:T(8,128)(2,1)S(1)} %slice.18), channel_id=1, source_target_pairs={{0,3},{1,0},{2,1},{3,2},{4,7},{5,4},{6,5},{7,6},{8,11},{9,8},{10,9... | collective-permute-start | bytes 2359304 | tf_op jit(solution)/shard_map/ppermute | solution.py:349
  109.8 56.0 %collective-permute-start.19 = (bf16[768,512]{1,0:T(8,128)(2,1)S(1)}, bf16[768,512]{1,0:T(8,128)(2,1)S(1)}, u32[]{:S(2)}, u32[]{:S(2)}) collective-permute-start(bf16[768,512]{1,0:T(8,128)(2,1)S(1)} %slice.19), channel_id=1, source_target_pairs={{0,1},{1,2},{2,3},{3,0},{4,5},{5,6},{6,7},{7,4},{8,9},{9,10},{10,1... | collective-permute-start | bytes 2359304 | tf_op jit(solution)/shard_map/ppermute | solution.py:350
  124.6 11.1 %collective-permute-start.10 = (s16[72,1152]{1,0:T(8,128)(2,1)}, s16[72,1152]{1,0:T(8,128)(2,1)S(1)}, u32[]{:S(2)}, u32[]{:S(2)}) collective-permute-start(s16[72,1152]{1,0:T(8,128)(2,1)} %get-tuple-element.19), channel_id=1, source_target_pairs={{0,1},{1,2},{2,3},{3,0},{4,5},{5,6},{6,7},{7,4},{8,9},{9,10},{10,1... | collective-permute-start | bytes 497672 | tf_op jit(solution)/shard_map/ppermute | solution.py:373
  126.6 10.0 %collective-permute-start.11 = (s16[72,1152]{1,0:T(8,128)(2,1)}, s16[72,1152]{1,0:T(8,128)(2,1)S(1)}, u32[]{:S(2)}, u32[]{:S(2)}) collective-permute-start(s16[72,1152]{1,0:T(8,128)(2,1)} %get-tuple-element.20), channel_id=1, source_target_pairs={{0,3},{1,0},{2,1},{3,2},{4,7},{5,4},{6,5},{7,6},{8,11},{9,8},{10,9... | collective-permute-start | bytes 497672 | tf_op jit(solution)/shard_map/ppermute | solution.py:374
  126.6 10.0 %collective-permute-start.12 = (s16[72,1152]{1,0:T(8,128)(2,1)}, s16[72,1152]{1,0:T(8,128)(2,1)S(1)}, u32[]{:S(2)}, u32[]{:S(2)}) collective-permute-start(s16[72,1152]{1,0:T(8,128)(2,1)} %get-tuple-element.21), channel_id=1, source_target_pairs={{0,2},{1,3},{2,0},{3,1},{4,6},{5,7},{6,4},{7,5},{8,10},{9,11},{10,... | collective-permute-start | bytes 497672 | tf_op jit(solution)/shard_map/ppermute | solution.py:375
  139.4 6.8 %collective-permute-start.15 = (bf16[64,1024]{1,0:T(8,128)(2,1)}, bf16[64,1024]{1,0:T(8,128)(2,1)S(1)}, u32[]{:S(2)}, u32[]{:S(2)}) collective-permute-start(bf16[64,1024]{1,0:T(8,128)(2,1)} %get-tuple-element.22.refs_1_), channel_id=1, source_target_pairs={{0,2},{1,3},{2,0},{3,1},{4,6},{5,7},{6,4},{7,5},{8,10},{9,11},{10,... | collective-permute-start | bytes 393224 | tf_op jit(solution)/shard_map/ppermute | solution.py:385
  140.2 7.3 %collective-permute-start.14 = (bf16[64,1024]{1,0:T(8,128)(2,1)}, bf16[64,1024]{1,0:T(8,128)(2,1)S(1)}, u32[]{:S(2)}, u32[]{:S(2)}) collective-permute-start(bf16[64,1024]{1,0:T(8,128)(2,1)} %get-tuple-element.22.refs_1_), channel_id=1, source_target_pairs={{0,3},{1,0},{2,1},{3,2},{4,7},{5,4},{6,5},{7,6},{8,11},{9,8},{10,9... | collective-permute-start | bytes 393224 | tf_op jit(solution)/shard_map/ppermute | solution.py:384
  143.0 5.2 %collective-permute-start.13 = (bf16[64,1024]{1,0:T(8,128)(2,1)}, bf16[64,1024]{1,0:T(8,128)(2,1)S(1)}, u32[]{:S(2)}, u32[]{:S(2)}) collective-permute-start(bf16[64,1024]{1,0:T(8,128)(2,1)} %get-tuple-element.22.refs_1_), channel_id=1, source_target_pairs={{0,1},{1,2},{2,3},{3,0},{4,5},{5,6},{6,7},{7,4},{8,9},{9,10},{10,1... | collective-permute-start | bytes 393224 | tf_op jit(solution)/shard_map/ppermute | solution.py:383
  (15 other events, 66.2 us)

commit v5 on v4

--- a/solution.py
+++ b/solution.py
@@ -189,9 +189,11 @@
     out[...] = to_code(coded[...])
 
 
-def weight_kernel(local_experts, quarter, *refs):
-    sources, (gate, up, down), (gate_out, up_out, down_out) = refs[0:5], refs[5:8], refs[8:11]
-    rows, scaled = refs[11:]
+def weight_kernel(local_experts, quarter, source_count, earlier_count, *refs):
+    sources, refs = refs[:source_count], refs[source_count:]
+    (gate, up, down), refs = refs[:3], refs[3:]
+    earlier, refs = refs[:earlier_count], refs[earlier_count:]
+    outs, (rows, scaled) = refs[:3], refs[3:]
     chunk = HALVES * 2 * local_experts * quarter
     hidden_width = gate.shape[2]
 
@@ -206,9 +208,9 @@
             both[:, :hidden_width], both[:, hidden_width:], hidden_grad
         )
         grads = mm(rows[...], jnp.concatenate([gate_grad, up_grad], axis=1), TN)
-        gate_out[expert] = grads[:, :hidden_width]
-        up_out[expert] = grads[:, hidden_width:]
-        down_out[expert] = mm(hidden.astype(BF16), scaled[...], TN)
+        down_grad = mm(hidden.astype(BF16), scaled[...], TN)
+        for at, part in enumerate((grads[:, :hidden_width], grads[:, hidden_width:], down_grad)):
+            outs[at][expert] = earlier[at][expert] + part if earlier else part
         return carry
 
     lax.fori_loop(0, local_experts, one, 0)
@@ -279,15 +281,10 @@
         gates_out[k : k + 1, :] = product[:, k * token_count : (k + 1) * token_count] / weights[k : k + 1, :]
 
 
-def place_kernel(members, member, own, from_left, from_right, from_opposite, out, sems):
+def place_kernel(members, member, own, from_left, from_right, from_opposite, out):
     count = own.shape[0]
-    copies = []
     for piece, distance in ((own, 0), (from_left, 3), (from_right, 1), (from_opposite, 2)):
-        to = out.at[member_rows(member[0], distance, members, count), :]
-        copies.append(pltpu.make_async_copy(piece, to, sems.at[distance]))
-        copies[-1].start()
-    for copy in copies:
-        copy.wait()
+        out[member_rows(member[0], distance, members, count), :] = piece[...]
 
 
 def step(tokens, cotangent, routing, gate_weights, gate_proj, up_proj, down_proj):
@@ -343,11 +340,14 @@
         send.reshape(groups, chunk, half), "ep", split_axis=0, concat_axis=0, tiled=True
     ).reshape(groups * chunk, half)
 
-    from_left = lax.ppermute(landed, "tp", right)
-    from_right = lax.ppermute(landed, "tp", left)
     middle = groups * chunk // 2
-    opposite_low = lax.ppermute(from_right[:middle], "tp", left)
-    opposite_high = lax.ppermute(from_left[middle:], "tp", right)
+    low, high = landed[:middle], landed[middle:]
+    right_low = lax.ppermute(low, "tp", left)
+    left_high = lax.ppermute(high, "tp", right)
+    right_high = lax.ppermute(high, "tp", left)
+    left_low = lax.ppermute(low, "tp", right)
+    opposite_low = lax.ppermute(right_low, "tp", left)
+    opposite_high = lax.ppermute(left_high, "tp", right)
 
     back_rows = (local_experts * quarter + 1) * SUBLANES
     back = call(
@@ -384,26 +384,30 @@
         lax.ppermute(summed, "tp", left),
         lax.ppermute(summed, "tp", across),
     )
-    anywhere = pl.BlockSpec(memory_space=pl.ANY)
-    tokens_grad = pl.pallas_call(
+    tokens_grad = call(
         lambda *refs: place_kernel(members, *refs),
-        out_shape=shape((token_count, model_width), BF16),
-        in_specs=[scalar] + [anywhere] * 4,
-        out_specs=anywhere,
-        scratch_shapes=[pltpu.SemaphoreType.DMA((4,))],
-        name="place",
-    )(member, summed, *pieces)
-
-    gate_grad, up_grad, down_grad = call(
-        lambda *refs: weight_kernel(local_experts, quarter, *refs),
-        (
-            shape((local_experts, model_width, hidden_width), F32),
-            shape((local_experts, model_width, hidden_width), F32),
-            shape((local_experts, hidden_width, model_width), F32),
-        ),
-        (landed, from_left, from_right, opposite_low, opposite_high, gate_proj, up_proj, down_proj),
-        scratch=[VMEM((members * own, model_width), BF16)] * 2,
-    )
+        shape((token_count, model_width), BF16),
+        (member, summed, *pieces),
+        scalars=1,
+    )
+
+    sums = (
+        shape((local_experts, model_width, hidden_width), F32),
+        shape((local_experts, model_width, hidden_width), F32),
+        shape((local_experts, hidden_width, model_width), F32),
+    )
+
+    def weight_sums(sources, earlier):
+        count = sum(source.shape[0] for source in sources) // chunk * quarter
+        return call(
+            lambda *refs: weight_kernel(local_experts, quarter, len(sources), len(earlier), *refs),
+            sums,
+            (*sources, gate_proj, up_proj, down_proj, *earlier),
+            scratch=[VMEM((count, model_width), BF16)] * 2,
+        )
+
+    near = weight_sums((landed, left_low, left_high, right_low, right_high), ())
+    gate_grad, up_grad, down_grad = weight_sums((opposite_low, opposite_high), near)
     return (tokens_grad, gates_grad.T, gate_grad, up_grad, down_grad)
 
 

time: 181 us -> 197 us (1.088)
  waiting for transfers between devices: 76.1 us -> 94.6 us
  Pallas kernels: 49.6 us -> 39.2 us
  starting transfers between devices: 46.1 us -> 54.6 us
    ppermute x1, waiting for transfers between devices: 7.12 us -> 25.2 us  [step(): lax.ppermute(to_right, 'tp', right)]
    pallas_call x1 -> x0, Pallas kernels: 17 us -> none  [step(): pl.pallas_call(lambda *refs: place_kernel(members, *refs), out_shape=shap...]
    all_to_all x1, waiting for transfers between devices: 7.17 us -> 0.01 us  [step(): back = lax.all_to_all(back, 'ep', split_axis=0, concat_axis=0, tiled=True)]
    pallas_call x5 -> x7, Pallas kernels: 32.5 us -> 39.2 us  [call(): pl.pallas_call(kernel, out_shape=out_shape, in_specs=[scalar] * scalars +...]
    ppermute x4 -> x6, starting transfers between devices: 3.08 us -> 8.49 us  [the longest x1 3.23 us: step(): left_high = lax.ppermute(high, 'tp', right)]
    ppermute x1, waiting for transfers between devices: 0.01 us -> 5.25 us  [step(): lax.ppermute(to_across, 'tp', across)]
    ppermute x1, waiting for transfers between devices: 0.89 us -> 5.53 us  [step(): lax.ppermute(to_left, 'tp', left)]
    ppermute x4 -> x6, waiting for transfers between devices: 13.6 us -> 16.6 us  [the longest x1 16.6 us: step(): right_low = lax.ppermute(low, 'tp', left)]
  transfers between devices with their start and end apart: 22 -> 24, of which waited for: 12 -> 8; matrix products, arithmetic and copies ran while one was open for 1% -> 1% of each run, Pallas kernels for 18% -> 12%
where the time goes in v5:
time: 197 us; the launch traced here: 196 us
  waiting for transfers between devices  94.6 us (48%)
  starting transfers between devices  54.6 us (28%)
  Pallas kernels  39.2 us (20%)
  local copies, waits for them, and re-layouts  7.24 us (4%)
    pallas_call x7, Pallas kernels, call(): pl.pallas_call(kernel, out_shape=out_shape, in_specs=[scalar] * scalars +...  39.2 us
    ppermute x1, waiting for transfers between devices, step(): lax.ppermute(to_right, 'tp', right)  25.2 us
    ppermute x3, waiting for transfers between devices, step(): kept.append(lax.ppermute(mine, 'tp', left))  20.6 us
    ppermute x1, waiting for transfers between devices, step(): right_low = lax.ppermute(low, 'tp', left)  16.6 us
    ppermute x1, waiting for transfers between devices, step(): down_even = lax.ppermute(downs[2][0:1], 'tp', left)  12.8 us
    all_to_all x1, starting transfers between devices, step(): lax.all_to_all(send.reshape(groups, chunk, half), 'ep', split_axis=0, con...  12.2 us
    all_to_all x1, starting transfers between devices, step(): back = lax.all_to_all(back, 'ep', split_axis=0, concat_axis=0, tiled=True)  10.4 us
    ppermute x3, waiting for transfers between devices, step(): kept.append(lax.ppermute(mine, 'tp', right))  8.7 us
  transfers between devices with their start and end apart: 24, of which 8 were waited for; matrix products, arithmetic and copies ran while one was open for 1% of the time, Pallas kernels for 12%

profile of v5, /device:TPU:14, one launch (start us, length us, event | category | flops | bytes accessed | tf_op | source)
XLA Modules:
  0.0 196.5 jit_solution(17953321413437871748)
XLA Ops:
  0.6 5.5 %shard_map.110 = (bf16[1536,512]{1,0:T(8,128)(2,1)}, bf16[2,384,256]{2,1,0:T(8,128)(2,1)}) custom-call(s32[1]{0:T(128)} %bitcast.refs_0_, s32[2,256]{1,0:T(2,128)} %bitcast.17, f32[2,256]{1,0:T(2,128)} %bitcast.15, bf16[256,1024]{1,0:T(8,128)(2,1)} %refs_3_.2, bf16[256,1024]{1,0:T(8,128)(2,1)} %refs_4_.2), custom_call_target="tpu_custom_call" | custom-call | tf_op jit(solution)/shard_map/pallas_call | solution.py:313
  6.1 12.2 %all-to-all-start = ((bf16[64,24,512]{2,1,0:T(8,128)(2,1)}), bf16[64,24,512]{2,1,0:T(8,128)(2,1)S(1)}, u32[]{:S(2)}, u32[]{:S(2)}) async-start(bf16[64,24,512]{2,1,0:T(8,128)(2,1)} %bitcast.14), calls=%async_computation | async-start | bytes 3145728 | tf_op jit(solution)/shard_map/all_to_all | solution.py:339
  19.3 2.4 %collective-permute-start.3 = (bf16[2,1024,128]{2,1,0:T(8,128)(2,1)S(1)}, bf16[2,1024,128]{2,1,0:T(8,128)(2,1)S(1)}, u32[]{:S(2)}, u32[]{:S(2)}) collective-permute-start(bf16[2,1024,128]{2,1,0:T(8,128)(2,1)S(1)} %copy-done.3), channel_id=1, source_target_pairs={{0,1},{1,2},{2,3},{3,0},{4,5},{5,6},{6,7},{7,4},{8,9},{9,10},{10,1... | collective-permute-start | bytes 1572872 | tf_op jit(solution)/shard_map/ppermute | solution.py:326
  21.7 3.2 %collective-permute-start.6 = (bf16[2,128,1024]{2,1,0:T(8,128)(2,1)S(1)}, bf16[2,128,1024]{2,1,0:T(8,128)(2,1)S(1)}, u32[]{:S(2)}, u32[]{:S(2)}) collective-permute-start(bf16[2,128,1024]{2,1,0:T(8,128)(2,1)S(1)} %copy-done.4), channel_id=1, source_target_pairs={{0,1},{1,2},{2,3},{3,0},{4,5},{5,6},{6,7},{7,4},{8,9},{9,10},{10,1... | collective-permute-start | bytes 1572872 | tf_op jit(solution)/shard_map/ppermute | solution.py:326
  25.0 9.5 %collective-permute-done.1.refs_3_ = bf16[2,1024,128]{2,1,0:T(8,128)(2,1)S(1)} collective-permute-done((bf16[2,1024,128]{2,1,0:T(8,128)(2,1)S(1)}, bf16[2,1024,128]{2,1,0:T(8,128)(2,1)S(1)}, u32[]{:S(2)}, u32[]{:S(2)}) %collective-permute-start.1) | collective-permute-done | bytes 524320 | tf_op jit(solution)/shard_map/ppermute | solution.py:327
  34.7 11.1 %collective-permute-done.7.refs_11_ = bf16[2,128,1024]{2,1,0:T(8,128)(2,1)S(1)} collective-permute-done((bf16[2,128,1024]{2,1,0:T(8,128)(2,1)S(1)}, bf16[2,128,1024]{2,1,0:T(8,128)(2,1)S(1)}, u32[]{:S(2)}, u32[]{:S(2)}) %collective-permute-start.7) | collective-permute-done | bytes 524320 | tf_op jit(solution)/shard_map/ppermute | solution.py:327
  45.8 2.1 %collective-permute-start.8 = (bf16[1,128,1024]{2,1,0:T(8,128)(2,1)S(1)}, bf16[1,128,1024]{2,1,0:T(8,128)(2,1)S(1)}, u32[]{:S(2)}, u32[]{:S(2)}) collective-permute-start(bf16[1,128,1024]{2,1,0:T(8,128)(2,1)S(1)} %slice.24), channel_id=1, source_target_pairs={{0,3},{1,0},{2,1},{3,2},{4,7},{5,4},{6,5},{7,6},{8,11},{9,8},{10,9... | collective-permute-start | bytes 786440 | tf_op jit(solution)/shard_map/ppermute | solution.py:330
  47.9 8.7 %collective-permute-done.refs_2_ = bf16[2,1024,128]{2,1,0:T(8,128)(2,1)S(1)} collective-permute-done((bf16[2,1024,128]{2,1,0:T(8,128)(2,1)S(1)}, bf16[2,1024,128]{2,1,0:T(8,128)(2,1)S(1)}, u32[]{:S(2)}, u32[]{:S(2)}) %collective-permute-start) | collective-permute-done | bytes 524320 | tf_op jit(solution)/shard_map/ppermute | solution.py:326
  56.6 3.6 %collective-permute-start.9 = (bf16[1,128,1024]{2,1,0:T(8,128)(2,1)S(1)}, bf16[1,128,1024]{2,1,0:T(8,128)(2,1)S(1)}, u32[]{:S(2)}, u32[]{:S(2)}) collective-permute-start(bf16[1,128,1024]{2,1,0:T(8,128)(2,1)S(1)} %slice.25), channel_id=1, source_target_pairs={{0,1},{1,2},{2,3},{3,0},{4,5},{5,6},{6,7},{7,4},{8,9},{9,10},{10,1... | collective-permute-start | bytes 786440 | tf_op jit(solution)/shard_map/ppermute | solution.py:331
  60.2 12.8 %collective-permute-done.8.refs_12_ = bf16[1,128,1024]{2,1,0:T(8,128)(2,1)S(1)} collective-permute-done((bf16[1,128,1024]{2,1,0:T(8,128)(2,1)S(1)}, bf16[1,128,1024]{2,1,0:T(8,128)(2,1)S(1)}, u32[]{:S(2)}, u32[]{:S(2)}) %collective-permute-start.8) | collective-permute-done | bytes 262176 | tf_op jit(solution)/shard_map/ppermute | solution.py:330
  75.2 8.8 %shard_map.111 = s16[3584,128]{1,0:T(8,128)(2,1)} custom-call(bf16[1536,512]{1,0:T(8,128)(2,1)} %bitcast.10, bf16[2,1024,128]{2,1,0:T(8,128)(2,1)} %refs_2_.1, bf16[2,1024,128]{2,1,0:T(8,128)(2,1)} %copy-done.13, bf16[2,1024,128]{2,1,0:T(8,128)(2,1)} %copy-done.11, bf16[2,1024,128]{2,1,0:T(8,128)(2,1)} %copy-done.15, bf16[2,1024,128]{2,1,0:T(8,128)(2,1)} %refs_3_.3, ...), custom_call_target="tpu_custom_call" | custom-call | tf_op jit(solution)/shard_map/pallas_call | solution.py:313
  84.0 10.4 %all-to-all-start.1 = ((s16[64,56,128]{2,1,0:T(8,128)(2,1)}), s16[64,56,128]{2,1,0:T(8,128)(2,1)S(1)}, u32[]{:S(2)}, u32[]{:S(2)}) async-start(s16[64,56,128]{2,1,0:T(8,128)(2,1)} %bitcast.12), calls=%async_computation.1 | async-start | bytes 1835008 | tf_op jit(solution)/shard_map/all_to_all | solution.py:360
  95.6 3.2 %collective-permute-start.18 = (bf16[768,512]{1,0:T(8,128)(2,1)}, bf16[768,512]{1,0:T(8,128)(2,1)S(1)}, u32[]{:S(2)}, u32[]{:S(2)}) collective-permute-start(bf16[768,512]{1,0:T(8,128)(2,1)} %bitcast.9), channel_id=1, source_target_pairs={{0,1},{1,2},{2,3},{3,0},{4,5},{5,6},{6,7},{7,4},{8,9},{9,10},{10,1... | collective-permute-start | bytes 2359304 | tf_op jit(solution)/shard_map/ppermute | solution.py:346
  100.9 16.6 %collective-permute-done.16.refs_3_ = bf16[768,512]{1,0:T(8,128)(2,1)S(1)} collective-permute-done((bf16[768,512]{1,0:T(8,128)(2,1)}, bf16[768,512]{1,0:T(8,128)(2,1)S(1)}, u32[]{:S(2)}, u32[]{:S(2)}) %collective-permute-start.16) | collective-permute-done | bytes 786464 | tf_op jit(solution)/shard_map/ppermute | solution.py:345
  117.5 3.2 %collective-permute-start.19 = (bf16[768,512]{1,0:T(8,128)(2,1)S(1)}, bf16[768,512]{1,0:T(8,128)(2,1)}, u32[]{:S(2)}, u32[]{:S(2)}) collective-permute-start(bf16[768,512]{1,0:T(8,128)(2,1)S(1)} %collective-permute-done.18.refs_2_), channel_id=1, source_target_pairs={{0,1},{1,2},{2,3},{3,0},{4,5},{5,6},{6,7},{7,4},{8,9},{9,10},{10,1... | collective-permute-start | bytes 2359304 | tf_op jit(solution)/shard_map/ppermute | solution.py:350
  121.7 4.0 %shard_map.112 = (s16[72,1152]{1,0:T(8,128)(2,1)}, s16[72,1152]{1,0:T(8,128)(2,1)}, s16[72,1152]{1,0:T(8,128)(2,1)}, s16[72,1152]{1,0:T(8,128)(2,1)}) custom-call(s32[1]{0:T(128)} %bitcast.refs_0_, s16[3584,128]{1,0:T(8,128)(2,1)} %bitcast.13, bf16[2,384,256]{2,1,0:T(8,128)(2,1)} %get-tuple-element.20.refs_2_), custom_call_target="tpu_custom_call" | custom-call | tf_op jit(solution)/shard_map/pallas_call | solution.py:313
  125.6 2.5 %collective-permute-start.10 = (s16[72,1152]{1,0:T(8,128)(2,1)}, s16[72,1152]{1,0:T(8,128)(2,1)S(1)}, u32[]{:S(2)}, u32[]{:S(2)}) collective-permute-start(s16[72,1152]{1,0:T(8,128)(2,1)} %get-tuple-element.22), channel_id=1, source_target_pairs={{0,1},{1,2},{2,3},{3,0},{4,5},{5,6},{6,7},{7,4},{8,9},{9,10},{10,1... | collective-permute-start | bytes 497672 | tf_op jit(solution)/shard_map/ppermute | solution.py:373
  128.1 25.2 %collective-permute-done.10.from_left = s16[72,1152]{1,0:T(8,128)(2,1)S(1)} collective-permute-done((s16[72,1152]{1,0:T(8,128)(2,1)}, s16[72,1152]{1,0:T(8,128)(2,1)S(1)}, u32[]{:S(2)}, u32[]{:S(2)}) %collective-permute-start.10) | collective-permute-done | bytes 165920 | tf_op jit(solution)/shard_map/ppermute | solution.py:373
  154.9 5.5 %collective-permute-done.11.from_right = s16[72,1152]{1,0:T(8,128)(2,1)S(1)} collective-permute-done((s16[72,1152]{1,0:T(8,128)(2,1)}, s16[72,1152]{1,0:T(8,128)(2,1)S(1)}, u32[]{:S(2)}, u32[]{:S(2)}) %collective-permute-start.11) | collective-permute-done | bytes 165920 | tf_op jit(solution)/shard_map/ppermute | solution.py:374
  162.3 5.2 %collective-permute-done.12.from_opposite = s16[72,1152]{1,0:T(8,128)(2,1)S(1)} collective-permute-done((s16[72,1152]{1,0:T(8,128)(2,1)}, s16[72,1152]{1,0:T(8,128)(2,1)S(1)}, u32[]{:S(2)}, u32[]{:S(2)}) %collective-permute-start.12) | collective-permute-done | bytes 165920 | tf_op jit(solution)/shard_map/ppermute | solution.py:375
  168.2 2.0 %shard_map.113 = (bf16[64,1024]{1,0:T(8,128)(2,1)}, f32[2,256]{1,0:T(2,128)}) custom-call(s16[72,1152]{1,0:T(8,128)(2,1)} %get-tuple-element.21.own, s16[72,1152]{1,0:T(8,128)(2,1)} %copy-done.18, s16[72,1152]{1,0:T(8,128)(2,1)} %copy-done.19, s16[72,1152]{1,0:T(8,128)(2,1)} %copy-done.20, f32[2,256]{1,0:T(2,128)} %bitcast.16), custom_call_target="tpu_custom_call" | custom-call | tf_op jit(solution)/shard_map/pallas_call | solution.py:313
  173.0 2.2 %collective-permute-start.13 = (bf16[64,1024]{1,0:T(8,128)(2,1)}, bf16[64,1024]{1,0:T(8,128)(2,1)S(1)}, u32[]{:S(2)}, u32[]{:S(2)}) collective-permute-start(bf16[64,1024]{1,0:T(8,128)(2,1)} %get-tuple-element.25.refs_1_), channel_id=1, source_target_pairs={{0,1},{1,2},{2,3},{3,0},{4,5},{5,6},{6,7},{7,4},{8,9},{9,10},{10,1... | collective-permute-start | bytes 393224 | tf_op jit(solution)/shard_map/ppermute | solution.py:383
  175.3 9.9 %shard_map.115 = (f32[2,1024,128]{2,1,0:T(8,128)}, f32[2,1024,128]{2,1,0:T(8,128)}, f32[2,128,1024]{2,1,0:T(8,128)}) custom-call(bf16[1536,512]{1,0:T(8,128)(2,1)} %bitcast.11, bf16[768,512]{1,0:T(8,128)(2,1)} %collective-permute-done.20.refs_1_, bf16[768,512]{1,0:T(8,128)(2,1)} %copy-done.9, bf16[768,512]{1,0:T(8,128)(2,1)} %copy-done.8, ...), custom_call_target="tpu_custom_call" | custom-call | tf_op jit(solution)/shard_map/pallas_call | solution.py:313
  186.1 7.0 %shard_map.116 = (f32[2,1024,128]{2,1,0:T(8,128)}, f32[2,1024,128]{2,1,0:T(8,128)}, f32[2,128,1024]{2,1,0:T(8,128)}) custom-call(bf16[768,512]{1,0:T(8,128)(2,1)} %copy-done.10, bf16[768,512]{1,0:T(8,128)(2,1)} %collective-permute-done.19.refs_1_, bf16[2,1024,128]{2,1,0:T(8,128)(2,1)} %refs_2_.1, bf16[2,1024,128]{2,1,0:T(8,128)(2,1)} %refs_3_.3, ...), custom_call_target="tpu_custom_call" | custom-call | tf_op jit(solution)/shard_map/pallas_call | solution.py:313
  (82 shorter events, 18.6 us)
Async XLA Ops:
  6.1 67.8 %all-to-all-start = ((bf16[64,24,512]{2,1,0:T(8,128)(2,1)}), bf16[64,24,512]{2,1,0:T(8,128)(2,1)S(1)}, u32[]{:S(2)}, u32[]{:S(2)}) async-start(bf16[64,24,512]{2,1,0:T(8,128)(2,1)} %bitcast.14), calls=%async_computation | async-start | bytes 3145728 | tf_op jit(solution)/shard_map/all_to_all | solution.py:339
  18.4 16.1 %collective-permute-start.1 = (bf16[2,1024,128]{2,1,0:T(8,128)(2,1)S(1)}, bf16[2,1024,128]{2,1,0:T(8,128)(2,1)S(1)}, u32[]{:S(2)}, u32[]{:S(2)}) collective-permute-start(bf16[2,1024,128]{2,1,0:T(8,128)(2,1)S(1)} %copy-done.2), channel_id=1, source_target_pairs={{0,3},{1,0},{2,1},{3,2},{4,7},{5,4},{6,5},{7,6},{8,11},{9,8},{10,9... | collective-permute-start | bytes 1572872 | tf_op jit(solution)/shard_map/ppermute | solution.py:327
  19.3 15.2 %collective-permute-start.3 = (bf16[2,1024,128]{2,1,0:T(8,128)(2,1)S(1)}, bf16[2,1024,128]{2,1,0:T(8,128)(2,1)S(1)}, u32[]{:S(2)}, u32[]{:S(2)}) collective-permute-start(bf16[2,1024,128]{2,1,0:T(8,128)(2,1)S(1)} %copy-done.3), channel_id=1, source_target_pairs={{0,1},{1,2},{2,3},{3,0},{4,5},{5,6},{6,7},{7,4},{8,9},{9,10},{10,1... | collective-permute-start | bytes 1572872 | tf_op jit(solution)/shard_map/ppermute | solution.py:326
  21.7 24.0 %collective-permute-start.7 = (bf16[2,128,1024]{2,1,0:T(8,128)(2,1)S(1)}, bf16[2,128,1024]{2,1,0:T(8,128)(2,1)S(1)}, u32[]{:S(2)}, u32[]{:S(2)}) collective-permute-start(bf16[2,128,1024]{2,1,0:T(8,128)(2,1)S(1)} %copy-done.4), channel_id=1, source_target_pairs={{0,3},{1,0},{2,1},{3,2},{4,7},{5,4},{6,5},{7,6},{8,11},{9,8},{10,9... | collective-permute-start | bytes 1572872 | tf_op jit(solution)/shard_map/ppermute | solution.py:327
  21.7 24.0 %collective-permute-start.6 = (bf16[2,128,1024]{2,1,0:T(8,128)(2,1)S(1)}, bf16[2,128,1024]{2,1,0:T(8,128)(2,1)S(1)}, u32[]{:S(2)}, u32[]{:S(2)}) collective-permute-start(bf16[2,128,1024]{2,1,0:T(8,128)(2,1)S(1)} %copy-done.4), channel_id=1, source_target_pairs={{0,1},{1,2},{2,3},{3,0},{4,5},{5,6},{6,7},{7,4},{8,9},{9,10},{10,1... | collective-permute-start | bytes 1572872 | tf_op jit(solution)/shard_map/ppermute | solution.py:326
  25.0 31.6 %collective-permute-start = (bf16[2,1024,128]{2,1,0:T(8,128)(2,1)S(1)}, bf16[2,1024,128]{2,1,0:T(8,128)(2,1)S(1)}, u32[]{:S(2)}, u32[]{:S(2)}) collective-permute-start(bf16[2,1024,128]{2,1,0:T(8,128)(2,1)S(1)} %copy-done.2), channel_id=1, source_target_pairs={{0,1},{1,2},{2,3},{3,0},{4,5},{5,6},{6,7},{7,4},{8,9},{9,10},{10,1... | collective-permute-start | bytes 1572872 | tf_op jit(solution)/shard_map/ppermute | solution.py:326
  34.5 25.7 %collective-permute-start.4 = (bf16[2,1024,128]{2,1,0:T(8,128)(2,1)S(1)}, bf16[2,1024,128]{2,1,0:T(8,128)(2,1)S(1)}, u32[]{:S(2)}, u32[]{:S(2)}) collective-permute-start(bf16[2,1024,128]{2,1,0:T(8,128)(2,1)S(1)} %copy-done.3), channel_id=1, source_target_pairs={{0,3},{1,0},{2,1},{3,2},{4,7},{5,4},{6,5},{7,6},{8,11},{9,8},{10,9... | collective-permute-start | bytes 1572872 | tf_op jit(solution)/shard_map/ppermute | solution.py:327
  34.5 38.5 %collective-permute-start.2 = (bf16[2,1024,128]{2,1,0:T(8,128)(2,1)S(1)}, bf16[2,1024,128]{2,1,0:T(8,128)(2,1)S(1)}, u32[]{:S(2)}, u32[]{:S(2)}) collective-permute-start(bf16[2,1024,128]{2,1,0:T(8,128)(2,1)S(1)} %collective-permute-done.1.refs_3_), channel_id=1, source_target_pairs={{0,3},{1,0},{2,1},{3,2},{4,7},{5,4},{6,5},{7,6},{8,11},{9,8},{10,9... | collective-permute-start | bytes 1572872 | tf_op jit(solution)/shard_map/ppermute | solution.py:328
  45.7 28.2 %collective-permute-start.5 = (bf16[2,1024,128]{2,1,0:T(8,128)(2,1)S(1)}, bf16[2,1024,128]{2,1,0:T(8,128)(2,1)}, u32[]{:S(2)}, u32[]{:S(2)}) collective-permute-start(bf16[2,1024,128]{2,1,0:T(8,128)(2,1)S(1)} %collective-permute-done.3.refs_6_), channel_id=1, source_target_pairs={{0,1},{1,2},{2,3},{3,0},{4,5},{5,6},{6,7},{7,4},{8,9},{9,10},{10,1... | collective-permute-start | bytes 1572872 | tf_op jit(solution)/shard_map/ppermute | solution.py:329
  45.8 27.2 %collective-permute-start.8 = (bf16[1,128,1024]{2,1,0:T(8,128)(2,1)S(1)}, bf16[1,128,1024]{2,1,0:T(8,128)(2,1)S(1)}, u32[]{:S(2)}, u32[]{:S(2)}) collective-permute-start(bf16[1,128,1024]{2,1,0:T(8,128)(2,1)S(1)} %slice.24), channel_id=1, source_target_pairs={{0,3},{1,0},{2,1},{3,2},{4,7},{5,4},{6,5},{7,6},{8,11},{9,8},{10,9... | collective-permute-start | bytes 786440 | tf_op jit(solution)/shard_map/ppermute | solution.py:330
  56.6 16.4 %collective-permute-start.9 = (bf16[1,128,1024]{2,1,0:T(8,128)(2,1)S(1)}, bf16[1,128,1024]{2,1,0:T(8,128)(2,1)S(1)}, u32[]{:S(2)}, u32[]{:S(2)}) collective-permute-start(bf16[1,128,1024]{2,1,0:T(8,128)(2,1)S(1)} %slice.25), channel_id=1, source_target_pairs={{0,1},{1,2},{2,3},{3,0},{4,5},{5,6},{6,7},{7,4},{8,9},{9,10},{10,1... | collective-permute-start | bytes 786440 | tf_op jit(solution)/shard_map/ppermute | solution.py:331
  84.0 36.8 %all-to-all-start.1 = ((s16[64,56,128]{2,1,0:T(8,128)(2,1)}), s16[64,56,128]{2,1,0:T(8,128)(2,1)S(1)}, u32[]{:S(2)}, u32[]{:S(2)}) async-start(s16[64,56,128]{2,1,0:T(8,128)(2,1)} %bitcast.12), calls=%async_computation.1 | async-start | bytes 1835008 | tf_op jit(solution)/shard_map/all_to_all | solution.py:360
  95.6 21.8 %collective-permute-start.16 = (bf16[768,512]{1,0:T(8,128)(2,1)}, bf16[768,512]{1,0:T(8,128)(2,1)S(1)}, u32[]{:S(2)}, u32[]{:S(2)}) collective-permute-start(bf16[768,512]{1,0:T(8,128)(2,1)} %bitcast.8), channel_id=1, source_target_pairs={{0,3},{1,0},{2,1},{3,2},{4,7},{5,4},{6,5},{7,6},{8,11},{9,8},{10,9... | collective-permute-start | bytes 2359304 | tf_op jit(solution)/shard_map/ppermute | solution.py:345
  95.6 21.8 %collective-permute-start.18 = (bf16[768,512]{1,0:T(8,128)(2,1)}, bf16[768,512]{1,0:T(8,128)(2,1)S(1)}, u32[]{:S(2)}, u32[]{:S(2)}) collective-permute-start(bf16[768,512]{1,0:T(8,128)(2,1)} %bitcast.9), channel_id=1, source_target_pairs={{0,1},{1,2},{2,3},{3,0},{4,5},{5,6},{6,7},{7,4},{8,9},{9,10},{10,1... | collective-permute-start | bytes 2359304 | tf_op jit(solution)/shard_map/ppermute | solution.py:346
  98.9 73.1 %collective-permute-start.20 = (bf16[768,512]{1,0:T(8,128)(2,1)}, bf16[768,512]{1,0:T(8,128)(2,1)}, u32[]{:S(2)}, u32[]{:S(2)}) collective-permute-start(bf16[768,512]{1,0:T(8,128)(2,1)} %bitcast.8), channel_id=1, source_target_pairs={{0,1},{1,2},{2,3},{3,0},{4,5},{5,6},{6,7},{7,4},{8,9},{9,10},{10,1... | collective-permute-start | bytes 2359304 | tf_op jit(solution)/shard_map/ppermute | solution.py:348
  100.5 72.5 %collective-permute-start.21 = (bf16[768,512]{1,0:T(8,128)(2,1)}, bf16[768,512]{1,0:T(8,128)(2,1)}, u32[]{:S(2)}, u32[]{:S(2)}) collective-permute-start(bf16[768,512]{1,0:T(8,128)(2,1)} %bitcast.9), channel_id=1, source_target_pairs={{0,3},{1,0},{2,1},{3,2},{4,7},{5,4},{6,5},{7,6},{8,11},{9,8},{10,9... | collective-permute-start | bytes 2359304 | tf_op jit(solution)/shard_map/ppermute | solution.py:347
  117.5 67.7 %collective-permute-start.17 = (bf16[768,512]{1,0:T(8,128)(2,1)S(1)}, bf16[768,512]{1,0:T(8,128)(2,1)S(1)}, u32[]{:S(2)}, u32[]{:S(2)}) collective-permute-start(bf16[768,512]{1,0:T(8,128)(2,1)S(1)} %collective-permute-done.16.refs_3_), channel_id=1, source_target_pairs={{0,3},{1,0},{2,1},{3,2},{4,7},{5,4},{6,5},{7,6},{8,11},{9,8},{10,9... | collective-permute-start | bytes 2359304 | tf_op jit(solution)/shard_map/ppermute | solution.py:349
  117.5 67.7 %collective-permute-start.19 = (bf16[768,512]{1,0:T(8,128)(2,1)S(1)}, bf16[768,512]{1,0:T(8,128)(2,1)}, u32[]{:S(2)}, u32[]{:S(2)}) collective-permute-start(bf16[768,512]{1,0:T(8,128)(2,1)S(1)} %collective-permute-done.18.refs_2_), channel_id=1, source_target_pairs={{0,1},{1,2},{2,3},{3,0},{4,5},{5,6},{6,7},{7,4},{8,9},{9,10},{10,1... | collective-permute-start | bytes 2359304 | tf_op jit(solution)/shard_map/ppermute | solution.py:350
  125.6 27.6 %collective-permute-start.10 = (s16[72,1152]{1,0:T(8,128)(2,1)}, s16[72,1152]{1,0:T(8,128)(2,1)S(1)}, u32[]{:S(2)}, u32[]{:S(2)}) collective-permute-start(s16[72,1152]{1,0:T(8,128)(2,1)} %get-tuple-element.22), channel_id=1, source_target_pairs={{0,1},{1,2},{2,3},{3,0},{4,5},{5,6},{6,7},{7,4},{8,9},{9,10},{10,1... | collective-permute-start | bytes 497672 | tf_op jit(solution)/shard_map/ppermute | solution.py:373
  153.3 7.2 %collective-permute-start.11 = (s16[72,1152]{1,0:T(8,128)(2,1)}, s16[72,1152]{1,0:T(8,128)(2,1)S(1)}, u32[]{:S(2)}, u32[]{:S(2)}) collective-permute-start(s16[72,1152]{1,0:T(8,128)(2,1)} %get-tuple-element.23), channel_id=1, source_target_pairs={{0,3},{1,0},{2,1},{3,2},{4,7},{5,4},{6,5},{7,6},{8,11},{9,8},{10,9... | collective-permute-start | bytes 497672 | tf_op jit(solution)/shard_map/ppermute | solution.py:374
  160.4 7.1 %collective-permute-start.12 = (s16[72,1152]{1,0:T(8,128)(2,1)}, s16[72,1152]{1,0:T(8,128)(2,1)S(1)}, u32[]{:S(2)}, u32[]{:S(2)}) collective-permute-start(s16[72,1152]{1,0:T(8,128)(2,1)} %get-tuple-element.24), channel_id=1, source_target_pairs={{0,2},{1,3},{2,0},{3,1},{4,6},{5,7},{6,4},{7,5},{8,10},{9,11},{10,... | collective-permute-start | bytes 497672 | tf_op jit(solution)/shard_map/ppermute | solution.py:375
  170.2 23.0 %collective-permute-start.15 = (bf16[64,1024]{1,0:T(8,128)(2,1)}, bf16[64,1024]{1,0:T(8,128)(2,1)S(1)}, u32[]{:S(2)}, u32[]{:S(2)}) collective-permute-start(bf16[64,1024]{1,0:T(8,128)(2,1)} %get-tuple-element.25.refs_1_), channel_id=1, source_target_pairs={{0,2},{1,3},{2,0},{3,1},{4,6},{5,7},{6,4},{7,5},{8,10},{9,11},{10,... | collective-permute-start | bytes 393224 | tf_op jit(solution)/shard_map/ppermute | solution.py:385
  172.0 21.2 %collective-permute-start.14 = (bf16[64,1024]{1,0:T(8,128)(2,1)}, bf16[64,1024]{1,0:T(8,128)(2,1)S(1)}, u32[]{:S(2)}, u32[]{:S(2)}) collective-permute-start(bf16[64,1024]{1,0:T(8,128)(2,1)} %get-tuple-element.25.refs_1_), channel_id=1, source_target_pairs={{0,3},{1,0},{2,1},{3,2},{4,7},{5,4},{6,5},{7,6},{8,11},{9,8},{10,9... | collective-permute-start | bytes 393224 | tf_op jit(solution)/shard_map/ppermute | solution.py:384
  173.0 20.2 %collective-permute-start.13 = (bf16[64,1024]{1,0:T(8,128)(2,1)}, bf16[64,1024]{1,0:T(8,128)(2,1)S(1)}, u32[]{:S(2)}, u32[]{:S(2)}) collective-permute-start(bf16[64,1024]{1,0:T(8,128)(2,1)} %get-tuple-element.25.refs_1_), channel_id=1, source_target_pairs={{0,1},{1,2},{2,3},{3,0},{4,5},{5,6},{6,7},{7,4},{8,9},{9,10},{10,1... | collective-permute-start | bytes 393224 | tf_op jit(solution)/shard_map/ppermute | solution.py:383
  (24 other events, 357.8 us)

commit v6 on v5

--- a/solution.py
+++ b/solution.py
@@ -406,8 +406,9 @@
             scratch=[VMEM((count, model_width), BF16)] * 2,
         )
 
-    near = weight_sums((landed, left_low, left_high, right_low, right_high), ())
-    gate_grad, up_grad, down_grad = weight_sums((opposite_low, opposite_high), near)
+    near = weight_sums((landed, right_low, left_high), ())
+    far = (right_high, left_low, opposite_low, opposite_high)
+    gate_grad, up_grad, down_grad = weight_sums(far, near)
     return (tokens_grad, gates_grad.T, gate_grad, up_grad, down_grad)
 
 

time: 197 us -> 195 us (0.990)
    ppermute x1, waiting for transfers between devices: 16.6 us -> 0.01 us  [step(): right_low = lax.ppermute(low, 'tp', left)]
    ppermute x1, waiting for transfers between devices: 0.01 us -> 15 us  [step(): left_high = lax.ppermute(high, 'tp', right)]
    unnamed x48 -> x46, local copies, waits for them, and re-layouts: 5.97 us -> 5.08 us
  transfers between devices with their start and end apart: 24 -> 24, of which waited for: 8 -> 9; matrix products, arithmetic and copies ran while one was open for 1% -> 1% of each run, Pallas kernels for 12% -> 12%
where the time goes in v6:
time: 195 us; the launch traced here: 194 us
  waiting for transfers between devices  95.7 us (49%)
  starting transfers between devices  52.7 us (27%)
  Pallas kernels  39 us (20%)
  local copies, waits for them, and re-layouts  6.11 us (3%)
    pallas_call x7, Pallas kernels, call(): pl.pallas_call(kernel, out_shape=out_shape, in_specs=[scalar] * scalars +...  39 us
    ppermute x1, waiting for transfers between devices, step(): lax.ppermute(to_right, 'tp', right)  24.7 us
    ppermute x3, waiting for transfers between devices, step(): kept.append(lax.ppermute(mine, 'tp', left))  20.6 us
    ppermute x1, waiting for transfers between devices, step(): left_high = lax.ppermute(high, 'tp', right)  15 us
    ppermute x1, waiting for transfers between devices, step(): down_even = lax.ppermute(downs[2][0:1], 'tp', left)  12.8 us
    all_to_all x1, starting transfers between devices, step(): lax.all_to_all(send.reshape(groups, chunk, half), 'ep', split_axis=0, con...  12.2 us
    all_to_all x1, starting transfers between devices, step(): back = lax.all_to_all(back, 'ep', split_axis=0, concat_axis=0, tiled=True)  10.4 us
    ppermute x3, waiting for transfers between devices, step(): kept.append(lax.ppermute(mine, 'tp', right))  8.7 us
  transfers between devices with their start and end apart: 24, of which 9 were waited for; matrix products, arithmetic and copies ran while one was open for 1% of the time, Pallas kernels for 12%

profile of v6, /device:TPU:14, one launch (start us, length us, event | category | flops | bytes accessed | tf_op | source)
XLA Modules:
  0.0 194.3 jit_solution(18305758111061966891)
XLA Ops:
  0.6 5.5 %shard_map.110 = (bf16[1536,512]{1,0:T(8,128)(2,1)}, bf16[2,384,256]{2,1,0:T(8,128)(2,1)}) custom-call(s32[1]{0:T(128)} %bitcast.refs_0_, s32[2,256]{1,0:T(2,128)} %bitcast.19, f32[2,256]{1,0:T(2,128)} %bitcast.17, bf16[256,1024]{1,0:T(8,128)(2,1)} %refs_3_.2, bf16[256,1024]{1,0:T(8,128)(2,1)} %refs_4_.3), custom_call_target="tpu_custom_call" | custom-call | tf_op jit(solution)/shard_map/pallas_call | solution.py:313
  6.1 12.2 %all-to-all-start = ((bf16[64,24,512]{2,1,0:T(8,128)(2,1)}), bf16[64,24,512]{2,1,0:T(8,128)(2,1)S(1)}, u32[]{:S(2)}, u32[]{:S(2)}) async-start(bf16[64,24,512]{2,1,0:T(8,128)(2,1)} %bitcast.14), calls=%async_computation | async-start | bytes 3145728 | tf_op jit(solution)/shard_map/all_to_all | solution.py:339
  19.3 2.4 %collective-permute-start.3 = (bf16[2,1024,128]{2,1,0:T(8,128)(2,1)S(1)}, bf16[2,1024,128]{2,1,0:T(8,128)(2,1)S(1)}, u32[]{:S(2)}, u32[]{:S(2)}) collective-permute-start(bf16[2,1024,128]{2,1,0:T(8,128)(2,1)S(1)} %copy-done.3), channel_id=1, source_target_pairs={{0,1},{1,2},{2,3},{3,0},{4,5},{5,6},{6,7},{7,4},{8,9},{9,10},{10,1... | collective-permute-start | bytes 1572872 | tf_op jit(solution)/shard_map/ppermute | solution.py:326
  21.7 3.2 %collective-permute-start.6 = (bf16[2,128,1024]{2,1,0:T(8,128)(2,1)S(1)}, bf16[2,128,1024]{2,1,0:T(8,128)(2,1)S(1)}, u32[]{:S(2)}, u32[]{:S(2)}) collective-permute-start(bf16[2,128,1024]{2,1,0:T(8,128)(2,1)S(1)} %copy-done.4), channel_id=1, source_target_pairs={{0,1},{1,2},{2,3},{3,0},{4,5},{5,6},{6,7},{7,4},{8,9},{9,10},{10,1... | collective-permute-start | bytes 1572872 | tf_op jit(solution)/shard_map/ppermute | solution.py:326
  25.0 9.5 %collective-permute-done.1.refs_3_ = bf16[2,1024,128]{2,1,0:T(8,128)(2,1)S(1)} collective-permute-done((bf16[2,1024,128]{2,1,0:T(8,128)(2,1)S(1)}, bf16[2,1024,128]{2,1,0:T(8,128)(2,1)S(1)}, u32[]{:S(2)}, u32[]{:S(2)}) %collective-permute-start.1) | collective-permute-done | bytes 524320 | tf_op jit(solution)/shard_map/ppermute | solution.py:327
  34.6 11.1 %collective-permute-done.7.refs_11_ = bf16[2,128,1024]{2,1,0:T(8,128)(2,1)S(1)} collective-permute-done((bf16[2,128,1024]{2,1,0:T(8,128)(2,1)S(1)}, bf16[2,128,1024]{2,1,0:T(8,128)(2,1)S(1)}, u32[]{:S(2)}, u32[]{:S(2)}) %collective-permute-start.7) | collective-permute-done | bytes 524320 | tf_op jit(solution)/shard_map/ppermute | solution.py:327
  45.8 2.1 %collective-permute-start.8 = (bf16[1,128,1024]{2,1,0:T(8,128)(2,1)S(1)}, bf16[1,128,1024]{2,1,0:T(8,128)(2,1)S(1)}, u32[]{:S(2)}, u32[]{:S(2)}) collective-permute-start(bf16[1,128,1024]{2,1,0:T(8,128)(2,1)S(1)} %slice.24), channel_id=1, source_target_pairs={{0,3},{1,0},{2,1},{3,2},{4,7},{5,4},{6,5},{7,6},{8,11},{9,8},{10,9... | collective-permute-start | bytes 786440 | tf_op jit(solution)/shard_map/ppermute | solution.py:330
  47.9 8.7 %collective-permute-done.refs_2_ = bf16[2,1024,128]{2,1,0:T(8,128)(2,1)S(1)} collective-permute-done((bf16[2,1024,128]{2,1,0:T(8,128)(2,1)S(1)}, bf16[2,1024,128]{2,1,0:T(8,128)(2,1)S(1)}, u32[]{:S(2)}, u32[]{:S(2)}) %collective-permute-start) | collective-permute-done | bytes 524320 | tf_op jit(solution)/shard_map/ppermute | solution.py:326
  56.6 3.6 %collective-permute-start.9 = (bf16[1,128,1024]{2,1,0:T(8,128)(2,1)S(1)}, bf16[1,128,1024]{2,1,0:T(8,128)(2,1)S(1)}, u32[]{:S(2)}, u32[]{:S(2)}) collective-permute-start(bf16[1,128,1024]{2,1,0:T(8,128)(2,1)S(1)} %slice.25), channel_id=1, source_target_pairs={{0,1},{1,2},{2,3},{3,0},{4,5},{5,6},{6,7},{7,4},{8,9},{9,10},{10,1... | collective-permute-start | bytes 786440 | tf_op jit(solution)/shard_map/ppermute | solution.py:331
  60.2 12.8 %collective-permute-done.8.refs_12_ = bf16[1,128,1024]{2,1,0:T(8,128)(2,1)S(1)} collective-permute-done((bf16[1,128,1024]{2,1,0:T(8,128)(2,1)S(1)}, bf16[1,128,1024]{2,1,0:T(8,128)(2,1)S(1)}, u32[]{:S(2)}, u32[]{:S(2)}) %collective-permute-start.8) | collective-permute-done | bytes 262176 | tf_op jit(solution)/shard_map/ppermute | solution.py:330
  75.1 8.8 %shard_map.111 = s16[3584,128]{1,0:T(8,128)(2,1)} custom-call(bf16[1536,512]{1,0:T(8,128)(2,1)} %bitcast.10, bf16[2,1024,128]{2,1,0:T(8,128)(2,1)} %refs_4_.5, bf16[2,1024,128]{2,1,0:T(8,128)(2,1)} %copy-done.12, bf16[2,1024,128]{2,1,0:T(8,128)(2,1)} %copy-done.10, bf16[2,1024,128]{2,1,0:T(8,128)(2,1)} %copy-done.14, bf16[2,1024,128]{2,1,0:T(8,128)(2,1)} %refs_5_.5, ...), custom_call_target="tpu_custom_call" | custom-call | tf_op jit(solution)/shard_map/pallas_call | solution.py:313
  84.0 10.4 %all-to-all-start.1 = ((s16[64,56,128]{2,1,0:T(8,128)(2,1)}), s16[64,56,128]{2,1,0:T(8,128)(2,1)S(1)}, u32[]{:S(2)}, u32[]{:S(2)}) async-start(s16[64,56,128]{2,1,0:T(8,128)(2,1)} %bitcast.12), calls=%async_computation.1 | async-start | bytes 1835008 | tf_op jit(solution)/shard_map/all_to_all | solution.py:360
  95.4 2.8 %collective-permute-start.20 = (bf16[768,512]{1,0:T(8,128)(2,1)}, bf16[768,512]{1,0:T(8,128)(2,1)S(1)}, u32[]{:S(2)}, u32[]{:S(2)}) collective-permute-start(bf16[768,512]{1,0:T(8,128)(2,1)} %bitcast.8), channel_id=1, source_target_pairs={{0,1},{1,2},{2,3},{3,0},{4,5},{5,6},{6,7},{7,4},{8,9},{9,10},{10,1... | collective-permute-start | bytes 2359304 | tf_op jit(solution)/shard_map/ppermute | solution.py:346
  98.2 3.3 %collective-permute-start.17 = (bf16[768,512]{1,0:T(8,128)(2,1)S(1)}, bf16[768,512]{1,0:T(8,128)(2,1)}, u32[]{:S(2)}, u32[]{:S(2)}) collective-permute-start(bf16[768,512]{1,0:T(8,128)(2,1)S(1)} %bitcast.16), channel_id=1, source_target_pairs={{0,1},{1,2},{2,3},{3,0},{4,5},{5,6},{6,7},{7,4},{8,9},{9,10},{10,1... | collective-permute-start | bytes 2359304 | tf_op jit(solution)/shard_map/ppermute | solution.py:348
  101.5 15.0 %collective-permute-done.20.refs_2_ = bf16[768,512]{1,0:T(8,128)(2,1)S(1)} collective-permute-done((bf16[768,512]{1,0:T(8,128)(2,1)}, bf16[768,512]{1,0:T(8,128)(2,1)S(1)}, u32[]{:S(2)}, u32[]{:S(2)}) %collective-permute-start.20) | collective-permute-done | bytes 786464 | tf_op jit(solution)/shard_map/ppermute | solution.py:346
  116.5 3.6 %collective-permute-start.21 = (bf16[768,512]{1,0:T(8,128)(2,1)S(1)}, bf16[768,512]{1,0:T(8,128)(2,1)}, u32[]{:S(2)}, u32[]{:S(2)}) collective-permute-start(bf16[768,512]{1,0:T(8,128)(2,1)S(1)} %collective-permute-done.20.refs_2_), channel_id=1, source_target_pairs={{0,1},{1,2},{2,3},{3,0},{4,5},{5,6},{6,7},{7,4},{8,9},{9,10},{10,1... | collective-permute-start | bytes 2359304 | tf_op jit(solution)/shard_map/ppermute | solution.py:350
  121.3 4.0 %shard_map.112 = (s16[72,1152]{1,0:T(8,128)(2,1)}, s16[72,1152]{1,0:T(8,128)(2,1)}, s16[72,1152]{1,0:T(8,128)(2,1)}, s16[72,1152]{1,0:T(8,128)(2,1)}) custom-call(s32[1]{0:T(128)} %bitcast.refs_0_, s16[3584,128]{1,0:T(8,128)(2,1)} %bitcast.13, bf16[2,384,256]{2,1,0:T(8,128)(2,1)} %get-tuple-element.20.refs_2_), custom_call_target="tpu_custom_call" | custom-call | tf_op jit(solution)/shard_map/pallas_call | solution.py:313
  125.2 3.0 %collective-permute-start.10 = (s16[72,1152]{1,0:T(8,128)(2,1)}, s16[72,1152]{1,0:T(8,128)(2,1)S(1)}, u32[]{:S(2)}, u32[]{:S(2)}) collective-permute-start(s16[72,1152]{1,0:T(8,128)(2,1)} %get-tuple-element.22), channel_id=1, source_target_pairs={{0,1},{1,2},{2,3},{3,0},{4,5},{5,6},{6,7},{7,4},{8,9},{9,10},{10,1... | collective-permute-start | bytes 497672 | tf_op jit(solution)/shard_map/ppermute | solution.py:373
  128.2 24.7 %collective-permute-done.10.from_left = s16[72,1152]{1,0:T(8,128)(2,1)S(1)} collective-permute-done((s16[72,1152]{1,0:T(8,128)(2,1)}, s16[72,1152]{1,0:T(8,128)(2,1)S(1)}, u32[]{:S(2)}, u32[]{:S(2)}) %collective-permute-start.10) | collective-permute-done | bytes 165920 | tf_op jit(solution)/shard_map/ppermute | solution.py:373
  152.9 7.5 %collective-permute-done.11.from_right = s16[72,1152]{1,0:T(8,128)(2,1)S(1)} collective-permute-done((s16[72,1152]{1,0:T(8,128)(2,1)}, s16[72,1152]{1,0:T(8,128)(2,1)S(1)}, u32[]{:S(2)}, u32[]{:S(2)}) %collective-permute-start.11) | collective-permute-done | bytes 165920 | tf_op jit(solution)/shard_map/ppermute | solution.py:374
  161.2 6.2 %collective-permute-done.12.from_opposite = s16[72,1152]{1,0:T(8,128)(2,1)S(1)} collective-permute-done((s16[72,1152]{1,0:T(8,128)(2,1)}, s16[72,1152]{1,0:T(8,128)(2,1)S(1)}, u32[]{:S(2)}, u32[]{:S(2)}) %collective-permute-start.12) | collective-permute-done | bytes 165920 | tf_op jit(solution)/shard_map/ppermute | solution.py:375
  168.1 2.0 %shard_map.113 = (bf16[64,1024]{1,0:T(8,128)(2,1)}, f32[2,256]{1,0:T(2,128)}) custom-call(s16[72,1152]{1,0:T(8,128)(2,1)} %get-tuple-element.21.own, s16[72,1152]{1,0:T(8,128)(2,1)} %copy-done.17, s16[72,1152]{1,0:T(8,128)(2,1)} %copy-done.18, s16[72,1152]{1,0:T(8,128)(2,1)} %copy-done.19, f32[2,256]{1,0:T(2,128)} %bitcast.18), custom_call_target="tpu_custom_call" | custom-call | tf_op jit(solution)/shard_map/pallas_call | solution.py:313
  174.2 7.9 %shard_map.115 = (f32[2,1024,128]{2,1,0:T(8,128)}, f32[2,1024,128]{2,1,0:T(8,128)}, f32[2,128,1024]{2,1,0:T(8,128)}) custom-call(bf16[1536,512]{1,0:T(8,128)(2,1)} %bitcast.11, bf16[768,512]{1,0:T(8,128)(2,1)} %copy-done.9, bf16[768,512]{1,0:T(8,128)(2,1)} %copy-done.8, bf16[2,1024,128]{2,1,0:T(8,128)(2,1)} %refs_4_.5, bf16[2,1024,128]{2,1,0:T(8,128)(2,1)} %refs_5_.5, ...), custom_call_target="tpu_custom_call" | custom-call | tf_op jit(solution)/shard_map/pallas_call | solution.py:313
  182.1 8.9 %shard_map.116 = (f32[2,1024,128]{2,1,0:T(8,128)}, f32[2,1024,128]{2,1,0:T(8,128)}, f32[2,128,1024]{2,1,0:T(8,128)}) custom-call(bf16[768,512]{1,0:T(8,128)(2,1)} %collective-permute-done.16.refs_0_, bf16[768,512]{1,0:T(8,128)(2,1)} %collective-permute-done.17.refs_1_, bf16[768,512]{1,0:T(8,128)(2,1)} %collective-permute-done.19.refs_2_, ...), custom_call_target="tpu_custom_call" | custom-call | tf_op jit(solution)/shard_map/pallas_call | solution.py:313
  (80 shorter events, 14.3 us)
Async XLA Ops:
  6.1 67.8 %all-to-all-start = ((bf16[64,24,512]{2,1,0:T(8,128)(2,1)}), bf16[64,24,512]{2,1,0:T(8,128)(2,1)S(1)}, u32[]{:S(2)}, u32[]{:S(2)}) async-start(bf16[64,24,512]{2,1,0:T(8,128)(2,1)} %bitcast.14), calls=%async_computation | async-start | bytes 3145728 | tf_op jit(solution)/shard_map/all_to_all | solution.py:339
  18.4 16.1 %collective-permute-start.1 = (bf16[2,1024,128]{2,1,0:T(8,128)(2,1)S(1)}, bf16[2,1024,128]{2,1,0:T(8,128)(2,1)S(1)}, u32[]{:S(2)}, u32[]{:S(2)}) collective-permute-start(bf16[2,1024,128]{2,1,0:T(8,128)(2,1)S(1)} %copy-done.2), channel_id=1, source_target_pairs={{0,3},{1,0},{2,1},{3,2},{4,7},{5,4},{6,5},{7,6},{8,11},{9,8},{10,9... | collective-permute-start | bytes 1572872 | tf_op jit(solution)/shard_map/ppermute | solution.py:327
  19.3 15.2 %collective-permute-start.3 = (bf16[2,1024,128]{2,1,0:T(8,128)(2,1)S(1)}, bf16[2,1024,128]{2,1,0:T(8,128)(2,1)S(1)}, u32[]{:S(2)}, u32[]{:S(2)}) collective-permute-start(bf16[2,1024,128]{2,1,0:T(8,128)(2,1)S(1)} %copy-done.3), channel_id=1, source_target_pairs={{0,1},{1,2},{2,3},{3,0},{4,5},{5,6},{6,7},{7,4},{8,9},{9,10},{10,1... | collective-permute-start | bytes 1572872 | tf_op jit(solution)/shard_map/ppermute | solution.py:326
  21.7 24.0 %collective-permute-start.7 = (bf16[2,128,1024]{2,1,0:T(8,128)(2,1)S(1)}, bf16[2,128,1024]{2,1,0:T(8,128)(2,1)S(1)}, u32[]{:S(2)}, u32[]{:S(2)}) collective-permute-start(bf16[2,128,1024]{2,1,0:T(8,128)(2,1)S(1)} %copy-done.4), channel_id=1, source_target_pairs={{0,3},{1,0},{2,1},{3,2},{4,7},{5,4},{6,5},{7,6},{8,11},{9,8},{10,9... | collective-permute-start | bytes 1572872 | tf_op jit(solution)/shard_map/ppermute | solution.py:327
  21.7 24.0 %collective-permute-start.6 = (bf16[2,128,1024]{2,1,0:T(8,128)(2,1)S(1)}, bf16[2,128,1024]{2,1,0:T(8,128)(2,1)S(1)}, u32[]{:S(2)}, u32[]{:S(2)}) collective-permute-start(bf16[2,128,1024]{2,1,0:T(8,128)(2,1)S(1)} %copy-done.4), channel_id=1, source_target_pairs={{0,1},{1,2},{2,3},{3,0},{4,5},{5,6},{6,7},{7,4},{8,9},{9,10},{10,1... | collective-permute-start | bytes 1572872 | tf_op jit(solution)/shard_map/ppermute | solution.py:326
  25.0 31.6 %collective-permute-start = (bf16[2,1024,128]{2,1,0:T(8,128)(2,1)S(1)}, bf16[2,1024,128]{2,1,0:T(8,128)(2,1)S(1)}, u32[]{:S(2)}, u32[]{:S(2)}) collective-permute-start(bf16[2,1024,128]{2,1,0:T(8,128)(2,1)S(1)} %copy-done.2), channel_id=1, source_target_pairs={{0,1},{1,2},{2,3},{3,0},{4,5},{5,6},{6,7},{7,4},{8,9},{9,10},{10,1... | collective-permute-start | bytes 1572872 | tf_op jit(solution)/shard_map/ppermute | solution.py:326
  34.5 25.7 %collective-permute-start.4 = (bf16[2,1024,128]{2,1,0:T(8,128)(2,1)S(1)}, bf16[2,1024,128]{2,1,0:T(8,128)(2,1)S(1)}, u32[]{:S(2)}, u32[]{:S(2)}) collective-permute-start(bf16[2,1024,128]{2,1,0:T(8,128)(2,1)S(1)} %copy-done.3), channel_id=1, source_target_pairs={{0,3},{1,0},{2,1},{3,2},{4,7},{5,4},{6,5},{7,6},{8,11},{9,8},{10,9... | collective-permute-start | bytes 1572872 | tf_op jit(solution)/shard_map/ppermute | solution.py:327
  34.5 38.5 %collective-permute-start.2 = (bf16[2,1024,128]{2,1,0:T(8,128)(2,1)S(1)}, bf16[2,1024,128]{2,1,0:T(8,128)(2,1)S(1)}, u32[]{:S(2)}, u32[]{:S(2)}) collective-permute-start(bf16[2,1024,128]{2,1,0:T(8,128)(2,1)S(1)} %collective-permute-done.1.refs_3_), channel_id=1, source_target_pairs={{0,3},{1,0},{2,1},{3,2},{4,7},{5,4},{6,5},{7,6},{8,11},{9,8},{10,9... | collective-permute-start | bytes 1572872 | tf_op jit(solution)/shard_map/ppermute | solution.py:328
  45.7 28.3 %collective-permute-start.5 = (bf16[2,1024,128]{2,1,0:T(8,128)(2,1)S(1)}, bf16[2,1024,128]{2,1,0:T(8,128)(2,1)}, u32[]{:S(2)}, u32[]{:S(2)}) collective-permute-start(bf16[2,1024,128]{2,1,0:T(8,128)(2,1)S(1)} %collective-permute-done.3.refs_6_), channel_id=1, source_target_pairs={{0,1},{1,2},{2,3},{3,0},{4,5},{5,6},{6,7},{7,4},{8,9},{9,10},{10,1... | collective-permute-start | bytes 1572872 | tf_op jit(solution)/shard_map/ppermute | solution.py:329
  45.8 27.2 %collective-permute-start.8 = (bf16[1,128,1024]{2,1,0:T(8,128)(2,1)S(1)}, bf16[1,128,1024]{2,1,0:T(8,128)(2,1)S(1)}, u32[]{:S(2)}, u32[]{:S(2)}) collective-permute-start(bf16[1,128,1024]{2,1,0:T(8,128)(2,1)S(1)} %slice.24), channel_id=1, source_target_pairs={{0,3},{1,0},{2,1},{3,2},{4,7},{5,4},{6,5},{7,6},{8,11},{9,8},{10,9... | collective-permute-start | bytes 786440 | tf_op jit(solution)/shard_map/ppermute | solution.py:330
  56.6 16.4 %collective-permute-start.9 = (bf16[1,128,1024]{2,1,0:T(8,128)(2,1)S(1)}, bf16[1,128,1024]{2,1,0:T(8,128)(2,1)S(1)}, u32[]{:S(2)}, u32[]{:S(2)}) collective-permute-start(bf16[1,128,1024]{2,1,0:T(8,128)(2,1)S(1)} %slice.25), channel_id=1, source_target_pairs={{0,1},{1,2},{2,3},{3,0},{4,5},{5,6},{6,7},{7,4},{8,9},{9,10},{10,1... | collective-permute-start | bytes 786440 | tf_op jit(solution)/shard_map/ppermute | solution.py:331
  84.0 36.4 %all-to-all-start.1 = ((s16[64,56,128]{2,1,0:T(8,128)(2,1)}), s16[64,56,128]{2,1,0:T(8,128)(2,1)S(1)}, u32[]{:S(2)}, u32[]{:S(2)}) async-start(s16[64,56,128]{2,1,0:T(8,128)(2,1)} %bitcast.12), calls=%async_computation.1 | async-start | bytes 1835008 | tf_op jit(solution)/shard_map/all_to_all | solution.py:360
  95.4 21.1 %collective-permute-start.20 = (bf16[768,512]{1,0:T(8,128)(2,1)}, bf16[768,512]{1,0:T(8,128)(2,1)S(1)}, u32[]{:S(2)}, u32[]{:S(2)}) collective-permute-start(bf16[768,512]{1,0:T(8,128)(2,1)} %bitcast.8), channel_id=1, source_target_pairs={{0,1},{1,2},{2,3},{3,0},{4,5},{5,6},{6,7},{7,4},{8,9},{9,10},{10,1... | collective-permute-start | bytes 2359304 | tf_op jit(solution)/shard_map/ppermute | solution.py:346
  98.2 21.8 %collective-permute-start.18 = (bf16[768,512]{1,0:T(8,128)(2,1)S(1)}, bf16[768,512]{1,0:T(8,128)(2,1)S(1)}, u32[]{:S(2)}, u32[]{:S(2)}) collective-permute-start(bf16[768,512]{1,0:T(8,128)(2,1)S(1)} %bitcast.15), channel_id=1, source_target_pairs={{0,3},{1,0},{2,1},{3,2},{4,7},{5,4},{6,5},{7,6},{8,11},{9,8},{10,9... | collective-permute-start | bytes 2359304 | tf_op jit(solution)/shard_map/ppermute | solution.py:345
  98.2 72.7 %collective-permute-start.16 = (bf16[768,512]{1,0:T(8,128)(2,1)}, bf16[768,512]{1,0:T(8,128)(2,1)}, u32[]{:S(2)}, u32[]{:S(2)}) collective-permute-start(bf16[768,512]{1,0:T(8,128)(2,1)} %bitcast.8), channel_id=1, source_target_pairs={{0,3},{1,0},{2,1},{3,2},{4,7},{5,4},{6,5},{7,6},{8,11},{9,8},{10,9... | collective-permute-start | bytes 2359304 | tf_op jit(solution)/shard_map/ppermute | solution.py:347
  98.2 74.5 %collective-permute-start.17 = (bf16[768,512]{1,0:T(8,128)(2,1)S(1)}, bf16[768,512]{1,0:T(8,128)(2,1)}, u32[]{:S(2)}, u32[]{:S(2)}) collective-permute-start(bf16[768,512]{1,0:T(8,128)(2,1)S(1)} %bitcast.16), channel_id=1, source_target_pairs={{0,1},{1,2},{2,3},{3,0},{4,5},{5,6},{6,7},{7,4},{8,9},{9,10},{10,1... | collective-permute-start | bytes 2359304 | tf_op jit(solution)/shard_map/ppermute | solution.py:348
  116.5 65.7 %collective-permute-start.21 = (bf16[768,512]{1,0:T(8,128)(2,1)S(1)}, bf16[768,512]{1,0:T(8,128)(2,1)}, u32[]{:S(2)}, u32[]{:S(2)}) collective-permute-start(bf16[768,512]{1,0:T(8,128)(2,1)S(1)} %collective-permute-done.20.refs_2_), channel_id=1, source_target_pairs={{0,1},{1,2},{2,3},{3,0},{4,5},{5,6},{6,7},{7,4},{8,9},{9,10},{10,1... | collective-permute-start | bytes 2359304 | tf_op jit(solution)/shard_map/ppermute | solution.py:350
  120.1 62.1 %collective-permute-start.19 = (bf16[768,512]{1,0:T(8,128)(2,1)S(1)}, bf16[768,512]{1,0:T(8,128)(2,1)}, u32[]{:S(2)}, u32[]{:S(2)}) collective-permute-start(bf16[768,512]{1,0:T(8,128)(2,1)S(1)} %collective-permute-done.18.refs_1_), channel_id=1, source_target_pairs={{0,3},{1,0},{2,1},{3,2},{4,7},{5,4},{6,5},{7,6},{8,11},{9,8},{10,9... | collective-permute-start | bytes 2359304 | tf_op jit(solution)/shard_map/ppermute | solution.py:349
  125.2 27.6 %collective-permute-start.10 = (s16[72,1152]{1,0:T(8,128)(2,1)}, s16[72,1152]{1,0:T(8,128)(2,1)S(1)}, u32[]{:S(2)}, u32[]{:S(2)}) collective-permute-start(s16[72,1152]{1,0:T(8,128)(2,1)} %get-tuple-element.22), channel_id=1, source_target_pairs={{0,1},{1,2},{2,3},{3,0},{4,5},{5,6},{6,7},{7,4},{8,9},{9,10},{10,1... | collective-permute-start | bytes 497672 | tf_op jit(solution)/shard_map/ppermute | solution.py:373
  152.9 7.5 %collective-permute-start.11 = (s16[72,1152]{1,0:T(8,128)(2,1)}, s16[72,1152]{1,0:T(8,128)(2,1)S(1)}, u32[]{:S(2)}, u32[]{:S(2)}) collective-permute-start(s16[72,1152]{1,0:T(8,128)(2,1)} %get-tuple-element.23), channel_id=1, source_target_pairs={{0,3},{1,0},{2,1},{3,2},{4,7},{5,4},{6,5},{7,6},{8,11},{9,8},{10,9... | collective-permute-start | bytes 497672 | tf_op jit(solution)/shard_map/ppermute | solution.py:374
  160.4 7.1 %collective-permute-start.12 = (s16[72,1152]{1,0:T(8,128)(2,1)}, s16[72,1152]{1,0:T(8,128)(2,1)S(1)}, u32[]{:S(2)}, u32[]{:S(2)}) collective-permute-start(s16[72,1152]{1,0:T(8,128)(2,1)} %get-tuple-element.24), channel_id=1, source_target_pairs={{0,2},{1,3},{2,0},{3,1},{4,6},{5,7},{6,4},{7,5},{8,10},{9,11},{10,... | collective-permute-start | bytes 497672 | tf_op jit(solution)/shard_map/ppermute | solution.py:375
  170.1 20.9 %collective-permute-start.15 = (bf16[64,1024]{1,0:T(8,128)(2,1)}, bf16[64,1024]{1,0:T(8,128)(2,1)S(1)}, u32[]{:S(2)}, u32[]{:S(2)}) collective-permute-start(bf16[64,1024]{1,0:T(8,128)(2,1)} %get-tuple-element.25.refs_1_), channel_id=1, source_target_pairs={{0,2},{1,3},{2,0},{3,1},{4,6},{5,7},{6,4},{7,5},{8,10},{9,11},{10,... | collective-permute-start | bytes 393224 | tf_op jit(solution)/shard_map/ppermute | solution.py:385
  171.0 20.1 %collective-permute-start.14 = (bf16[64,1024]{1,0:T(8,128)(2,1)}, bf16[64,1024]{1,0:T(8,128)(2,1)S(1)}, u32[]{:S(2)}, u32[]{:S(2)}) collective-permute-start(bf16[64,1024]{1,0:T(8,128)(2,1)} %get-tuple-element.25.refs_1_), channel_id=1, source_target_pairs={{0,3},{1,0},{2,1},{3,2},{4,7},{5,4},{6,5},{7,6},{8,11},{9,8},{10,9... | collective-permute-start | bytes 393224 | tf_op jit(solution)/shard_map/ppermute | solution.py:384
  172.7 18.3 %collective-permute-start.13 = (bf16[64,1024]{1,0:T(8,128)(2,1)}, bf16[64,1024]{1,0:T(8,128)(2,1)S(1)}, u32[]{:S(2)}, u32[]{:S(2)}) collective-permute-start(bf16[64,1024]{1,0:T(8,128)(2,1)} %get-tuple-element.25.refs_1_), channel_id=1, source_target_pairs={{0,1},{1,2},{2,3},{3,0},{4,5},{5,6},{6,7},{7,4},{8,9},{9,10},{10,1... | collective-permute-start | bytes 393224 | tf_op jit(solution)/shard_map/ppermute | solution.py:383
  (23 other events, 353.5 us)

commit v7 on v6

--- a/solution.py
+++ b/solution.py
@@ -75,14 +75,11 @@
 
 
 def dispatch_kernel(
-    experts, local_experts, quarter, member, routing, weights, tokens, cotangent, rows_out, pick
+    experts, local_experts, quarter, member, routing, weights, tokens, cotangent, rows_out, pick, laid
 ):
-    token_count, width = tokens.shape
-    half = width // HALVES
-    row_count = rows_out.shape[0]
+    token_count, _ = tokens.shape
     slots = pick.shape[1]
     group = local_experts * quarter
-    chunk = HALVES * 2 * group
     devices = experts // local_experts
     expert = iota((experts, token_count), 0)
     chosen = [routing[k : k + 1, :] for k in range(2)]
@@ -91,30 +88,32 @@
     later = iota((token_count, token_count), 1)
     upper = jnp.where(earlier < later, 1.0, 0.0).astype(BF16)
     before = mm((onehot[0] + onehot[1]).astype(BF16), upper)
-    row = iota((row_count, token_count), 0)
     slot = iota((slots, token_count), 0)
-    token_rows = []
+    hits = []
     for k in range(2):
         position = jnp.sum(onehot[k] * before, axis=0, keepdims=True).astype(I32)
         local = position - member[0] * quarter
         present = (local >= 0) & (local < quarter)
         device = chosen[k] // local_experts
         within = (chosen[k] - device * local_experts) * quarter + local
-        pick[k] = jnp.where(slot == jnp.where(present, within * devices + device, -1), 1.0, 0.0).astype(BF16)
-        token_rows.append(jnp.where(present, device * chunk + within, -chunk))
-    total = None
-    for h in range(HALVES):
-        columns = slice(h * half, (h + 1) * half)
-        base = h * 2 * group
-        hits = [row == r + base for r in token_rows]
-        part = mm(jnp.where(hits[0] | hits[1], 1.0, 0.0).astype(BF16), tokens[:, columns])
-        hits = [row == r + (base + group) for r in token_rows]
-        weighted = jnp.where(hits[0], weights[0:1, :], jnp.where(hits[1], weights[1:2, :], 0.0))
-        slot_weight = jnp.sum(weighted, axis=1, keepdims=True)
-        chosen_rows = jnp.where(hits[0] | hits[1], 1.0, 0.0).astype(BF16)
-        part = part + slot_weight * mm(chosen_rows, cotangent[:, columns])
-        total = part if total is None else total + part
-    rows_out[...] = total.astype(BF16)
+        hits.append(slot == jnp.where(present, within * devices + device, -1))
+        pick[k] = jnp.where(hits[k], 1.0, 0.0).astype(BF16)
+    weighted = jnp.where(hits[0], weights[0:1, :], jnp.where(hits[1], weights[1:2, :], 0.0))
+    slot_weight = jnp.sum(weighted, axis=1, keepdims=True)
+    both = jnp.where(hits[0] | hits[1], 1.0, 0.0).astype(BF16)
+    values = (mm(both, tokens[...]), mm(both, cotangent[...]) * slot_weight)
+    tiles = laid.shape[0]
+    chunk = HALVES * 2 * group
+    for kind, value in enumerate(values):
+        for h in range(HALVES):
+            for at in range(group):
+                to = (2 * h + kind) * group + at
+                for tile in range(tiles):
+                    column = (h * tiles + tile) * LANES
+                    piece = value[at * devices : (at + 1) * devices, column : column + LANES]
+                    laid[tile, pl.ds(to, devices, stride=chunk), :] = piece
+    for tile in range(tiles):
+        rows_out[:, tile * LANES : (tile + 1) * LANES] = laid[tile].astype(BF16)
 
 
 def land(source, expert, local_experts, quarter, rows, scaled, offset):
@@ -240,7 +239,7 @@
         columns.append(jnp.concatenate(pieces, axis=0))
     grad = jnp.concatenate(columns, axis=1) * scale
     both = pick[0] + pick[1]
-    grad, power, steps = code_rows(sum(mm(both, part, TN) for part in split3(grad)))
+    grad, power, steps = code_rows(sum(mm(both, part, TN) for part in split3(grad)[:2]))
     total[:, 0:width] = grad
     lane = iota((token_count, LANES), 1)
     total[:, width:] = jnp.where(lane == 0, power, jnp.where(lane == 1, steps, 0.0))
@@ -335,6 +334,7 @@
         (shape((groups * chunk, half), BF16), shape((2, slots, token_count), BF16)),
         (member, routing.T, gate_weights.T, tokens, cotangent),
         scalars=1,
+        scratch=[VMEM((half // LANES, groups * chunk, LANES), F32)],
     )
     landed = lax.all_to_all(
         send.reshape(groups, chunk, half), "ep", split_axis=0, concat_axis=0, tiled=True
@@ -407,8 +407,8 @@
         )
 
     near = weight_sums((landed, right_low, left_high), ())
-    far = (right_high, left_low, opposite_low, opposite_high)
-    gate_grad, up_grad, down_grad = weight_sums(far, near)
+    mid = weight_sums((right_high, left_low), near)
+    gate_grad, up_grad, down_grad = weight_sums((opposite_low, opposite_high), mid)
     return (tokens_grad, gates_grad.T, gate_grad, up_grad, down_grad)
 
 

time: 195 us -> 200 us (1.026)
  Pallas kernels: 39 us -> 42.1 us
  starting transfers between devices: 52.7 us -> 54.8 us
    ppermute x1, waiting for transfers between devices: 0.01 us -> 16.6 us  [step(): right_low = lax.ppermute(low, 'tp', left)]
    ppermute x1, waiting for transfers between devices: 15 us -> 0.01 us  [step(): left_high = lax.ppermute(high, 'tp', right)]
    pallas_call x7 -> x8, Pallas kernels: 39 us -> 42.1 us  [call(): pl.pallas_call(kernel, out_shape=out_shape, in_specs=[scalar] * scalars +...]
    unnamed x46 -> x48, local copies, waits for them, and re-layouts: 5.08 us -> 5.93 us
  transfers between devices with their start and end apart: 24 -> 24, of which waited for: 9 -> 8; matrix products, arithmetic and copies ran while one was open for 1% -> 1% of each run, Pallas kernels for 12% -> 14%
where the time goes in v7:
time: 200 us
  waiting for transfers between devices  94.8 us (47%)
  starting transfers between devices  54.8 us (27%)
  Pallas kernels  42.1 us (21%)
  local copies, waits for them, and re-layouts  7.21 us (4%)
    pallas_call x8, Pallas kernels, call(): pl.pallas_call(kernel, out_shape=out_shape, in_specs=[scalar] * scalars +...  42.1 us
    ppermute x1, waiting for transfers between devices, step(): lax.ppermute(to_right, 'tp', right)  25.5 us
    ppermute x3, waiting for transfers between devices, step(): kept.append(lax.ppermute(mine, 'tp', left))  20.6 us
    ppermute x1, waiting for transfers between devices, step(): right_low = lax.ppermute(low, 'tp', left)  16.6 us
    ppermute x1, waiting for transfers between devices, step(): down_even = lax.ppermute(downs[2][0:1], 'tp', left)  12.8 us
    all_to_all x1, starting transfers between devices, step(): lax.all_to_all(send.reshape(groups, chunk, half), 'ep', split_axis=0, con...  12.2 us
    all_to_all x1, starting transfers between devices, step(): back = lax.all_to_all(back, 'ep', split_axis=0, concat_axis=0, tiled=True)  10.4 us
    ppermute x3, waiting for transfers between devices, step(): kept.append(lax.ppermute(mine, 'tp', right))  8.68 us
  transfers between devices with their start and end apart: 24, of which 8 were waited for; matrix products, arithmetic and copies ran while one was open for 1% of the time, Pallas kernels for 14%

profile of v7, /device:TPU:14, one launch (start us, length us, event | category | flops | bytes accessed | tf_op | source)
XLA Modules:
  0.0 199.7 jit_solution(3818152708296494250)
XLA Ops:
  0.6 3.8 %shard_map.110 = (bf16[1536,512]{1,0:T(8,128)(2,1)}, bf16[2,384,256]{2,1,0:T(8,128)(2,1)}) custom-call(s32[1]{0:T(128)} %bitcast.refs_0_, s32[2,256]{1,0:T(2,128)} %bitcast.17, f32[2,256]{1,0:T(2,128)} %bitcast.15, bf16[256,1024]{1,0:T(8,128)(2,1)} %refs_3_.4, bf16[256,1024]{1,0:T(8,128)(2,1)} %refs_4_.4), custom_call_target="tpu_custom_call" | custom-call | tf_op jit(solution)/shard_map/pallas_call | solution.py:312
  4.4 12.2 %all-to-all-start = ((bf16[64,24,512]{2,1,0:T(8,128)(2,1)}), bf16[64,24,512]{2,1,0:T(8,128)(2,1)S(1)}, u32[]{:S(2)}, u32[]{:S(2)}) async-start(bf16[64,24,512]{2,1,0:T(8,128)(2,1)} %bitcast.14), calls=%async_computation | async-start | bytes 3145728 | tf_op jit(solution)/shard_map/all_to_all | solution.py:339
  17.6 2.4 %collective-permute-start.3 = (bf16[2,1024,128]{2,1,0:T(8,128)(2,1)S(1)}, bf16[2,1024,128]{2,1,0:T(8,128)(2,1)S(1)}, u32[]{:S(2)}, u32[]{:S(2)}) collective-permute-start(bf16[2,1024,128]{2,1,0:T(8,128)(2,1)S(1)} %copy-done.3), channel_id=1, source_target_pairs={{0,1},{1,2},{2,3},{3,0},{4,5},{5,6},{6,7},{7,4},{8,9},{9,10},{10,1... | collective-permute-start | bytes 1572872 | tf_op jit(solution)/shard_map/ppermute | solution.py:325
  20.0 3.2 %collective-permute-start.6 = (bf16[2,128,1024]{2,1,0:T(8,128)(2,1)S(1)}, bf16[2,128,1024]{2,1,0:T(8,128)(2,1)S(1)}, u32[]{:S(2)}, u32[]{:S(2)}) collective-permute-start(bf16[2,128,1024]{2,1,0:T(8,128)(2,1)S(1)} %copy-done.4), channel_id=1, source_target_pairs={{0,1},{1,2},{2,3},{3,0},{4,5},{5,6},{6,7},{7,4},{8,9},{9,10},{10,1... | collective-permute-start | bytes 1572872 | tf_op jit(solution)/shard_map/ppermute | solution.py:325
  23.3 9.5 %collective-permute-done.1.refs_3_ = bf16[2,1024,128]{2,1,0:T(8,128)(2,1)S(1)} collective-permute-done((bf16[2,1024,128]{2,1,0:T(8,128)(2,1)S(1)}, bf16[2,1024,128]{2,1,0:T(8,128)(2,1)S(1)}, u32[]{:S(2)}, u32[]{:S(2)}) %collective-permute-start.1) | collective-permute-done | bytes 524320 | tf_op jit(solution)/shard_map/ppermute | solution.py:326
  32.9 11.1 %collective-permute-done.7.refs_11_ = bf16[2,128,1024]{2,1,0:T(8,128)(2,1)S(1)} collective-permute-done((bf16[2,128,1024]{2,1,0:T(8,128)(2,1)S(1)}, bf16[2,128,1024]{2,1,0:T(8,128)(2,1)S(1)}, u32[]{:S(2)}, u32[]{:S(2)}) %collective-permute-start.7) | collective-permute-done | bytes 524320 | tf_op jit(solution)/shard_map/ppermute | solution.py:326
  44.0 2.1 %collective-permute-start.8 = (bf16[1,128,1024]{2,1,0:T(8,128)(2,1)S(1)}, bf16[1,128,1024]{2,1,0:T(8,128)(2,1)S(1)}, u32[]{:S(2)}, u32[]{:S(2)}) collective-permute-start(bf16[1,128,1024]{2,1,0:T(8,128)(2,1)S(1)} %slice.24), channel_id=1, source_target_pairs={{0,3},{1,0},{2,1},{3,2},{4,7},{5,4},{6,5},{7,6},{8,11},{9,8},{10,9... | collective-permute-start | bytes 786440 | tf_op jit(solution)/shard_map/ppermute | solution.py:329
  46.2 8.7 %collective-permute-done.refs_2_ = bf16[2,1024,128]{2,1,0:T(8,128)(2,1)S(1)} collective-permute-done((bf16[2,1024,128]{2,1,0:T(8,128)(2,1)S(1)}, bf16[2,1024,128]{2,1,0:T(8,128)(2,1)S(1)}, u32[]{:S(2)}, u32[]{:S(2)}) %collective-permute-start) | collective-permute-done | bytes 524320 | tf_op jit(solution)/shard_map/ppermute | solution.py:325
  54.8 3.6 %collective-permute-start.9 = (bf16[1,128,1024]{2,1,0:T(8,128)(2,1)S(1)}, bf16[1,128,1024]{2,1,0:T(8,128)(2,1)S(1)}, u32[]{:S(2)}, u32[]{:S(2)}) collective-permute-start(bf16[1,128,1024]{2,1,0:T(8,128)(2,1)S(1)} %slice.25), channel_id=1, source_target_pairs={{0,1},{1,2},{2,3},{3,0},{4,5},{5,6},{6,7},{7,4},{8,9},{9,10},{10,1... | collective-permute-start | bytes 786440 | tf_op jit(solution)/shard_map/ppermute | solution.py:330
  58.5 12.8 %collective-permute-done.8.refs_12_ = bf16[1,128,1024]{2,1,0:T(8,128)(2,1)S(1)} collective-permute-done((bf16[1,128,1024]{2,1,0:T(8,128)(2,1)S(1)}, bf16[1,128,1024]{2,1,0:T(8,128)(2,1)S(1)}, u32[]{:S(2)}, u32[]{:S(2)}) %collective-permute-start.8) | collective-permute-done | bytes 262176 | tf_op jit(solution)/shard_map/ppermute | solution.py:329
  73.4 8.8 %shard_map.111 = s16[3584,128]{1,0:T(8,128)(2,1)} custom-call(bf16[1536,512]{1,0:T(8,128)(2,1)} %bitcast.10, bf16[2,1024,128]{2,1,0:T(8,128)(2,1)} %refs_2_.3, bf16[2,1024,128]{2,1,0:T(8,128)(2,1)} %copy-done.13, bf16[2,1024,128]{2,1,0:T(8,128)(2,1)} %copy-done.11, bf16[2,1024,128]{2,1,0:T(8,128)(2,1)} %copy-done.15, bf16[2,1024,128]{2,1,0:T(8,128)(2,1)} %refs_3_.7, ...), custom_call_target="tpu_custom_call" | custom-call | tf_op jit(solution)/shard_map/pallas_call | solution.py:312
  82.2 10.4 %all-to-all-start.1 = ((s16[64,56,128]{2,1,0:T(8,128)(2,1)}), s16[64,56,128]{2,1,0:T(8,128)(2,1)S(1)}, u32[]{:S(2)}, u32[]{:S(2)}) async-start(s16[64,56,128]{2,1,0:T(8,128)(2,1)} %bitcast.12), calls=%async_computation.1 | async-start | bytes 1835008 | tf_op jit(solution)/shard_map/all_to_all | solution.py:360
  93.9 3.2 %collective-permute-start.18 = (bf16[768,512]{1,0:T(8,128)(2,1)}, bf16[768,512]{1,0:T(8,128)(2,1)S(1)}, u32[]{:S(2)}, u32[]{:S(2)}) collective-permute-start(bf16[768,512]{1,0:T(8,128)(2,1)} %bitcast.9), channel_id=1, source_target_pairs={{0,1},{1,2},{2,3},{3,0},{4,5},{5,6},{6,7},{7,4},{8,9},{9,10},{10,1... | collective-permute-start | bytes 2359304 | tf_op jit(solution)/shard_map/ppermute | solution.py:346
  99.2 16.6 %collective-permute-done.16.refs_1_ = bf16[768,512]{1,0:T(8,128)(2,1)S(1)} collective-permute-done((bf16[768,512]{1,0:T(8,128)(2,1)}, bf16[768,512]{1,0:T(8,128)(2,1)S(1)}, u32[]{:S(2)}, u32[]{:S(2)}) %collective-permute-start.16) | collective-permute-done | bytes 786464 | tf_op jit(solution)/shard_map/ppermute | solution.py:345
  115.7 3.2 %collective-permute-start.19 = (bf16[768,512]{1,0:T(8,128)(2,1)S(1)}, bf16[768,512]{1,0:T(8,128)(2,1)}, u32[]{:S(2)}, u32[]{:S(2)}) collective-permute-start(bf16[768,512]{1,0:T(8,128)(2,1)S(1)} %collective-permute-done.18.refs_2_), channel_id=1, source_target_pairs={{0,1},{1,2},{2,3},{3,0},{4,5},{5,6},{6,7},{7,4},{8,9},{9,10},{10,1... | collective-permute-start | bytes 2359304 | tf_op jit(solution)/shard_map/ppermute | solution.py:350
  119.9 3.6 %shard_map.112 = (s16[72,1152]{1,0:T(8,128)(2,1)}, s16[72,1152]{1,0:T(8,128)(2,1)}, s16[72,1152]{1,0:T(8,128)(2,1)}, s16[72,1152]{1,0:T(8,128)(2,1)}) custom-call(s32[1]{0:T(128)} %bitcast.refs_0_, s16[3584,128]{1,0:T(8,128)(2,1)} %bitcast.13, bf16[2,384,256]{2,1,0:T(8,128)(2,1)} %get-tuple-element.23.refs_2_), custom_call_target="tpu_custom_call" | custom-call | tf_op jit(solution)/shard_map/pallas_call | solution.py:312
  123.5 2.5 %collective-permute-start.10 = (s16[72,1152]{1,0:T(8,128)(2,1)}, s16[72,1152]{1,0:T(8,128)(2,1)S(1)}, u32[]{:S(2)}, u32[]{:S(2)}) collective-permute-start(s16[72,1152]{1,0:T(8,128)(2,1)} %get-tuple-element.25), channel_id=1, source_target_pairs={{0,1},{1,2},{2,3},{3,0},{4,5},{5,6},{6,7},{7,4},{8,9},{9,10},{10,1... | collective-permute-start | bytes 497672 | tf_op jit(solution)/shard_map/ppermute | solution.py:373
  126.0 25.5 %collective-permute-done.10.from_left = s16[72,1152]{1,0:T(8,128)(2,1)S(1)} collective-permute-done((s16[72,1152]{1,0:T(8,128)(2,1)}, s16[72,1152]{1,0:T(8,128)(2,1)S(1)}, u32[]{:S(2)}, u32[]{:S(2)}) %collective-permute-start.10) | collective-permute-done | bytes 165920 | tf_op jit(solution)/shard_map/ppermute | solution.py:373
  153.2 5.5 %collective-permute-done.11.from_right = s16[72,1152]{1,0:T(8,128)(2,1)S(1)} collective-permute-done((s16[72,1152]{1,0:T(8,128)(2,1)}, s16[72,1152]{1,0:T(8,128)(2,1)S(1)}, u32[]{:S(2)}, u32[]{:S(2)}) %collective-permute-start.11) | collective-permute-done | bytes 165920 | tf_op jit(solution)/shard_map/ppermute | solution.py:374
  160.5 5.2 %collective-permute-done.12.from_opposite = s16[72,1152]{1,0:T(8,128)(2,1)S(1)} collective-permute-done((s16[72,1152]{1,0:T(8,128)(2,1)}, s16[72,1152]{1,0:T(8,128)(2,1)S(1)}, u32[]{:S(2)}, u32[]{:S(2)}) %collective-permute-start.12) | collective-permute-done | bytes 165920 | tf_op jit(solution)/shard_map/ppermute | solution.py:375
  171.3 2.3 %collective-permute-start.13 = (bf16[64,1024]{1,0:T(8,128)(2,1)}, bf16[64,1024]{1,0:T(8,128)(2,1)S(1)}, u32[]{:S(2)}, u32[]{:S(2)}) collective-permute-start(bf16[64,1024]{1,0:T(8,128)(2,1)} %get-tuple-element.28.refs_1_), channel_id=1, source_target_pairs={{0,1},{1,2},{2,3},{3,0},{4,5},{5,6},{6,7},{7,4},{8,9},{9,10},{10,1... | collective-permute-start | bytes 393224 | tf_op jit(solution)/shard_map/ppermute | solution.py:383
  173.6 7.9 %shard_map.115 = (f32[2,1024,128]{2,1,0:T(8,128)}, f32[2,1024,128]{2,1,0:T(8,128)}, f32[2,128,1024]{2,1,0:T(8,128)}) custom-call(bf16[1536,512]{1,0:T(8,128)(2,1)} %bitcast.11, bf16[768,512]{1,0:T(8,128)(2,1)} %copy-done.8, bf16[768,512]{1,0:T(8,128)(2,1)} %copy-done.9, bf16[2,1024,128]{2,1,0:T(8,128)(2,1)} %refs_2_.3, bf16[2,1024,128]{2,1,0:T(8,128)(2,1)} %refs_3_.7, ...), custom_call_target="tpu_custom_call" | custom-call | tf_op jit(solution)/shard_map/pallas_call | solution.py:312
  181.5 7.0 %shard_map.116 = (f32[2,1024,128]{2,1,0:T(8,128)}, f32[2,1024,128]{2,1,0:T(8,128)}, f32[2,128,1024]{2,1,0:T(8,128)}) custom-call(bf16[768,512]{1,0:T(8,128)(2,1)} %collective-permute-done.20.refs_0_, bf16[768,512]{1,0:T(8,128)(2,1)} %collective-permute-done.21.refs_1_, bf16[2,1024,128]{2,1,0:T(8,128)(2,1)} %refs_2_.3, bf16[2,1024,128]{2,1,0:T(8,128)(2,1)} %refs_3_.7, ...), custom_call_target="tpu_custom_call" | custom-call | tf_op jit(solution)/shard_map/pallas_call | solution.py:312
  189.4 7.0 %shard_map.117 = (f32[2,1024,128]{2,1,0:T(8,128)}, f32[2,1024,128]{2,1,0:T(8,128)}, f32[2,128,1024]{2,1,0:T(8,128)}) custom-call(bf16[768,512]{1,0:T(8,128)(2,1)} %copy-done.10, bf16[768,512]{1,0:T(8,128)(2,1)} %collective-permute-done.19.refs_1_, bf16[2,1024,128]{2,1,0:T(8,128)(2,1)} %refs_2_.3, bf16[2,1024,128]{2,1,0:T(8,128)(2,1)} %refs_3_.7, ...), custom_call_target="tpu_custom_call" | custom-call | tf_op jit(solution)/shard_map/pallas_call | solution.py:312
  (83 shorter events, 20.7 us)
Async XLA Ops:
  4.4 67.8 %all-to-all-start = ((bf16[64,24,512]{2,1,0:T(8,128)(2,1)}), bf16[64,24,512]{2,1,0:T(8,128)(2,1)S(1)}, u32[]{:S(2)}, u32[]{:S(2)}) async-start(bf16[64,24,512]{2,1,0:T(8,128)(2,1)} %bitcast.14), calls=%async_computation | async-start | bytes 3145728 | tf_op jit(solution)/shard_map/all_to_all | solution.py:339
  16.7 16.1 %collective-permute-start.1 = (bf16[2,1024,128]{2,1,0:T(8,128)(2,1)S(1)}, bf16[2,1024,128]{2,1,0:T(8,128)(2,1)S(1)}, u32[]{:S(2)}, u32[]{:S(2)}) collective-permute-start(bf16[2,1024,128]{2,1,0:T(8,128)(2,1)S(1)} %copy-done.2), channel_id=1, source_target_pairs={{0,3},{1,0},{2,1},{3,2},{4,7},{5,4},{6,5},{7,6},{8,11},{9,8},{10,9... | collective-permute-start | bytes 1572872 | tf_op jit(solution)/shard_map/ppermute | solution.py:326
  17.6 15.2 %collective-permute-start.3 = (bf16[2,1024,128]{2,1,0:T(8,128)(2,1)S(1)}, bf16[2,1024,128]{2,1,0:T(8,128)(2,1)S(1)}, u32[]{:S(2)}, u32[]{:S(2)}) collective-permute-start(bf16[2,1024,128]{2,1,0:T(8,128)(2,1)S(1)} %copy-done.3), channel_id=1, source_target_pairs={{0,1},{1,2},{2,3},{3,0},{4,5},{5,6},{6,7},{7,4},{8,9},{9,10},{10,1... | collective-permute-start | bytes 1572872 | tf_op jit(solution)/shard_map/ppermute | solution.py:325
  20.0 24.0 %collective-permute-start.7 = (bf16[2,128,1024]{2,1,0:T(8,128)(2,1)S(1)}, bf16[2,128,1024]{2,1,0:T(8,128)(2,1)S(1)}, u32[]{:S(2)}, u32[]{:S(2)}) collective-permute-start(bf16[2,128,1024]{2,1,0:T(8,128)(2,1)S(1)} %copy-done.4), channel_id=1, source_target_pairs={{0,3},{1,0},{2,1},{3,2},{4,7},{5,4},{6,5},{7,6},{8,11},{9,8},{10,9... | collective-permute-start | bytes 1572872 | tf_op jit(solution)/shard_map/ppermute | solution.py:326
  20.0 24.0 %collective-permute-start.6 = (bf16[2,128,1024]{2,1,0:T(8,128)(2,1)S(1)}, bf16[2,128,1024]{2,1,0:T(8,128)(2,1)S(1)}, u32[]{:S(2)}, u32[]{:S(2)}) collective-permute-start(bf16[2,128,1024]{2,1,0:T(8,128)(2,1)S(1)} %copy-done.4), channel_id=1, source_target_pairs={{0,1},{1,2},{2,3},{3,0},{4,5},{5,6},{6,7},{7,4},{8,9},{9,10},{10,1... | collective-permute-start | bytes 1572872 | tf_op jit(solution)/shard_map/ppermute | solution.py:325
  23.2 31.6 %collective-permute-start = (bf16[2,1024,128]{2,1,0:T(8,128)(2,1)S(1)}, bf16[2,1024,128]{2,1,0:T(8,128)(2,1)S(1)}, u32[]{:S(2)}, u32[]{:S(2)}) collective-permute-start(bf16[2,1024,128]{2,1,0:T(8,128)(2,1)S(1)} %copy-done.2), channel_id=1, source_target_pairs={{0,1},{1,2},{2,3},{3,0},{4,5},{5,6},{6,7},{7,4},{8,9},{9,10},{10,1... | collective-permute-start | bytes 1572872 | tf_op jit(solution)/shard_map/ppermute | solution.py:325
  32.8 25.7 %collective-permute-start.4 = (bf16[2,1024,128]{2,1,0:T(8,128)(2,1)S(1)}, bf16[2,1024,128]{2,1,0:T(8,128)(2,1)S(1)}, u32[]{:S(2)}, u32[]{:S(2)}) collective-permute-start(bf16[2,1024,128]{2,1,0:T(8,128)(2,1)S(1)} %copy-done.3), channel_id=1, source_target_pairs={{0,3},{1,0},{2,1},{3,2},{4,7},{5,4},{6,5},{7,6},{8,11},{9,8},{10,9... | collective-permute-start | bytes 1572872 | tf_op jit(solution)/shard_map/ppermute | solution.py:326
  32.8 38.5 %collective-permute-start.2 = (bf16[2,1024,128]{2,1,0:T(8,128)(2,1)S(1)}, bf16[2,1024,128]{2,1,0:T(8,128)(2,1)S(1)}, u32[]{:S(2)}, u32[]{:S(2)}) collective-permute-start(bf16[2,1024,128]{2,1,0:T(8,128)(2,1)S(1)} %collective-permute-done.1.refs_3_), channel_id=1, source_target_pairs={{0,3},{1,0},{2,1},{3,2},{4,7},{5,4},{6,5},{7,6},{8,11},{9,8},{10,9... | collective-permute-start | bytes 1572872 | tf_op jit(solution)/shard_map/ppermute | solution.py:327
  44.0 28.2 %collective-permute-start.5 = (bf16[2,1024,128]{2,1,0:T(8,128)(2,1)S(1)}, bf16[2,1024,128]{2,1,0:T(8,128)(2,1)}, u32[]{:S(2)}, u32[]{:S(2)}) collective-permute-start(bf16[2,1024,128]{2,1,0:T(8,128)(2,1)S(1)} %collective-permute-done.3.refs_6_), channel_id=1, source_target_pairs={{0,1},{1,2},{2,3},{3,0},{4,5},{5,6},{6,7},{7,4},{8,9},{9,10},{10,1... | collective-permute-start | bytes 1572872 | tf_op jit(solution)/shard_map/ppermute | solution.py:328
  44.0 27.2 %collective-permute-start.8 = (bf16[1,128,1024]{2,1,0:T(8,128)(2,1)S(1)}, bf16[1,128,1024]{2,1,0:T(8,128)(2,1)S(1)}, u32[]{:S(2)}, u32[]{:S(2)}) collective-permute-start(bf16[1,128,1024]{2,1,0:T(8,128)(2,1)S(1)} %slice.24), channel_id=1, source_target_pairs={{0,3},{1,0},{2,1},{3,2},{4,7},{5,4},{6,5},{7,6},{8,11},{9,8},{10,9... | collective-permute-start | bytes 786440 | tf_op jit(solution)/shard_map/ppermute | solution.py:329
  54.8 16.4 %collective-permute-start.9 = (bf16[1,128,1024]{2,1,0:T(8,128)(2,1)S(1)}, bf16[1,128,1024]{2,1,0:T(8,128)(2,1)S(1)}, u32[]{:S(2)}, u32[]{:S(2)}) collective-permute-start(bf16[1,128,1024]{2,1,0:T(8,128)(2,1)S(1)} %slice.25), channel_id=1, source_target_pairs={{0,1},{1,2},{2,3},{3,0},{4,5},{5,6},{6,7},{7,4},{8,9},{9,10},{10,1... | collective-permute-start | bytes 786440 | tf_op jit(solution)/shard_map/ppermute | solution.py:330
  82.2 36.8 %all-to-all-start.1 = ((s16[64,56,128]{2,1,0:T(8,128)(2,1)}), s16[64,56,128]{2,1,0:T(8,128)(2,1)S(1)}, u32[]{:S(2)}, u32[]{:S(2)}) async-start(s16[64,56,128]{2,1,0:T(8,128)(2,1)} %bitcast.12), calls=%async_computation.1 | async-start | bytes 1835008 | tf_op jit(solution)/shard_map/all_to_all | solution.py:360
  93.9 21.8 %collective-permute-start.16 = (bf16[768,512]{1,0:T(8,128)(2,1)}, bf16[768,512]{1,0:T(8,128)(2,1)S(1)}, u32[]{:S(2)}, u32[]{:S(2)}) collective-permute-start(bf16[768,512]{1,0:T(8,128)(2,1)} %bitcast.8), channel_id=1, source_target_pairs={{0,3},{1,0},{2,1},{3,2},{4,7},{5,4},{6,5},{7,6},{8,11},{9,8},{10,9... | collective-permute-start | bytes 2359304 | tf_op jit(solution)/shard_map/ppermute | solution.py:345
  93.9 21.8 %collective-permute-start.18 = (bf16[768,512]{1,0:T(8,128)(2,1)}, bf16[768,512]{1,0:T(8,128)(2,1)S(1)}, u32[]{:S(2)}, u32[]{:S(2)}) collective-permute-start(bf16[768,512]{1,0:T(8,128)(2,1)} %bitcast.9), channel_id=1, source_target_pairs={{0,1},{1,2},{2,3},{3,0},{4,5},{5,6},{6,7},{7,4},{8,9},{9,10},{10,1... | collective-permute-start | bytes 2359304 | tf_op jit(solution)/shard_map/ppermute | solution.py:346
  97.1 73.2 %collective-permute-start.21 = (bf16[768,512]{1,0:T(8,128)(2,1)}, bf16[768,512]{1,0:T(8,128)(2,1)}, u32[]{:S(2)}, u32[]{:S(2)}) collective-permute-start(bf16[768,512]{1,0:T(8,128)(2,1)} %bitcast.8), channel_id=1, source_target_pairs={{0,1},{1,2},{2,3},{3,0},{4,5},{5,6},{6,7},{7,4},{8,9},{9,10},{10,1... | collective-permute-start | bytes 2359304 | tf_op jit(solution)/shard_map/ppermute | solution.py:348
  98.8 72.5 %collective-permute-start.20 = (bf16[768,512]{1,0:T(8,128)(2,1)}, bf16[768,512]{1,0:T(8,128)(2,1)}, u32[]{:S(2)}, u32[]{:S(2)}) collective-permute-start(bf16[768,512]{1,0:T(8,128)(2,1)} %bitcast.9), channel_id=1, source_target_pairs={{0,3},{1,0},{2,1},{3,2},{4,7},{5,4},{6,5},{7,6},{8,11},{9,8},{10,9... | collective-permute-start | bytes 2359304 | tf_op jit(solution)/shard_map/ppermute | solution.py:347
  115.7 72.8 %collective-permute-start.17 = (bf16[768,512]{1,0:T(8,128)(2,1)S(1)}, bf16[768,512]{1,0:T(8,128)(2,1)S(1)}, u32[]{:S(2)}, u32[]{:S(2)}) collective-permute-start(bf16[768,512]{1,0:T(8,128)(2,1)S(1)} %collective-permute-done.16.refs_1_), channel_id=1, source_target_pairs={{0,3},{1,0},{2,1},{3,2},{4,7},{5,4},{6,5},{7,6},{8,11},{9,8},{10,9... | collective-permute-start | bytes 2359304 | tf_op jit(solution)/shard_map/ppermute | solution.py:349
  115.7 72.8 %collective-permute-start.19 = (bf16[768,512]{1,0:T(8,128)(2,1)S(1)}, bf16[768,512]{1,0:T(8,128)(2,1)}, u32[]{:S(2)}, u32[]{:S(2)}) collective-permute-start(bf16[768,512]{1,0:T(8,128)(2,1)S(1)} %collective-permute-done.18.refs_2_), channel_id=1, source_target_pairs={{0,1},{1,2},{2,3},{3,0},{4,5},{5,6},{6,7},{7,4},{8,9},{9,10},{10,1... | collective-permute-start | bytes 2359304 | tf_op jit(solution)/shard_map/ppermute | solution.py:350
  123.5 28.0 %collective-permute-start.10 = (s16[72,1152]{1,0:T(8,128)(2,1)}, s16[72,1152]{1,0:T(8,128)(2,1)S(1)}, u32[]{:S(2)}, u32[]{:S(2)}) collective-permute-start(s16[72,1152]{1,0:T(8,128)(2,1)} %get-tuple-element.25), channel_id=1, source_target_pairs={{0,1},{1,2},{2,3},{3,0},{4,5},{5,6},{6,7},{7,4},{8,9},{9,10},{10,1... | collective-permute-start | bytes 497672 | tf_op jit(solution)/shard_map/ppermute | solution.py:373
  151.5 7.2 %collective-permute-start.11 = (s16[72,1152]{1,0:T(8,128)(2,1)}, s16[72,1152]{1,0:T(8,128)(2,1)S(1)}, u32[]{:S(2)}, u32[]{:S(2)}) collective-permute-start(s16[72,1152]{1,0:T(8,128)(2,1)} %get-tuple-element.26), channel_id=1, source_target_pairs={{0,3},{1,0},{2,1},{3,2},{4,7},{5,4},{6,5},{7,6},{8,11},{9,8},{10,9... | collective-permute-start | bytes 497672 | tf_op jit(solution)/shard_map/ppermute | solution.py:374
  158.7 7.1 %collective-permute-start.12 = (s16[72,1152]{1,0:T(8,128)(2,1)}, s16[72,1152]{1,0:T(8,128)(2,1)S(1)}, u32[]{:S(2)}, u32[]{:S(2)}) collective-permute-start(s16[72,1152]{1,0:T(8,128)(2,1)} %get-tuple-element.27), channel_id=1, source_target_pairs={{0,2},{1,3},{2,0},{3,1},{4,6},{5,7},{6,4},{7,5},{8,10},{9,11},{10,... | collective-permute-start | bytes 497672 | tf_op jit(solution)/shard_map/ppermute | solution.py:375
  168.5 28.0 %collective-permute-start.15 = (bf16[64,1024]{1,0:T(8,128)(2,1)}, bf16[64,1024]{1,0:T(8,128)(2,1)S(1)}, u32[]{:S(2)}, u32[]{:S(2)}) collective-permute-start(bf16[64,1024]{1,0:T(8,128)(2,1)} %get-tuple-element.28.refs_1_), channel_id=1, source_target_pairs={{0,2},{1,3},{2,0},{3,1},{4,6},{5,7},{6,4},{7,5},{8,10},{9,11},{10,... | collective-permute-start | bytes 393224 | tf_op jit(solution)/shard_map/ppermute | solution.py:385
  170.3 26.1 %collective-permute-start.14 = (bf16[64,1024]{1,0:T(8,128)(2,1)}, bf16[64,1024]{1,0:T(8,128)(2,1)S(1)}, u32[]{:S(2)}, u32[]{:S(2)}) collective-permute-start(bf16[64,1024]{1,0:T(8,128)(2,1)} %get-tuple-element.28.refs_1_), channel_id=1, source_target_pairs={{0,3},{1,0},{2,1},{3,2},{4,7},{5,4},{6,5},{7,6},{8,11},{9,8},{10,9... | collective-permute-start | bytes 393224 | tf_op jit(solution)/shard_map/ppermute | solution.py:384
  171.3 25.2 %collective-permute-start.13 = (bf16[64,1024]{1,0:T(8,128)(2,1)}, bf16[64,1024]{1,0:T(8,128)(2,1)S(1)}, u32[]{:S(2)}, u32[]{:S(2)}) collective-permute-start(bf16[64,1024]{1,0:T(8,128)(2,1)} %get-tuple-element.28.refs_1_), channel_id=1, source_target_pairs={{0,1},{1,2},{2,3},{3,0},{4,5},{5,6},{6,7},{7,4},{8,9},{9,10},{10,1... | collective-permute-start | bytes 393224 | tf_op jit(solution)/shard_map/ppermute | solution.py:383
  (24 other events, 357.8 us)
